TPU v7x, 32 devices: a whole 2x2x4 slice. The times are simulated.
32 devices in a mesh: ep: 32 (over z, y, x, core).
Axes of the slice: x: 2, y: 2, z: 4, core: 2. Of those that a mesh axis runs over, the one named last changes fastest.
Arguments:
- tokens: bfloat16 [256, 2048], P('ep'), may hold values from -6 to 6
- premix_gain: float32 [2048], replicated, may hold values from 0.1 to 1.9
- postmix_gain: float32 [2048], replicated, may hold values from 0.1 to 1.9
- prefeed_gain: float32 [2048], replicated, may hold values from 0.1 to 1.9
- postfeed_gain: float32 [2048], replicated, may hold values from 0.1 to 1.9
- query_weight: bfloat16 [2048, 1024], P('ep'), may hold values from -0.125 to 0.125
- key_weight: bfloat16 [2048, 1024], P('ep'), may hold values from -0.125 to 0.125
- value_weight: bfloat16 [2048, 1024], P('ep'), may hold values from -0.125 to 0.125
- outgate_weight: bfloat16 [2048, 1024], P('ep'), may hold values from -0.125 to 0.125
- ingate_weight: bfloat16 [2048, 8], replicated, may hold values from -0.125 to 0.125
- forget_weight: bfloat16 [2048, 8], replicated, may hold values from -0.125 to 0.125
- ingate_bias: float32 [8], replicated, may hold values from -1 to 1
- forget_bias: float32 [8], replicated, may hold values from -1 to 5
- memory_state: float32 [256, 8, 128, 128], P('ep'), may hold values from -1.25 to 1.25
- normalizer: float32 [256, 8, 128], P('ep'), may hold values from -1.75 to 1.75
- stabilizer: float32 [256, 8], P('ep'), may hold values from -2 to 2
- output_weight: bfloat16 [1024, 2048], P(None, 'ep'), may hold values from -0.1875 to 0.1875
- expert_ids: int32 [256, 6], P('ep'), may hold values from 0 to 31, all different within a row; in each aligned block of 8 rows (0 to 7, 8 to 15, ...) at most 4 rows name the same one
- route_weights: float32 [256, 6], P('ep'), may hold values from 0.2 to 0.8
- expert_gate: bfloat16 [32, 2048, 512], P('ep'), may hold values from -0.125 to 0.125
- expert_up: bfloat16 [32, 2048, 512], P('ep'), may hold values from -0.125 to 0.125
- expert_down: bfloat16 [32, 512, 2048], P('ep'), may hold values from -0.25 to 0.25
- shared_gate: bfloat16 [2048, 512], replicated, may hold values from -0.125 to 0.125
- shared_up: bfloat16 [2048, 512], replicated, may hold values from -0.125 to 0.125
- shared_down: bfloat16 [512, 2048], replicated, may hold values from -0.25 to 0.25
Outputs:
- next_tokens: bfloat16 [256, 2048], P('ep')
- next_memory: float32 [256, 8, 128, 128], P('ep')
- next_normalizer: float32 [256, 8, 128], P('ep')
- next_stabilizer: float32 [256, 8], P('ep')
Inputs may be any that keep to these rules, and one draw needn't show every extreme that they name: `expert_ids`: each row names 6 different experts. Among the rows of one device no expert is named more than 4 times, and in every draw some expert is named exactly 4 times by the rows of some device.
All inputs are finite; a program needn't handle non-finite values.
Results may differ from a plain program's by a relative error of at most 0.0097.
Values may be sent and summed in bfloat16 or wider, within the bound.
No kernel may reach another device: no remote copies, remote signals or barrier semaphores. Data moves between devices by JAX's collectives and lax.ppermute only.
A program may use at most 128 MiB of HBM per device.

v0:
```python
import jax
import jax.numpy as jnp
from jax import lax
from jax.sharding import PartitionSpec as P

epsilon = 1e-06


def rms_scale(values, gain_row):
    return (
        values * lax.rsqrt(jnp.mean(values * values, axis=-1, keepdims=True) + epsilon) * gain_row
    )


def rounded(values):
    return lax.optimization_barrier(values.astype(jnp.bfloat16))


def memory_step(
    queries,
    key_rows,
    value_rows,
    out_gate,
    input_pre,
    forget_pre,
    memory_state,
    normalizer,
    stabilizer,
):
    sequences = queries.shape[0]
    head_count = memory_state.shape[1]
    head_width = memory_state.shape[2]
    query_heads = queries.astype(jnp.float32).reshape(sequences, head_count, head_width)
    key_heads = key_rows.astype(jnp.float32).reshape(
        sequences, head_count, head_width
    ) * head_width ** (-0.5)
    value_heads = value_rows.astype(jnp.float32).reshape(sequences, head_count, head_width)
    carried = jax.nn.log_sigmoid(forget_pre) + stabilizer
    next_stabilizer = jnp.maximum(carried, input_pre)
    keep_old = jnp.exp(carried - next_stabilizer)
    write_new = jnp.exp(input_pre - next_stabilizer)
    local_score = write_new * jnp.sum(query_heads * key_heads, axis=-1)
    read_memory = jnp.einsum(
        "shvk,shk->shv", memory_state, query_heads, precision=lax.Precision.HIGHEST
    )
    numerator = keep_old[..., None] * read_memory + local_score[..., None] * value_heads
    denominator = keep_old * jnp.sum(normalizer * query_heads, axis=-1) + local_score
    memory_read = numerator / jnp.maximum(jnp.abs(denominator), 1.0)[..., None]
    gated_out = (
        jax.nn.sigmoid(out_gate.astype(jnp.float32))
        * memory_read.reshape(sequences, head_count * head_width)
    ).astype(jnp.bfloat16)
    next_memory = (
        keep_old[..., None, None] * memory_state
        + write_new[..., None, None] * value_heads[..., :, None] * key_heads[..., None, :]
    )
    next_normalizer = keep_old[..., None] * normalizer + write_new[..., None] * key_heads
    return (gated_out, next_memory, next_normalizer, next_stabilizer)


def expert_rows(row_block, gate_weight, up_weight, down_weight):
    gate_values = jnp.dot(row_block, gate_weight, preferred_element_type=jnp.float32)
    up_values = jnp.dot(row_block, up_weight, preferred_element_type=jnp.float32)
    inner_rows = (jax.nn.silu(gate_values) * up_values).astype(jnp.bfloat16)
    return jnp.dot(inner_rows, down_weight, preferred_element_type=jnp.float32)


def on_device(
    tokens,
    premix_gain,
    postmix_gain,
    prefeed_gain,
    postfeed_gain,
    query_weight,
    key_weight,
    value_weight,
    outgate_weight,
    ingate_weight,
    forget_weight,
    ingate_bias,
    forget_bias,
    memory_state,
    normalizer,
    stabilizer,
    output_weight,
    expert_ids,
    route_weights,
    expert_gate,
    expert_up,
    expert_down,
    shared_gate,
    shared_up,
    shared_down,
):
    sequences = tokens.shape[0]
    model_width = tokens.shape[1]
    memory_width = query_weight.shape[1]
    devices = lax.axis_size("ep")
    residual = tokens.astype(jnp.float32)
    normed = rms_scale(residual, premix_gain).astype(jnp.bfloat16)
    columns = (
        lax.all_to_all(query_weight, "ep", split_axis=1, concat_axis=0, tiled=True),
        lax.all_to_all(key_weight, "ep", split_axis=1, concat_axis=0, tiled=True),
        lax.all_to_all(value_weight, "ep", split_axis=1, concat_axis=0, tiled=True),
        lax.all_to_all(outgate_weight, "ep", split_axis=1, concat_axis=0, tiled=True),
    )
    stacked = jnp.concatenate(columns, axis=1)
    column_width = memory_width // devices
    piece_rows = lax.all_gather(normed, "ep", axis=0, tiled=True)
    product = jnp.dot(piece_rows, stacked, preferred_element_type=jnp.float32).astype(jnp.bfloat16)
    gathered = product.reshape(piece_rows.shape[0], 4, column_width)
    projected = lax.all_to_all(gathered, "ep", split_axis=0, concat_axis=2, tiled=True)
    input_pre = jnp.dot(normed, ingate_weight, preferred_element_type=jnp.float32) + ingate_bias
    forget_pre = jnp.dot(normed, forget_weight, preferred_element_type=jnp.float32) + forget_bias
    gated_out, next_memory, next_normalizer, next_stabilizer = memory_step(
        projected[:, 0],
        projected[:, 1],
        projected[:, 2],
        projected[:, 3],
        input_pre,
        forget_pre,
        memory_state,
        normalizer,
        stabilizer,
    )
    mixed_cols = jnp.dot(
        lax.all_gather(gated_out, "ep", axis=0, tiled=True),
        output_weight,
        preferred_element_type=jnp.float32,
    ).astype(jnp.bfloat16)
    mixed = lax.all_to_all(mixed_cols, "ep", split_axis=0, concat_axis=1, tiled=True)
    after_mix = rounded(residual + rms_scale(mixed.astype(jnp.float32), postmix_gain))
    after_float = after_mix.astype(jnp.float32)
    expert_input = rms_scale(after_float, prefeed_gain).astype(jnp.bfloat16)
    local_count = expert_gate.shape[0]
    experts_total = local_count * devices
    choose_count = expert_ids.shape[1]
    capacity = min(
        sequences, max(2, 2 * ((sequences * choose_count + experts_total - 1) // experts_total))
    )
    flat_ids = expert_ids.reshape(-1)
    one_hot = (flat_ids[:, None] == jnp.arange(experts_total, dtype=jnp.int32)[None, :]).astype(
        jnp.int32
    )
    earlier = jnp.cumsum(one_hot, axis=0) - one_hot
    slot_ids = jnp.sum(earlier * one_hot, axis=1)
    target = flat_ids * capacity + slot_ids
    pair_hot = (
        target[:, None] == jnp.arange(experts_total * capacity, dtype=jnp.int32)[None, :]
    ).astype(jnp.bfloat16)
    pair_rows = jnp.repeat(expert_input, choose_count, axis=0)
    outgoing = jnp.dot(pair_hot.T, pair_rows, preferred_element_type=jnp.float32).astype(
        jnp.bfloat16
    )
    outgoing = outgoing.reshape(experts_total, capacity, model_width)
    arrived = lax.all_to_all(outgoing, "ep", split_axis=0, concat_axis=0, tiled=True)
    item_count = arrived.shape[1]
    grouped = arrived.reshape(devices, local_count, item_count, model_width)
    gate_values = jnp.einsum(
        "nlid,ldf->nlif", grouped, expert_gate, preferred_element_type=jnp.float32
    )
    up_values = jnp.einsum("nlid,ldf->nlif", grouped, expert_up, preferred_element_type=jnp.float32)
    inner_rows = (jax.nn.silu(gate_values) * up_values).astype(jnp.bfloat16)
    answer = jnp.einsum(
        "nlif,lfd->nlid", inner_rows, expert_down, preferred_element_type=jnp.float32
    ).astype(jnp.bfloat16)
    answered = answer.reshape(devices * local_count, item_count, model_width)
    returned = lax.all_to_all(answered, "ep", split_axis=0, concat_axis=0, tiled=True)
    picked = jnp.dot(
        pair_hot,
        returned.reshape(experts_total * capacity, model_width),
        preferred_element_type=jnp.float32,
    )
    routed = jnp.sum(
        picked.reshape(sequences, choose_count, model_width) * route_weights[:, :, None], axis=1
    )
    shared_out = expert_rows(expert_input, shared_gate, shared_up, shared_down)
    next_tokens = (after_float + rms_scale(routed + shared_out, postfeed_gain)).astype(jnp.bfloat16)
    return (next_tokens, next_memory, next_normalizer, next_stabilizer)


def solution(mesh):
    in_specs = (
        P("ep", None),
        P(),
        P(),
        P(),
        P(),
        P("ep", None),
        P("ep", None),
        P("ep", None),
        P("ep", None),
        P(),
        P(),
        P(),
        P(),
        P("ep", None, None, None),
        P("ep", None, None),
        P("ep", None),
        P(None, "ep"),
        P("ep", None),
        P("ep", None),
        P("ep", None, None),
        P("ep", None, None),
        P("ep", None, None),
        P(),
        P(),
        P(),
    )
    out_specs = (P("ep", None), P("ep", None, None, None), P("ep", None, None), P("ep", None))
    return jax.shard_map(
        on_device, mesh=mesh, in_specs=in_specs, out_specs=out_specs, check_vma=False
    )
```

profile of v0, /device:TPU:0, one launch (start us, length us, event | category | flops | bytes accessed | tf_op | source)
XLA Modules:
  0.0 195.0 jit_solution(7154558388813392408)
XLA Ops:
  11.8 7.3 %all-to-all-start = ((bf16[32,2,1024]{2,1,0:T(2,128)(2,1)}), bf16[32,2,1024]{2,1,0:T(2,128)(2,1)S(1)}, u32[]{:S(2)}, u32[]{:S(2)}) async-start(bf16[32,2,1024]{2,1,0:T(2,128)(2,1)} %reshape.205), calls=%async_computation | async-start | bytes 262144 | tf_op jit(solution)/shard_map/all_to_all | solution.py:102
  21.0 6.3 %all-to-all-done = bf16[32,2,1024]{2,1,0:T(2,128)(2,1)S(1)} async-done(((bf16[32,2,1024]{2,1,0:T(2,128)(2,1)}), bf16[32,2,1024]{2,1,0:T(2,128)(2,1)S(1)}, u32[]{:S(2)}, u32[]{:S(2)}) %all-to-all-start) | async-done | bytes 131104 | tf_op jit(solution)/shard_map/all_to_all | solution.py:102
  27.3 2.6 %all-to-all-start.1 = ((bf16[32,2,1024]{2,1,0:T(2,128)(2,1)}), bf16[32,2,1024]{2,1,0:T(2,128)(2,1)S(1)}, u32[]{:S(2)}, u32[]{:S(2)}) async-start(bf16[32,2,1024]{2,1,0:T(2,128)(2,1)} %reshape.203), calls=%async_computation.1 | async-start | bytes 262144 | tf_op jit(solution)/shard_map/all_to_all | solution.py:103
  31.1 7.0 %all-to-all-done.1 = bf16[32,2,1024]{2,1,0:T(2,128)(2,1)S(1)} async-done(((bf16[32,2,1024]{2,1,0:T(2,128)(2,1)}), bf16[32,2,1024]{2,1,0:T(2,128)(2,1)S(1)}, u32[]{:S(2)}, u32[]{:S(2)}) %all-to-all-start.1) | async-done | bytes 131104 | tf_op jit(solution)/shard_map/all_to_all | solution.py:103
  38.1 2.6 %all-to-all-start.2 = ((bf16[32,2,1024]{2,1,0:T(2,128)(2,1)}), bf16[32,2,1024]{2,1,0:T(2,128)(2,1)S(1)}, u32[]{:S(2)}, u32[]{:S(2)}) async-start(bf16[32,2,1024]{2,1,0:T(2,128)(2,1)} %reshape.201), calls=%async_computation.2 | async-start | bytes 262144 | tf_op jit(solution)/shard_map/all_to_all | solution.py:104
  42.5 6.7 %all-to-all-done.2 = bf16[32,2,1024]{2,1,0:T(2,128)(2,1)S(1)} async-done(((bf16[32,2,1024]{2,1,0:T(2,128)(2,1)}), bf16[32,2,1024]{2,1,0:T(2,128)(2,1)S(1)}, u32[]{:S(2)}, u32[]{:S(2)}) %all-to-all-start.2) | async-done | bytes 131104 | tf_op jit(solution)/shard_map/all_to_all | solution.py:104
  49.2 2.6 %all-to-all-start.3 = ((bf16[32,2,1024]{2,1,0:T(2,128)(2,1)}), bf16[32,2,1024]{2,1,0:T(2,128)(2,1)S(1)}, u32[]{:S(2)}, u32[]{:S(2)}) async-start(bf16[32,2,1024]{2,1,0:T(2,128)(2,1)} %reshape.199), calls=%async_computation.3 | async-start | bytes 262144 | tf_op jit(solution)/shard_map/all_to_all | solution.py:105
  53.2 6.8 %all-to-all-done.3 = bf16[32,2,1024]{2,1,0:T(2,128)(2,1)S(1)} async-done(((bf16[32,2,1024]{2,1,0:T(2,128)(2,1)}), bf16[32,2,1024]{2,1,0:T(2,128)(2,1)S(1)}, u32[]{:S(2)}, u32[]{:S(2)}) %all-to-all-start.3) | async-done | bytes 131104 | tf_op jit(solution)/shard_map/all_to_all | solution.py:105
  60.7 7.7 %all-gather.2.cloned.1.call-done = bf16[256,2048]{1,0:T(8,128)(2,1)} async-done(((bf16[8,2048]{1,0:T(8,128)(2,1)}), bf16[256,2048]{1,0:T(8,128)(2,1)}) %all-gather.2.cloned.1.call-update) | async-done | bytes 1048592 | tf_op jit(solution)/shard_map/all_gather | solution.py:109
  68.4 1.7 convolution_convert_fusion.2
  71.1 3.5 %all-to-all-start.4 = ((bf16[32,2,512]{2,1,0:T(2,128)(2,1)}), bf16[32,2,512]{2,1,0:T(2,128)(2,1)S(1)}, u32[]{:S(2)}, u32[]{:S(2)}) async-start(bf16[32,2,512]{2,1,0:T(2,128)(2,1)} %reshape.207), calls=%async_computation.4 | async-start | bytes 131072 | tf_op jit(solution)/shard_map/all_to_all | solution.py:112
  75.0 7.1 %all-to-all-done.4 = bf16[32,2,512]{2,1,0:T(2,128)(2,1)S(1)} async-done(((bf16[32,2,512]{2,1,0:T(2,128)(2,1)}), bf16[32,2,512]{2,1,0:T(2,128)(2,1)S(1)}, u32[]{:S(2)}, u32[]{:S(2)}) %all-to-all-start.4) | async-done | bytes 65568 | tf_op jit(solution)/shard_map/all_to_all | solution.py:112
  82.7 5.6 %fusion.53 = f32[8,8,1,128]{3,2,1,0:T(1,128)S(1)} fusion(f32[8,8,128,128]{3,2,1,0:T(8,128)} %param.38, bf16[8,8,128,1]{2,0,1,3:T(8,128)(2,1)S(1)} %get-tuple-element.13), kind=kOutput, calls=%fused_computation.63 | convolution fusion | flops 12582912 | bytes 4243456 | tf_op jit(solution)/shard_map/shvk,shk->shv/dot_general | solution.py:43
  89.2 38.7 %all_gather.7 = bf16[256,1024]{1,0:T(8,128)(2,1)S(1)} all-gather(bf16[8,1024]{1,0:T(8,128)(2,1)S(1)} %fusion.52), channel_id=1, replica_groups=mesh['ep'=32] {'ep'}, dimensions={0}, use_global_device_ids=true | all-gather | bytes 540672 | tf_op jit(solution)/shard_map/all_gather | solution.py:127
  129.0 2.6 %all-to-all-start.5 = ((bf16[32,2,256]{2,1,0:T(2,128)(2,1)}), bf16[32,2,256]{2,1,0:T(2,128)(2,1)S(1)}, u32[]{:S(2)}, u32[]{:S(2)}) async-start(bf16[32,2,256]{2,1,0:T(2,128)(2,1)} %reshape.209), calls=%async_computation.5 | async-start | bytes 65536 | tf_op jit(solution)/shard_map/all_to_all | solution.py:131
  131.6 7.2 %all-to-all-done.5 = bf16[32,2,256]{2,1,0:T(2,128)(2,1)S(1)} async-done(((bf16[32,2,256]{2,1,0:T(2,128)(2,1)}), bf16[32,2,256]{2,1,0:T(2,128)(2,1)S(1)}, u32[]{:S(2)}, u32[]{:S(2)}) %all-to-all-start.5) | async-done | bytes 32800 | tf_op jit(solution)/shard_map/all_to_all | solution.py:131
  141.1 2.8 %all-to-all-start.6 = ((bf16[32,4,2048]{2,1,0:T(4,128)(2,1)}), bf16[32,4,2048]{2,1,0:T(4,128)(2,1)S(1)}, u32[]{:S(2)}, u32[]{:S(2)}) async-start(bf16[32,4,2048]{2,1,0:T(4,128)(2,1)} %reshape.181), calls=%async_computation.6 | async-start | bytes 1048576 | tf_op jit(solution)/shard_map/all_to_all | solution.py:156
  144.0 15.4 %all-to-all-done.6 = bf16[32,4,2048]{2,1,0:T(4,128)(2,1)S(1)} async-done(((bf16[32,4,2048]{2,1,0:T(4,128)(2,1)}), bf16[32,4,2048]{2,1,0:T(4,128)(2,1)S(1)}, u32[]{:S(2)}, u32[]{:S(2)}) %all-to-all-start.6) | async-done | bytes 524320 | tf_op jit(solution)/shard_map/all_to_all | solution.py:156
  159.4 2.2 %fusion.5 = f32[32,1,4,512]{3,0,2,1:T(8,128)S(1)} fusion(bf16[1,2048,512]{2,1,0:T(8,128)(2,1)} %param.44, bf16[32,4,2048]{2,1,0:T(4,128)(2,1)S(1)} %all-to-all-done.6), kind=kOutput, calls=%fused_computation.10 | convolution fusion | flops 268435456 | bytes 2883584 | tf_op jit(solution)/shard_map/nlid,ldf->nlif/dot_general | solution.py:159
  161.6 2.6 %convolution_convert_fusion = bf16[32,4,2048]{2,0,1:T(8,128)(2,1)S(1)} fusion(bf16[1,512,2048]{2,1,0:T(8,128)(2,1)S(1)} %copy-done, bf16[1,2048,512]{2,1,0:T(8,128)(2,1)} %param.45, bf16[32,4,2048]{2,1,0:T(4,128)(2,1)S(1)} %all-to-all-done.6, f32[32,1,4,512]{3,0,2,1:T(8,128)S(1)} %fusion.5), kind=kOutput, calls=%fused_computation.1 | convolution fusion | flops 537526272 | bytes 5505024 | tf_op jit(solution)/shard_map/nlif,lfd->nlid/dot_general | solution.py:164
  165.5 2.9 %all-to-all-start.7 = ((bf16[32,4,2048]{2,1,0:T(4,128)(2,1)}), bf16[32,4,2048]{2,1,0:T(4,128)(2,1)S(1)}, u32[]{:S(2)}, u32[]{:S(2)}) async-start(bf16[32,4,2048]{2,1,0:T(4,128)(2,1)} %copy.90), calls=%async_computation.7 | async-start | bytes 1048576 | tf_op jit(solution)/shard_map/all_to_all | solution.py:168
  168.7 4.5 %multiply_add_fusion = f32[8,8,128,128]{3,2,1,0:T(8,128)} fusion(f32[8,8,128,128]{3,2,1,0:T(8,128)} %param.38, f32[8,8,128]{2,1,0:T(8,128)S(1)} %copy-done.4, f32[8,8,128]{2,1,0:T(8,128)S(1)} %copy.93, f32[8,8]{1,0:T(8,128)S(1)} %get-tuple-element.10), kind=kLoop, calls=%fused_computation | loop fusion | flops 3145728 | bytes 8454400 | tf_op jit(solution)/shard_map/add | solution.py:54
  173.6 10.4 %all-to-all-done.7 = bf16[32,4,2048]{2,1,0:T(4,128)(2,1)S(1)} async-done(((bf16[32,4,2048]{2,1,0:T(4,128)(2,1)}), bf16[32,4,2048]{2,1,0:T(4,128)(2,1)S(1)}, u32[]{:S(2)}, u32[]{:S(2)}) %all-to-all-start.7) | async-done | bytes 524320 | tf_op jit(solution)/shard_map/all_to_all | solution.py:168
  184.4 3.1 %multiply_reduce_fusion = (f32[8]{0:T(128)S(1)}, f32[8,2048]{1,0:T(8,128)S(1)}) fusion(f32[8,2048]{1,0:T(8,128)S(1)} %fusion.11, bf16[512,2048]{1,0:T(8,128)(2,1)} %param.49, bf16[8,2048]{1,0:T(8,128)(2,1)S(1)} %fusion.48, bf16[2048,512]{1,0:T(8,128)(2,1)} %param.48, f32[8,512]{1,0:T(8,128)S(1)} %fusion.76), kind=kOutput, calls=%fused_computation.56 | convolution fusion | flops 33628152 | bytes 4374560 | tf_op jit(solution)/shard_map/dot_general | solution.py:65
  (117 shorter events, 20.6 us)
Async XLA Ops:
  7.2 154.4 %copy-start = (bf16[1,512,2048]{2,1,0:T(8,128)(2,1)S(1)}, bf16[1,512,2048]{2,1,0:T(8,128)(2,1)}, u32[]{:S(2)}) copy-start(bf16[1,512,2048]{2,1,0:T(8,128)(2,1)} %param.46) | copy-start | bytes 6291460
  7.2 22.7 %copy-start.5 = (bf16[64,1024]{1,0:T(8,128)(2,1)S(1)}, bf16[64,1024]{1,0:T(8,128)(2,1)}, u32[]{:S(2)}) copy-start(bf16[64,1024]{1,0:T(8,128)(2,1)} %param.32) | copy-start | bytes 393220
  7.2 23.8 %copy-start.16 = (f32[8,8]{1,0:T(8,128)S(1)}, f32[8,8]{1,0:T(8,128)}, u32[]{:S(2)}) copy-start(f32[8,8]{1,0:T(8,128)} %param.40) | copy-start | bytes 772
  7.2 23.7 %copy-start.18 = (f32[8]{0:T(128)S(1)}, f32[8]{0:T(128)}, u32[]{:S(2)}) copy-start(f32[8]{0:T(128)} %param.37) | copy-start | bytes 100
  7.2 23.7 %copy-start.9 = (bf16[2048,8]{0,1:T(8,128)(2,1)S(1)}, bf16[2048,8]{0,1:T(8,128)(2,1)}, u32[]{:S(2)}) copy-start(bf16[2048,8]{0,1:T(8,128)(2,1)} %param.35) | copy-start | bytes 98308
  7.2 33.5 %copy-start.19 = (f32[8]{0:T(128)S(1)}, f32[8]{0:T(128)}, u32[]{:S(2)}) copy-start(f32[8]{0:T(128)} %param.36) | copy-start | bytes 100
  7.2 33.5 %copy-start.10 = (bf16[2048,8]{0,1:T(8,128)(2,1)S(1)}, bf16[2048,8]{0,1:T(8,128)(2,1)}, u32[]{:S(2)}) copy-start(bf16[2048,8]{0,1:T(8,128)(2,1)} %param.34) | copy-start | bytes 98308
  7.2 33.6 %copy-start.11 = (s32[8,6]{1,0:T(8,128)S(1)}, s32[8,6]{1,0:T(8,128)}, u32[]{:S(2)}) copy-start(s32[8,6]{1,0:T(8,128)} %param.42) | copy-start | bytes 580
  7.3 33.7 %copy-start.6 = (bf16[64,1024]{1,0:T(8,128)(2,1)S(1)}, bf16[64,1024]{1,0:T(8,128)(2,1)}, u32[]{:S(2)}) copy-start(bf16[64,1024]{1,0:T(8,128)(2,1)} %param.33) | copy-start | bytes 393220
  7.3 61.1 %all-gather.2.cloned.1.call-start = ((), (), s32[]{:S(2)}) async-start(), calls=%async_computation.8 | async-start | bytes 1081344 | tf_op jit(solution)/shard_map/all_gather | solution.py:109
  9.8 21.1 %copy-start.2 = (bf16[8,2048]{1,0:T(8,128)(2,1)S(1)}, bf16[8,2048]{1,0:T(8,128)(2,1)}, u32[]{:S(2)}) copy-start(bf16[8,2048]{1,0:T(8,128)(2,1)} %fusion.44) | copy-start | bytes 98308
  11.8 15.5 %all-to-all-start = ((bf16[32,2,1024]{2,1,0:T(2,128)(2,1)}), bf16[32,2,1024]{2,1,0:T(2,128)(2,1)S(1)}, u32[]{:S(2)}, u32[]{:S(2)}) async-start(bf16[32,2,1024]{2,1,0:T(2,128)(2,1)} %reshape.205), calls=%async_computation | async-start | bytes 262144 | tf_op jit(solution)/shard_map/all_to_all | solution.py:102
  27.3 10.8 %all-to-all-start.1 = ((bf16[32,2,1024]{2,1,0:T(2,128)(2,1)}), bf16[32,2,1024]{2,1,0:T(2,128)(2,1)S(1)}, u32[]{:S(2)}, u32[]{:S(2)}) async-start(bf16[32,2,1024]{2,1,0:T(2,128)(2,1)} %reshape.203), calls=%async_computation.1 | async-start | bytes 262144 | tf_op jit(solution)/shard_map/all_to_all | solution.py:103
  38.1 11.1 %all-to-all-start.2 = ((bf16[32,2,1024]{2,1,0:T(2,128)(2,1)}), bf16[32,2,1024]{2,1,0:T(2,128)(2,1)S(1)}, u32[]{:S(2)}, u32[]{:S(2)}) async-start(bf16[32,2,1024]{2,1,0:T(2,128)(2,1)} %reshape.201), calls=%async_computation.2 | async-start | bytes 262144 | tf_op jit(solution)/shard_map/all_to_all | solution.py:104
  40.9 47.5 %copy-start.12 = (f32[8,8]{1,0:T(8,128)}, f32[8,8]{1,0:T(8,128)S(1)}, u32[]{:S(2)}) copy-start(f32[8,8]{1,0:T(8,128)S(1)} %get-tuple-element.8) | copy-start | bytes 772
  49.2 10.8 %all-to-all-start.3 = ((bf16[32,2,1024]{2,1,0:T(2,128)(2,1)}), bf16[32,2,1024]{2,1,0:T(2,128)(2,1)S(1)}, u32[]{:S(2)}, u32[]{:S(2)}) async-start(bf16[32,2,1024]{2,1,0:T(2,128)(2,1)} %reshape.199), calls=%async_computation.3 | async-start | bytes 262144 | tf_op jit(solution)/shard_map/all_to_all | solution.py:105
  71.1 11.0 %all-to-all-start.4 = ((bf16[32,2,512]{2,1,0:T(2,128)(2,1)}), bf16[32,2,512]{2,1,0:T(2,128)(2,1)S(1)}, u32[]{:S(2)}, u32[]{:S(2)}) async-start(bf16[32,2,512]{2,1,0:T(2,128)(2,1)} %reshape.207), calls=%async_computation.4 | async-start | bytes 131072 | tf_op jit(solution)/shard_map/all_to_all | solution.py:112
  82.7 45.2 %copy-start.8 = (bf16[1024,64]{0,1:T(8,128)(2,1)S(1)}, bf16[1024,64]{0,1:T(8,128)(2,1)}, u32[]{:S(2)}) copy-start(bf16[1024,64]{0,1:T(8,128)(2,1)} %param.41) | copy-start | bytes 393220
  88.3 51.0 %copy-start.3 = (bf16[8,2048]{1,0:T(8,128)(2,1)S(1)}, bf16[8,2048]{1,0:T(8,128)(2,1)}, u32[]{:S(2)}) copy-start(bf16[8,2048]{1,0:T(8,128)(2,1)} %param.25) | copy-start | bytes 98308
  88.3 51.0 %copy-start.13 = (f32[2048]{0:T(1024)S(1)}, f32[2048]{0:T(1024)}, u32[]{:S(2)}) copy-start(f32[2048]{0:T(1024)} %param.27) | copy-start | bytes 24580
  88.3 51.2 %copy-start.14 = (f32[2048]{0:T(1024)S(1)}, f32[2048]{0:T(1024)}, u32[]{:S(2)}) copy-start(f32[2048]{0:T(1024)} %param.28) | copy-start | bytes 24580
  129.0 9.8 %all-to-all-start.5 = ((bf16[32,2,256]{2,1,0:T(2,128)(2,1)}), bf16[32,2,256]{2,1,0:T(2,128)(2,1)S(1)}, u32[]{:S(2)}, u32[]{:S(2)}) async-start(bf16[32,2,256]{2,1,0:T(2,128)(2,1)} %reshape.209), calls=%async_computation.5 | async-start | bytes 65536 | tf_op jit(solution)/shard_map/all_to_all | solution.py:131
  141.1 18.2 %all-to-all-start.6 = ((bf16[32,4,2048]{2,1,0:T(4,128)(2,1)}), bf16[32,4,2048]{2,1,0:T(4,128)(2,1)S(1)}, u32[]{:S(2)}, u32[]{:S(2)}) async-start(bf16[32,4,2048]{2,1,0:T(4,128)(2,1)} %reshape.181), calls=%async_computation.6 | async-start | bytes 1048576 | tf_op jit(solution)/shard_map/all_to_all | solution.py:156
  165.5 18.5 %all-to-all-start.7 = ((bf16[32,4,2048]{2,1,0:T(4,128)(2,1)}), bf16[32,4,2048]{2,1,0:T(4,128)(2,1)S(1)}, u32[]{:S(2)}, u32[]{:S(2)}) async-start(bf16[32,4,2048]{2,1,0:T(4,128)(2,1)} %copy.90), calls=%async_computation.7 | async-start | bytes 1048576 | tf_op jit(solution)/shard_map/all_to_all | solution.py:168
  (5 other events, 21.9 us)
Sparse Core Ops, SparseCore 0:
  11.5 56.8 all-gather.1
where the time goes:
time: 196 us; the launch traced here: 195 us
  waiting for transfers between devices  74.7 us (38%)
  blocking collectives  38.7 us (20%)
  starting transfers between devices  26.9 us (14%)
  matrix products  16.8 us (9%)
  between operations  14.6 us (7%)
  local copies, waits for them, and re-layouts  14 us (7%)
  other arithmetic  9.39 us (5%)
    all_gather x1, blocking collectives, on_device(): lax.all_gather(gated_out, 'ep', axis=0, tiled=True)  38.7 us
    all_to_all x1, waiting for transfers between devices, on_device(): lax.all_to_all(outgoing, 'ep', split_axis=0, concat_axis=0, tiled=True)  15.4 us
    all_to_all x1, waiting for transfers between devices, on_device(): lax.all_to_all(answered, 'ep', split_axis=0, concat_axis=0, tiled=True)  10.4 us
    unnamed x57, local copies, waits for them, and re-layouts  8.88 us
    all_gather x1, waiting for transfers between devices, on_device(): piece_rows = lax.all_gather(normed, 'ep', axis=0, tiled=True)  7.7 us
    all_to_all x1, starting transfers between devices, on_device(): lax.all_to_all(query_weight, 'ep', split_axis=1, concat_axis=0, tiled=True)  7.33 us
    all_to_all x1, waiting for transfers between devices, on_device(): lax.all_to_all(mixed_cols, 'ep', split_axis=0, concat_axis=1, tiled=True)  7.24 us
    all_to_all x1, waiting for transfers between devices, on_device(): lax.all_to_all(gathered, 'ep', split_axis=0, concat_axis=2, tiled=True)  7.08 us
  transfers between devices with their start and end apart: 9, of which 9 were waited for; matrix products, arithmetic and copies ran while one was open for 7% of the time, Pallas kernels for 0%

commit v1 on v0

--- a/solution.py
+++ b/solution.py
@@ -63,6 +63,64 @@
     up_values = jnp.dot(row_block, up_weight, preferred_element_type=jnp.float32)
     inner_rows = (jax.nn.silu(gate_values) * up_values).astype(jnp.bfloat16)
     return jnp.dot(inner_rows, down_weight, preferred_element_type=jnp.float32)
+
+
+def swap(values, bit):
+    devices = lax.axis_size("ep")
+    return lax.ppermute(values, "ep", [(i, i ^ bit) for i in range(devices)])
+
+
+def deal_heads(weights, head_count, place):
+    rows, width = weights[0].shape
+    head_width = width // head_count
+    held = jnp.stack([w.reshape(rows, head_count, head_width) for w in weights], axis=2)
+    held = held.reshape(rows, head_count, len(weights) * head_width).swapaxes(0, 1)
+    bit = 1
+    while bit < head_count:
+        side = (place // bit) % 2
+        halves = held.reshape(held.shape[0] // 2, 2, *held.shape[1:])
+        kept = jnp.where(side == 0, halves[:, 0], halves[:, 1])
+        sent = jnp.where(side == 0, halves[:, 1], halves[:, 0])
+        came = swap(sent, bit)
+        first = jnp.where(side == 0, kept, came)
+        second = jnp.where(side == 0, came, kept)
+        held = jnp.concatenate([first, second], axis=1)
+        bit *= 2
+    return held.reshape(rows * head_count, len(weights) * head_width)
+
+
+def gather_far(weight, place):
+    devices = lax.axis_size("ep")
+    held = weight[None]
+    bit = 4
+    while bit < devices:
+        side = (place // bit) % 2
+        came = swap(held, bit)
+        first = jnp.where(side == 0, held, came)
+        second = jnp.where(side == 0, came, held)
+        held = jnp.concatenate([first, second], axis=0)
+        bit *= 2
+    return held
+
+
+def mix_rows(gated_out, far_weight, place):
+    blocks, depth, width = far_weight.shape
+    sequences = gated_out.shape[0]
+    near = swap(gated_out, 1)
+    both = jnp.concatenate([gated_out, near], axis=0)
+    rows = jnp.concatenate([both, swap(both, 2)], axis=0)
+    flat = far_weight.swapaxes(0, 1).reshape(depth, blocks * width)
+    out = jnp.dot(rows, flat, preferred_element_type=jnp.float32).astype(jnp.bfloat16)
+    out = out.reshape(4, sequences, blocks * width)
+    far = swap(out[2:], 2)
+    close = swap(jnp.stack([out[1], far[1]]), 1)
+    found = (out[0], close[0], far[0], close[1])
+    odd = place % 2
+    high = (place // 2) % 2
+    pick = [jnp.where(odd == 0, found[k], found[k ^ 1]) for k in range(4)]
+    pick = [jnp.where(high == 0, pick[k], pick[k ^ 2]) for k in range(4)]
+    stacked = jnp.stack([p.reshape(sequences, blocks, width) for p in pick], axis=2)
+    return stacked.reshape(sequences, blocks * 4 * width).astype(jnp.float32)
 
 
 def on_device(
@@ -94,42 +152,47 @@
 ):
     sequences = tokens.shape[0]
     model_width = tokens.shape[1]
-    memory_width = query_weight.shape[1]
     devices = lax.axis_size("ep")
+    head_count = memory_state.shape[1]
+    head_width = memory_state.shape[2]
+    place = lax.axis_index("ep")
     residual = tokens.astype(jnp.float32)
     normed = rms_scale(residual, premix_gain).astype(jnp.bfloat16)
-    columns = (
-        lax.all_to_all(query_weight, "ep", split_axis=1, concat_axis=0, tiled=True),
-        lax.all_to_all(key_weight, "ep", split_axis=1, concat_axis=0, tiled=True),
-        lax.all_to_all(value_weight, "ep", split_axis=1, concat_axis=0, tiled=True),
-        lax.all_to_all(outgate_weight, "ep", split_axis=1, concat_axis=0, tiled=True),
-    )
-    stacked = jnp.concatenate(columns, axis=1)
-    column_width = memory_width // devices
-    piece_rows = lax.all_gather(normed, "ep", axis=0, tiled=True)
-    product = jnp.dot(piece_rows, stacked, preferred_element_type=jnp.float32).astype(jnp.bfloat16)
-    gathered = product.reshape(piece_rows.shape[0], 4, column_width)
-    projected = lax.all_to_all(gathered, "ep", split_axis=0, concat_axis=2, tiled=True)
+    planes = devices // head_count
+    pieces = normed.reshape(sequences, planes, model_width // planes).swapaxes(0, 1)
+    pieces = jnp.broadcast_to(
+        pieces[:, None], (planes, head_count, sequences, model_width // planes)
+    ).reshape(devices, sequences, model_width // planes)
+    rows_in = lax.all_to_all(pieces, "ep", split_axis=0, concat_axis=0, tiled=True)
+    stacked = deal_heads(
+        (query_weight, key_weight, value_weight, outgate_weight), head_count, place
+    )
+    partial = jnp.dot(
+        rows_in.reshape(devices * sequences, model_width // planes),
+        stacked,
+        preferred_element_type=jnp.float32,
+    ).astype(jnp.bfloat16)
+    partial = partial.reshape(devices, sequences, 4 * head_width)
+    parts = lax.all_to_all(partial, "ep", split_axis=0, concat_axis=0, tiled=True)
+    summed = jnp.sum(
+        parts.reshape(planes, head_count, sequences, 4, head_width).astype(jnp.float32), axis=0
+    )
+    projected = summed.transpose(2, 1, 0, 3).reshape(4, sequences, head_count * head_width)
     input_pre = jnp.dot(normed, ingate_weight, preferred_element_type=jnp.float32) + ingate_bias
     forget_pre = jnp.dot(normed, forget_weight, preferred_element_type=jnp.float32) + forget_bias
     gated_out, next_memory, next_normalizer, next_stabilizer = memory_step(
-        projected[:, 0],
-        projected[:, 1],
-        projected[:, 2],
-        projected[:, 3],
+        projected[0],
+        projected[1],
+        projected[2],
+        projected[3],
         input_pre,
         forget_pre,
         memory_state,
         normalizer,
         stabilizer,
     )
-    mixed_cols = jnp.dot(
-        lax.all_gather(gated_out, "ep", axis=0, tiled=True),
-        output_weight,
-        preferred_element_type=jnp.float32,
-    ).astype(jnp.bfloat16)
-    mixed = lax.all_to_all(mixed_cols, "ep", split_axis=0, concat_axis=1, tiled=True)
-    after_mix = rounded(residual + rms_scale(mixed.astype(jnp.float32), postmix_gain))
+    mixed = mix_rows(gated_out, gather_far(output_weight, place), place)
+    after_mix = rounded(residual + rms_scale(mixed, postmix_gain))
     after_float = after_mix.astype(jnp.float32)
     expert_input = rms_scale(after_float, prefeed_gain).astype(jnp.bfloat16)
     local_count = expert_gate.shape[0]

time: 196 us -> 137 us (0.70)
  blocking collectives: 38.7 us -> 0 us
  between operations: 14.6 us -> 1.15 us
  waiting for transfers between devices: 74.7 us -> 62.6 us
  matrix products: 16.8 us -> 20.8 us
  local copies, waits for them, and re-layouts: 14 us -> 10.2 us
  other arithmetic: 9.39 us -> 12.3 us
  starting transfers between devices: 26.9 us -> 29.7 us
    all_gather x1 -> x0, blocking collectives: 38.7 us -> none  [on_device(): lax.all_gather(gated_out, 'ep', axis=0, tiled=True)]
    all_to_all x6 -> x2, waiting for transfers between devices: 41.2 us -> 18.2 us  [the longest x1 18.2 us: on_device(): lax.all_to_all(partial, 'ep', split_axis=0, concat_axis=0, tiled=True)]
    ppermute x0 -> x10, waiting for transfers between devices: none -> 19.2 us  [swap(): return lax.ppermute(values, 'ep', [(i, i ^ bit) for i in range(devices)])]
    ppermute x0 -> x10, starting transfers between devices: none -> 13.6 us  [swap(): return lax.ppermute(values, 'ep', [(i, i ^ bit) for i in range(devices)])]
    all_to_all x6 -> x2, starting transfers between devices: 21.2 us -> 9.44 us  [the longest x1 5 us: on_device(): lax.all_to_all(pieces, 'ep', split_axis=0, concat_axis=0, tiled=True)]
    all_gather x1 -> x0, waiting for transfers between devices: 7.7 us -> none  [on_device(): piece_rows = lax.all_gather(normed, 'ep', axis=0, tiled=True)]
    select_n x0 -> x10, other arithmetic: none -> 4.57 us  [the longest x3 2.14 us: gather_far(): first = jnp.where(side == 0, held, came)]
    unnamed x57 -> x38, local copies, waits for them, and re-layouts: 8.88 us -> 4.49 us
  transfers between devices with their start and end apart: 9 -> 14, of which waited for: 9 -> 9; matrix products, arithmetic and copies ran while one was open for 7% -> 21% of each run, Pallas kernels for 0% -> 0%
where the time goes in v1:
time: 137 us
  waiting for transfers between devices  62.6 us (46%)
  starting transfers between devices  29.7 us (22%)
  matrix products  20.8 us (15%)
  other arithmetic  12.3 us (9%)
  local copies, waits for them, and re-layouts  10.2 us (7%)
    ppermute x10, waiting for transfers between devices, swap(): return lax.ppermute(values, 'ep', [(i, i ^ bit) for i in range(devices)])  19.2 us
    all_to_all x1, waiting for transfers between devices, on_device(): lax.all_to_all(partial, 'ep', split_axis=0, concat_axis=0, tiled=True)  18.2 us
    all_to_all x1, waiting for transfers between devices, on_device(): lax.all_to_all(outgoing, 'ep', split_axis=0, concat_axis=0, tiled=True)  15.5 us
    ppermute x10, starting transfers between devices, swap(): return lax.ppermute(values, 'ep', [(i, i ^ bit) for i in range(devices)])  13.6 us
    all_to_all x1, waiting for transfers between devices, on_device(): lax.all_to_all(answered, 'ep', split_axis=0, concat_axis=0, tiled=True)  9.71 us
    dot_general x1, matrix products, memory_step(): jnp.einsum('shvk,shk->shv', memory_state, query_heads, precision=lax.Prec...  8.31 us
    all_to_all x1, starting transfers between devices, on_device(): lax.all_to_all(pieces, 'ep', split_axis=0, concat_axis=0, tiled=True)  5 us
    unnamed x38, local copies, waits for them, and re-layouts  4.49 us
  transfers between devices with their start and end apart: 14, of which 9 were waited for; matrix products, arithmetic and copies ran while one was open for 21% of the time, Pallas kernels for 0%

profile of v1, /device:TPU:0, one launch (start us, length us, event | category | flops | bytes accessed | tf_op | source)
XLA Modules:
  0.0 136.7 jit_solution(5634202895870882945)
XLA Ops:
  0.7 3.1 %collective-permute-start.5 = (bf16[1,1024,64]{1,2,0:T(8,128)(2,1)}, bf16[1,1024,64]{1,2,0:T(8,128)(2,1)}, u32[]{:S(2)}, u32[]{:S(2)}) collective-permute-start(bf16[1,1024,64]{1,2,0:T(8,128)(2,1)} %bitcast.257), channel_id=1, source_target_pairs={{0,4},{1,5},{2,6},{3,7},{4,0},{5,1},{6,2},{7,3},{8,12},{9,13},{10,... | collective-permute-start | bytes 393224 | tf_op jit(solution)/shard_map/ppermute | solution.py:70
  9.5 5.0 %all-to-all-start = ((bf16[32,8,512]{2,1,0:T(8,128)(2,1)}), bf16[32,8,512]{2,1,0:T(8,128)(2,1)S(1)}, u32[]{:S(2)}, u32[]{:S(2)}) async-start(bf16[32,8,512]{2,1,0:T(8,128)(2,1)} %bitcast.2), calls=%async_computation | async-start | bytes 524288 | tf_op jit(solution)/shard_map/all_to_all | solution.py:166
  15.3 1.8 %collective-permute-start.1 = (bf16[2,128,512]{2,1,0:T(8,128)(2,1)}, bf16[2,128,512]{2,1,0:T(8,128)(2,1)S(1)}, u32[]{:S(2)}, u32[]{:S(2)}) collective-permute-start(bf16[2,128,512]{2,1,0:T(8,128)(2,1)} %fusion.32), channel_id=1, source_target_pairs={{0,2},{1,3},{2,0},{3,1},{4,6},{5,7},{6,4},{7,5},{8,10},{9,11},{10,... | collective-permute-start | bytes 786440 | tf_op jit(solution)/shard_map/ppermute | solution.py:70
  17.5 8.6 %collective-permute-done.1 = bf16[2,128,512]{2,1,0:T(8,128)(2,1)S(1)} collective-permute-done((bf16[2,128,512]{2,1,0:T(8,128)(2,1)}, bf16[2,128,512]{2,1,0:T(8,128)(2,1)S(1)}, u32[]{:S(2)}, u32[]{:S(2)}) %collective-permute-start.1) | collective-permute-done | bytes 262176 | tf_op jit(solution)/shard_map/ppermute | solution.py:70
  26.2 1.5 %collective-permute-start.2 = (bf16[1,256,512]{2,1,0:T(8,128)(2,1)S(1)}, bf16[1,256,512]{2,1,0:T(8,128)(2,1)S(1)}, u32[]{:S(2)}, u32[]{:S(2)}) collective-permute-start(bf16[1,256,512]{2,1,0:T(8,128)(2,1)S(1)} %select_bitcast_fusion), channel_id=1, source_target_pairs={{0,4},{1,5},{2,6},{3,7},{4,0},{5,1},{6,2},{7,3},{8,12},{9,13},{10,... | collective-permute-start | bytes 786440 | tf_op jit(solution)/shard_map/ppermute | solution.py:70
  30.3 4.0 %collective-permute-done.2 = bf16[1,256,512]{2,1,0:T(8,128)(2,1)S(1)} collective-permute-done((bf16[1,256,512]{2,1,0:T(8,128)(2,1)S(1)}, bf16[1,256,512]{2,1,0:T(8,128)(2,1)S(1)}, u32[]{:S(2)}, u32[]{:S(2)}) %collective-permute-start.2) | collective-permute-done | bytes 262176 | tf_op jit(solution)/shard_map/ppermute | solution.py:70
  35.1 2.0 %fusion.5 = bf16[32,8,512]{2,1,0:T(8,128)(2,1)} fusion(bf16[1,256,512]{2,1,0:T(8,128)(2,1)} %get-tuple-element.23, bf16[1,256,512]{2,1,0:T(8,128)(2,1)} %get-tuple-element.22, bf16[32,8,512]{2,1,0:T(8,128)(2,1)S(1)} %all-to-all-done), kind=kOutput, calls=%fused_computation.11 | convolution fusion | flops 135397376 | bytes 1048576 | tf_op jit(solution)/shard_map/dot_general | solution.py:170
  37.2 4.4 %all-to-all-start.1 = ((bf16[32,8,512]{2,1,0:T(8,128)(2,1)}), bf16[32,8,512]{2,1,0:T(8,128)(2,1)S(1)}, u32[]{:S(2)}, u32[]{:S(2)}) async-start(bf16[32,8,512]{2,1,0:T(8,128)(2,1)} %fusion.5), calls=%async_computation.1 | async-start | bytes 524288 | tf_op jit(solution)/shard_map/all_to_all | solution.py:176
  42.8 2.7 %collective-permute-start.7 = (bf16[4,1024,64]{1,2,0:T(8,128)(2,1)}, bf16[4,1024,64]{1,2,0:T(8,128)(2,1)}, u32[]{:S(2)}, u32[]{:S(2)}) collective-permute-start(bf16[4,1024,64]{1,2,0:T(8,128)(2,1)} %pad_maximum_fusion.2), channel_id=1, source_target_pairs={{0,16},{1,17},{2,18},{3,19},{4,20},{5,21},{6,22},{7,23},{8,24},{9,... | collective-permute-start | bytes 1572872 | tf_op jit(solution)/shard_map/ppermute | solution.py:70
  45.5 18.2 %all-to-all-done.1 = bf16[32,8,512]{2,1,0:T(8,128)(2,1)S(1)} async-done(((bf16[32,8,512]{2,1,0:T(8,128)(2,1)}), bf16[32,8,512]{2,1,0:T(8,128)(2,1)S(1)}, u32[]{:S(2)}, u32[]{:S(2)}) %all-to-all-start.1) | async-done | bytes 262176 | tf_op jit(solution)/shard_map/all_to_all | solution.py:176
  64.2 8.3 %fusion.64 = f32[8,8,1,128]{3,2,1,0:T(1,128)S(1)} fusion(f32[8,8,128,128]{3,2,1,0:T(8,128)} %param.38, f32[8,8,128,1]{2,0,1,3:T(8,128)S(1)} %slice_bitcast_fusion.2), kind=kOutput, calls=%fused_computation.103 | convolution fusion | flops 12582912 | bytes 4259840 | tf_op jit(solution)/shard_map/shvk,shk->shv/dot_general | solution.py:43
  74.7 1.5 %collective-permute-start.4 = (bf16[16,1024]{1,0:T(8,128)(2,1)S(1)}, bf16[16,1024]{1,0:T(8,128)(2,1)S(1)}, u32[]{:S(2)}, u32[]{:S(2)}) collective-permute-start(bf16[16,1024]{1,0:T(8,128)(2,1)S(1)} %pad_maximum_fusion.4), channel_id=1, source_target_pairs={{0,2},{1,3},{2,0},{3,1},{4,6},{5,7},{6,4},{7,5},{8,10},{9,11},{10,... | collective-permute-start | bytes 98312 | tf_op jit(solution)/shard_map/ppermute | solution.py:70
  76.3 2.3 %collective-permute-done.4 = bf16[16,1024]{1,0:T(8,128)(2,1)S(1)} collective-permute-done((bf16[16,1024]{1,0:T(8,128)(2,1)S(1)}, bf16[16,1024]{1,0:T(8,128)(2,1)S(1)}, u32[]{:S(2)}, u32[]{:S(2)}) %collective-permute-start.4) | collective-permute-done | bytes 32800 | tf_op jit(solution)/shard_map/ppermute | solution.py:70
  79.1 1.5 %collective-permute-start.8 = (bf16[2,8,512]{2,1,0:T(8,128)(2,1)S(1)}, bf16[2,8,512]{2,1,0:T(8,128)(2,1)S(1)}, u32[]{:S(2)}, u32[]{:S(2)}) collective-permute-start(bf16[2,8,512]{2,1,0:T(8,128)(2,1)S(1)} %slice_bitcast_fusion.3), channel_id=1, source_target_pairs={{0,2},{1,3},{2,0},{3,1},{4,6},{5,7},{6,4},{7,5},{8,10},{9,11},{10,... | collective-permute-start | bytes 49160 | tf_op jit(solution)/shard_map/ppermute | solution.py:70
  80.6 2.3 %collective-permute-done.8 = bf16[2,8,512]{2,1,0:T(8,128)(2,1)S(1)} collective-permute-done((bf16[2,8,512]{2,1,0:T(8,128)(2,1)S(1)}, bf16[2,8,512]{2,1,0:T(8,128)(2,1)S(1)}, u32[]{:S(2)}, u32[]{:S(2)}) %collective-permute-start.8) | collective-permute-done | bytes 16416 | tf_op jit(solution)/shard_map/ppermute | solution.py:70
  86.7 3.6 %all-to-all-start.2 = ((bf16[32,4,2048]{2,1,0:T(4,128)(2,1)}), bf16[32,4,2048]{2,1,0:T(4,128)(2,1)S(1)}, u32[]{:S(2)}, u32[]{:S(2)}) async-start(bf16[32,4,2048]{2,1,0:T(4,128)(2,1)} %reshape.262), calls=%async_computation.2 | async-start | bytes 1048576 | tf_op jit(solution)/shard_map/all_to_all | solution.py:219
  90.4 15.5 %all-to-all-done.2 = bf16[32,4,2048]{2,1,0:T(4,128)(2,1)S(1)} async-done(((bf16[32,4,2048]{2,1,0:T(4,128)(2,1)}), bf16[32,4,2048]{2,1,0:T(4,128)(2,1)S(1)}, u32[]{:S(2)}, u32[]{:S(2)}) %all-to-all-start.2) | async-done | bytes 524320 | tf_op jit(solution)/shard_map/all_to_all | solution.py:219
  106.0 2.2 %fusion.6 = f32[32,1,4,512]{3,0,2,1:T(8,128)S(1)} fusion(bf16[1,2048,512]{2,1,0:T(8,128)(2,1)} %param.44, bf16[32,4,2048]{2,1,0:T(4,128)(2,1)S(1)} %all-to-all-done.2), kind=kOutput, calls=%fused_computation.12 | convolution fusion | flops 268435456 | bytes 2883584 | tf_op jit(solution)/shard_map/nlid,ldf->nlif/dot_general | solution.py:222
  108.2 3.4 %convolution_convert_fusion = bf16[32,4,2048]{2,0,1:T(8,128)(2,1)} fusion(bf16[1,512,2048]{2,1,0:T(8,128)(2,1)S(1)} %copy-done, bf16[1,2048,512]{2,1,0:T(8,128)(2,1)} %param.45, bf16[32,4,2048]{2,1,0:T(4,128)(2,1)S(1)} %all-to-all-done.2, f32[32,1,4,512]{3,0,2,1:T(8,128)S(1)} %fusion.6), kind=kOutput, calls=%fused_computation.1 | convolution fusion | flops 537526272 | bytes 5505024 | tf_op jit(solution)/shard_map/nlif,lfd->nlid/dot_general | solution.py:227
  111.7 2.3 %copy.95 = bf16[32,4,2048]{2,1,0:T(4,128)(2,1)} copy(bf16[32,4,2048]{2,0,1:T(8,128)(2,1)} %convolution_convert_fusion) | data formatting | bytes 1048576 | tf_op jit(solution)/shard_map/convert_element_type | solution.py:229
  113.9 3.0 %all-to-all-start.3 = ((bf16[32,4,2048]{2,1,0:T(4,128)(2,1)}), bf16[32,4,2048]{2,1,0:T(4,128)(2,1)S(1)}, u32[]{:S(2)}, u32[]{:S(2)}) async-start(bf16[32,4,2048]{2,1,0:T(4,128)(2,1)} %copy.95), calls=%async_computation.3 | async-start | bytes 1048576 | tf_op jit(solution)/shard_map/all_to_all | solution.py:231
  118.0 4.5 %multiply_add_fusion = f32[8,8,128,128]{3,2,1,0:T(8,128)} fusion(f32[8,8,128,128]{3,2,1,0:T(8,128)} %param.38, f32[8,8,128]{2,1,0:T(8,128)S(1)} %copy.99, f32[8,8,128]{2,1,0:T(8,128)S(1)} %copy.98, f32[8,8]{1,0:T(8,128)S(1)} %get-tuple-element.18), kind=kLoop, calls=%fused_computation | loop fusion | flops 3145728 | bytes 8454400 | tf_op jit(solution)/shard_map/add | solution.py:54
  122.8 9.7 %all-to-all-done.3 = bf16[32,4,2048]{2,1,0:T(4,128)(2,1)S(1)} async-done(((bf16[32,4,2048]{2,1,0:T(4,128)(2,1)}), bf16[32,4,2048]{2,1,0:T(4,128)(2,1)S(1)}, u32[]{:S(2)}, u32[]{:S(2)}) %all-to-all-start.3) | async-done | bytes 524320 | tf_op jit(solution)/shard_map/all_to_all | solution.py:231
  132.9 3.1 %multiply_reduce_fusion.1 = (f32[8]{0:T(128)S(1)}, f32[8,2048]{1,0:T(8,128)S(1)}) fusion(f32[8,2048]{1,0:T(8,128)S(1)} %fusion.12, bf16[512,2048]{1,0:T(8,128)(2,1)} %param.49, bf16[8,2048]{1,0:T(8,128)(2,1)S(1)} %fusion.48, bf16[2048,512]{1,0:T(8,128)(2,1)} %param.48, f32[8,512]{1,0:T(8,128)S(1)} %fusion.86), kind=kOutput, calls=%fused_computation.86 | convolution fusion | flops 33628152 | bytes 4374560 | tf_op jit(solution)/shard_map/dot_general | solution.py:65
  (123 shorter events, 21.0 us)
Async XLA Ops:
  0.6 107.6 %copy-start = (bf16[1,512,2048]{2,1,0:T(8,128)(2,1)S(1)}, bf16[1,512,2048]{2,1,0:T(8,128)(2,1)}, u32[]{:S(2)}) copy-start(bf16[1,512,2048]{2,1,0:T(8,128)(2,1)} %param.46) | copy-start | bytes 6291460
  0.7 27.1 %collective-permute-start.5 = (bf16[1,1024,64]{1,2,0:T(8,128)(2,1)}, bf16[1,1024,64]{1,2,0:T(8,128)(2,1)}, u32[]{:S(2)}, u32[]{:S(2)}) collective-permute-start(bf16[1,1024,64]{1,2,0:T(8,128)(2,1)} %bitcast.257), channel_id=1, source_target_pairs={{0,4},{1,5},{2,6},{3,7},{4,0},{5,1},{6,2},{7,3},{8,12},{9,13},{10,... | collective-permute-start | bytes 393224 | tf_op jit(solution)/shard_map/ppermute | solution.py:70
  8.5 8.7 %copy-start.12 = (f32[8,8]{1,0:T(8,128)S(1)}, f32[8,8]{1,0:T(8,128)}, u32[]{:S(2)}) copy-start(f32[8,8]{1,0:T(8,128)} %param.40) | copy-start | bytes 772
  8.5 8.7 %copy-start.14 = (f32[8]{0:T(128)S(1)}, f32[8]{0:T(128)}, u32[]{:S(2)}) copy-start(f32[8]{0:T(128)} %param.37) | copy-start | bytes 100
  8.5 6.0 %collective-permute-start = (bf16[4,64,512]{2,1,0:T(8,128)(2,1)}, bf16[4,64,512]{2,1,0:T(8,128)(2,1)S(1)}, u32[]{:S(2)}, u32[]{:S(2)}) collective-permute-start(bf16[4,64,512]{2,1,0:T(8,128)(2,1)} %fusion.31), channel_id=1, source_target_pairs={{0,1},{1,0},{2,3},{3,2},{4,5},{5,4},{6,7},{7,6},{8,9},{9,8},{10,11... | collective-permute-start | bytes 786440 | tf_op jit(solution)/shard_map/ppermute | solution.py:70
  8.6 8.7 %copy-start.6 = (s32[8,6]{1,0:T(8,128)S(1)}, s32[8,6]{1,0:T(8,128)}, u32[]{:S(2)}) copy-start(s32[8,6]{1,0:T(8,128)} %param.42) | copy-start | bytes 580
  8.6 8.7 %copy-start.5 = (bf16[2048,8]{0,1:T(8,128)(2,1)S(1)}, bf16[2048,8]{0,1:T(8,128)(2,1)}, u32[]{:S(2)}) copy-start(bf16[2048,8]{0,1:T(8,128)(2,1)} %param.34) | copy-start | bytes 98308
  8.7 8.7 %copy-start.15 = (f32[8]{0:T(128)S(1)}, f32[8]{0:T(128)}, u32[]{:S(2)}) copy-start(f32[8]{0:T(128)} %param.36) | copy-start | bytes 100
  9.5 25.6 %all-to-all-start = ((bf16[32,8,512]{2,1,0:T(8,128)(2,1)}), bf16[32,8,512]{2,1,0:T(8,128)(2,1)S(1)}, u32[]{:S(2)}, u32[]{:S(2)}) async-start(bf16[32,8,512]{2,1,0:T(8,128)(2,1)} %bitcast.2), calls=%async_computation | async-start | bytes 524288 | tf_op jit(solution)/shard_map/all_to_all | solution.py:166
  15.3 10.8 %collective-permute-start.1 = (bf16[2,128,512]{2,1,0:T(8,128)(2,1)}, bf16[2,128,512]{2,1,0:T(8,128)(2,1)S(1)}, u32[]{:S(2)}, u32[]{:S(2)}) collective-permute-start(bf16[2,128,512]{2,1,0:T(8,128)(2,1)} %fusion.32), channel_id=1, source_target_pairs={{0,2},{1,3},{2,0},{3,1},{4,6},{5,7},{6,4},{7,5},{8,10},{9,11},{10,... | collective-permute-start | bytes 786440 | tf_op jit(solution)/shard_map/ppermute | solution.py:70
  17.5 46.5 %copy-start.7 = (f32[8,8]{1,0:T(8,128)}, f32[8,8]{1,0:T(8,128)S(1)}, u32[]{:S(2)}) copy-start(f32[8,8]{1,0:T(8,128)S(1)} %get-tuple-element.16) | copy-start | bytes 772
  26.2 8.0 %collective-permute-start.2 = (bf16[1,256,512]{2,1,0:T(8,128)(2,1)S(1)}, bf16[1,256,512]{2,1,0:T(8,128)(2,1)S(1)}, u32[]{:S(2)}, u32[]{:S(2)}) collective-permute-start(bf16[1,256,512]{2,1,0:T(8,128)(2,1)S(1)} %select_bitcast_fusion), channel_id=1, source_target_pairs={{0,4},{1,5},{2,6},{3,7},{4,0},{5,1},{6,2},{7,3},{8,12},{9,13},{10,... | collective-permute-start | bytes 786440 | tf_op jit(solution)/shard_map/ppermute | solution.py:70
  28.8 13.1 %collective-permute-start.6 = (bf16[2,1024,64]{1,2,0:T(8,128)(2,1)S(1)}, bf16[2,1024,64]{1,2,0:T(8,128)(2,1)S(1)}, u32[]{:S(2)}, u32[]{:S(2)}) collective-permute-start(bf16[2,1024,64]{1,2,0:T(8,128)(2,1)S(1)} %pad_maximum_fusion.3), channel_id=1, source_target_pairs={{0,8},{1,9},{2,10},{3,11},{4,12},{5,13},{6,14},{7,15},{8,0},{9,1},... | collective-permute-start | bytes 786440 | tf_op jit(solution)/shard_map/ppermute | solution.py:70
  35.1 28.7 %copy-start.3 = (f32[8,8,128]{2,1,0:T(8,128)S(1)}, f32[8,8,128]{2,1,0:T(8,128)}, u32[]{:S(2)}) copy-start(f32[8,8,128]{2,1,0:T(8,128)} %param.39) | copy-start | bytes 98308
  37.2 26.6 %all-to-all-start.1 = ((bf16[32,8,512]{2,1,0:T(8,128)(2,1)}), bf16[32,8,512]{2,1,0:T(8,128)(2,1)S(1)}, u32[]{:S(2)}, u32[]{:S(2)}) async-start(bf16[32,8,512]{2,1,0:T(8,128)(2,1)} %fusion.5), calls=%async_computation.1 | async-start | bytes 524288 | tf_op jit(solution)/shard_map/all_to_all | solution.py:176
  42.8 30.7 %collective-permute-start.7 = (bf16[4,1024,64]{1,2,0:T(8,128)(2,1)}, bf16[4,1024,64]{1,2,0:T(8,128)(2,1)}, u32[]{:S(2)}, u32[]{:S(2)}) collective-permute-start(bf16[4,1024,64]{1,2,0:T(8,128)(2,1)} %pad_maximum_fusion.2), channel_id=1, source_target_pairs={{0,16},{1,17},{2,18},{3,19},{4,20},{5,21},{6,22},{7,23},{8,24},{9,... | collective-permute-start | bytes 1572872 | tf_op jit(solution)/shard_map/ppermute | solution.py:70
  72.7 2.0 %collective-permute-start.3 = (bf16[8,1024]{1,0:T(8,128)(2,1)S(1)}, bf16[8,1024]{1,0:T(8,128)(2,1)S(1)}, u32[]{:S(2)}, u32[]{:S(2)}) collective-permute-start(bf16[8,1024]{1,0:T(8,128)(2,1)S(1)} %fusion.66), channel_id=1, source_target_pairs={{0,1},{1,0},{2,3},{3,2},{4,5},{5,4},{6,7},{7,6},{8,9},{9,8},{10,11... | collective-permute-start | bytes 49160 | tf_op jit(solution)/shard_map/ppermute | solution.py:70
  74.7 4.0 %collective-permute-start.4 = (bf16[16,1024]{1,0:T(8,128)(2,1)S(1)}, bf16[16,1024]{1,0:T(8,128)(2,1)S(1)}, u32[]{:S(2)}, u32[]{:S(2)}) collective-permute-start(bf16[16,1024]{1,0:T(8,128)(2,1)S(1)} %pad_maximum_fusion.4), channel_id=1, source_target_pairs={{0,2},{1,3},{2,0},{3,1},{4,6},{5,7},{6,4},{7,5},{8,10},{9,11},{10,... | collective-permute-start | bytes 98312 | tf_op jit(solution)/shard_map/ppermute | solution.py:70
  76.2 8.7 %copy-start.9 = (f32[2048]{0:T(1024)S(1)}, f32[2048]{0:T(1024)}, u32[]{:S(2)}) copy-start(f32[2048]{0:T(1024)} %param.27) | copy-start | bytes 24580
  76.2 8.9 %copy-start.10 = (f32[2048]{0:T(1024)S(1)}, f32[2048]{0:T(1024)}, u32[]{:S(2)}) copy-start(f32[2048]{0:T(1024)} %param.28) | copy-start | bytes 24580
  79.1 3.8 %collective-permute-start.8 = (bf16[2,8,512]{2,1,0:T(8,128)(2,1)S(1)}, bf16[2,8,512]{2,1,0:T(8,128)(2,1)S(1)}, u32[]{:S(2)}, u32[]{:S(2)}) collective-permute-start(bf16[2,8,512]{2,1,0:T(8,128)(2,1)S(1)} %slice_bitcast_fusion.3), channel_id=1, source_target_pairs={{0,2},{1,3},{2,0},{3,1},{4,6},{5,7},{6,4},{7,5},{8,10},{9,11},{10,... | collective-permute-start | bytes 49160 | tf_op jit(solution)/shard_map/ppermute | solution.py:70
  82.9 1.2 collective-permute-start.9
  86.7 19.2 %all-to-all-start.2 = ((bf16[32,4,2048]{2,1,0:T(4,128)(2,1)}), bf16[32,4,2048]{2,1,0:T(4,128)(2,1)S(1)}, u32[]{:S(2)}, u32[]{:S(2)}) async-start(bf16[32,4,2048]{2,1,0:T(4,128)(2,1)} %reshape.262), calls=%async_computation.2 | async-start | bytes 1048576 | tf_op jit(solution)/shard_map/all_to_all | solution.py:219
  113.9 18.6 %all-to-all-start.3 = ((bf16[32,4,2048]{2,1,0:T(4,128)(2,1)}), bf16[32,4,2048]{2,1,0:T(4,128)(2,1)S(1)}, u32[]{:S(2)}, u32[]{:S(2)}) async-start(bf16[32,4,2048]{2,1,0:T(4,128)(2,1)} %copy.95), calls=%async_computation.3 | async-start | bytes 1048576 | tf_op jit(solution)/shard_map/all_to_all | solution.py:231
  (6 other events, 37.4 us)

commit v2 on v0

v2 whole, which is shorter than its diff:
```python
import functools
import jax
import jax.numpy as jnp
from jax import lax
from jax.experimental import pallas as pl
from jax.experimental.pallas import tpu as pltpu
from jax.sharding import PartitionSpec as P

epsilon = 1e-06
CORE = 1
WIDE, HALF = jnp.float32, jnp.bfloat16


def rms_scale(values, gain_row):
    return (
        values * lax.rsqrt(jnp.mean(values * values, axis=-1, keepdims=True) + epsilon) * gain_row
    )


def swap(values, bit):
    devices = lax.axis_size("ep")
    return lax.ppermute(values, "ep", [(i, i ^ bit) for i in range(devices)])


def exchange(values, groups=None):
    return lax.all_to_all(
        values, "ep", split_axis=0, concat_axis=0, tiled=True, axis_index_groups=groups
    )


SPACES = {"v": pltpu.VMEM, "h": pltpu.HBM, "s": pltpu.SMEM}


def local_call(body, outs, args, spaces=None, scratch=(), limit=16):
    spaces = spaces or "v" * len(args)
    args = [
        pltpu.with_memory_space_constraint(arg, SPACES[space]) if space != "s" else arg
        for arg, space in zip(args, spaces)
    ]
    return pl.pallas_call(
        body,
        out_shape=[SPACES[space](shape, kind) for shape, kind, space in outs],
        in_specs=[pl.BlockSpec(memory_space=SPACES[space]) for space in spaces],
        out_specs=[pl.BlockSpec(memory_space=pltpu.VMEM)] * len(outs),
        scratch_shapes=list(scratch),
        compiler_params=pltpu.CompilerParams(vmem_limit_bytes=limit * 2**20),
    )(*args)


def fetch(pairs, done):
    copies = [
        pltpu.make_async_copy(source, target, done.at[number])
        for number, (source, target) in enumerate(pairs)
    ]
    for copy in copies:
        copy.start()
    for copy in copies:
        copy.wait()


def start_kernel(at_ref, tokens_ref, gain_ref, *refs, planes):
    weights, outs, (scale_ref, done) = refs[:4], refs[4:-2], refs[-2:]
    kept_ref, sent_ref, held_ref, normed_ref, pieces_ref = outs
    loads = [
        pltpu.make_async_copy(source, target, done.at[number])
        for number, (source, target) in enumerate([(tokens_ref, held_ref), (gain_ref, scale_ref)])
    ]
    for load in loads:
        load.start()

    def place(kept, sent):
        pairs = [(weight, kept_ref.at[number]) for number, weight in enumerate(kept)]
        pairs += [(weight, sent_ref.at[number]) for number, weight in enumerate(sent)]
        for number, (source, target) in enumerate(pairs):
            pltpu.make_async_copy(source, target, done.at[2 + number]).start()

    pl.when(at_ref[0] == 0)(lambda: place(weights[:2], weights[2:]))
    pl.when(at_ref[0] != 0)(lambda: place(weights[2:], weights[:2]))
    for load in loads:
        load.wait()
    normed = rms_scale(held_ref[...].astype(WIDE), scale_ref[...]).astype(HALF)
    normed_ref[...] = normed
    width = normed.shape[1] // planes
    copies = pieces_ref.shape[0] // planes
    for plane in range(planes):
        piece = normed[:, plane * width : (plane + 1) * width]
        for copy in range(copies):
            pieces_ref[plane * copies + copy] = piece
    for number in range(2):
        for side, target in enumerate((kept_ref, sent_ref)):
            source = weights[number]
            pltpu.make_async_copy(source, target.at[number], done.at[2 + 2 * side + number]).wait()


def deal_kernel(at_ref, kept_ref, came_ref, *outs):
    core, chip = at_ref[0], at_ref[1]
    count, rows, _ = kept_ref.shape
    lanes = outs[0].shape[1] // count
    mine = pl.multiple_of(core * rows, rows)
    other = pl.multiple_of((1 - core) * rows, rows)
    for turn, out in enumerate(outs):
        start = pl.multiple_of((chip ^ turn) * lanes, lanes)
        for number in range(count):
            across = slice(number * lanes, (number + 1) * lanes)
            out[pl.ds(mine, rows), across] = kept_ref[number, :, pl.ds(start, lanes)]
            out[pl.ds(other, rows), across] = came_ref[number, :, pl.ds(start, lanes)]


def prepare_kernel(
    normed_ref, *refs, fold, capacity
):
    sources, outs, held, done = refs[:11], refs[11:20], refs[20:-1], refs[-1]
    keep_ref, write_ref, next_ref, hot_ref, pick_ref = outs[:5]
    fetch(list(zip(sources, outs[5:] + held)), done)
    ingate_ref, forget_ref, ingate_bias, forget_bias, stabilizer_ref, ids_ref, route_ref = held
    normed = normed_ref[...]
    dims = (((1,), (1,)), ((), ()))
    input_pre = lax.dot_general(normed, ingate_ref[...], dims, preferred_element_type=WIDE)
    input_pre = input_pre + ingate_bias[...]
    forget_pre = lax.dot_general(normed, forget_ref[...], dims, preferred_element_type=WIDE)
    forget_pre = forget_pre + forget_bias[...]
    carried = jax.nn.log_sigmoid(forget_pre) + stabilizer_ref[...]
    following = jnp.maximum(carried, input_pre)
    next_ref[...] = following
    keep_ref[...] = jnp.exp(carried - following)
    write_ref[...] = jnp.exp(input_pre - following)

    sequences, choose_count = ids_ref.shape
    slots = hot_ref.shape[1]
    slot = lax.broadcasted_iota(jnp.int32, (sequences, slots), 1)
    order = lax.broadcasted_iota(jnp.int32, (sequences, slots), 0)
    expert = slot // (fold * capacity)
    named = jnp.zeros((sequences, slots), WIDE)
    share = jnp.zeros((sequences, slots), WIDE)
    for choice in range(choose_count):
        match = ids_ref[:, choice : choice + 1] == expert
        named = jnp.where(match, 1.0, named)
        share = jnp.where(match, route_ref[:, choice : choice + 1], share)
    rank = jnp.zeros((sequences, slots), WIDE)
    for earlier in range(sequences - 1):
        rank = rank + jnp.where(order > earlier, named[earlier : earlier + 1], 0.0)
    taken = (named > 0.0) & (rank == (slot % capacity).astype(WIDE))
    part_of = (slot // capacity) % fold
    high = share.astype(HALF).astype(WIDE)
    low = share - high
    for part in range(fold):
        here = taken & (part_of == part)
        rows = slice(part * sequences, (part + 1) * sequences)
        hot_ref[rows] = jnp.where(here, 1.0, 0.0).astype(HALF)
        start = 2 * part * sequences
        pick_ref[start : start + sequences] = jnp.where(here, high, 0.0).astype(HALF)
        pick_ref[start + sequences : start + 2 * sequences] = jnp.where(here, low, 0.0).astype(HALF)


def project_kernel(at_ref, rows_ref, *refs):
    blocks, out_ref, held_ref = refs[:-2], refs[-2], refs[-1]
    chip = at_ref[1]
    depth = blocks[0].shape[0]
    for turn, block in enumerate(blocks):
        start = pl.multiple_of((chip ^ turn) * depth, depth)
        held_ref[pl.ds(start, depth), :] = block[...]
    out_ref[...] = jnp.dot(
        rows_ref[...], held_ref[...], preferred_element_type=WIDE
    ).astype(HALF)


def hold_kernel(after_ref, memory_ref, held_ref, done):
    load = pltpu.make_async_copy(memory_ref.at[pl.ds(0, held_ref.shape[0])], held_ref, done)
    load.start()
    load.wait()


def read_kernel(
    parts_ref,
    keep_ref,
    write_ref,
    normalizer_ref,
    early_ref,
    memory_ref,
    gated_ref,
    keys_ref,
    values_ref,
    late_ref,
    done,
):
    early = early_ref.shape[0]
    loads = [
        pltpu.make_async_copy(memory_ref.at[early + at], late_ref.at[at], done.at[at])
        for at in range(late_ref.shape[0])
    ]
    for load in loads:
        load.start()
    copies, sequences, _ = gated_ref.shape
    heads, width = memory_ref.shape[1], memory_ref.shape[3]
    planes = parts_ref.shape[0] // heads
    row = lax.broadcasted_iota(jnp.int32, (sequences, width), 0)
    pieces, asked = [], []
    for head in range(heads):
        first = head % 2 * width
        found = []
        for core in range(2):
            for start in (first, first + 2 * width):
                total = 0.0
                for plane in range(planes):
                    part = parts_ref[plane * heads + head // 2 * 2 + core]
                    total = total + part[:, start : start + width].astype(WIDE)
                found.append(total)
        found[1] = found[1] * width ** (-0.5)
        keys_ref[head] = found[1]
        values_ref[head] = found[2]
        pieces.append(found)
        high = found[0].astype(HALF)
        low = (found[0] - high.astype(WIDE)).astype(HALF)
        both = jnp.concatenate([high, low], axis=0)
        asked.append(jnp.concatenate([both, both], axis=1))
    dims = (((1,), (1,)), ((), ()))
    reads = [jnp.zeros((sequences, width), WIDE)] * heads
    for sequence in range(sequences):
        if sequence >= early:
            loads[sequence - early].wait()
        for first in range(0, heads, 2):
            held = []
            for head in (first, first + 1):
                if sequence < early:
                    memory = early_ref[sequence, head]
                else:
                    memory = late_ref[sequence - early, head]
                upper = memory.astype(HALF)
                lower = (memory - upper.astype(WIDE)).astype(HALF)
                held.append(jnp.concatenate([upper, lower], axis=1))
            answer = lax.dot_general(
                jnp.concatenate([asked[first], asked[first + 1]], axis=0),
                jnp.concatenate(held, axis=0),
                dims,
                preferred_element_type=WIDE,
            )
            for side in range(2):
                start = 2 * side * sequences
                mine = answer[start : start + 2 * sequences, side * width : (side + 1) * width]
                mine = mine[:sequences] + mine[sequences:]
                head = first + side
                reads[head] = jnp.where(row == sequence, mine, reads[head])
    for head in range(heads):
        queries, keys, values, gate = pieces[head]
        keep = keep_ref[:, head : head + 1]
        score = write_ref[:, head : head + 1] * jnp.sum(queries * keys, axis=-1, keepdims=True)
        below = (
            keep * jnp.sum(normalizer_ref[:, head] * queries, axis=-1, keepdims=True) + score
        )
        answer = (keep * reads[head] + score * values) / jnp.maximum(jnp.abs(below), 1.0)
        gated = (jax.nn.sigmoid(gate) * answer).astype(HALF)
        for copy in range(copies):
            gated_ref[copy, :, head * width : (head + 1) * width] = gated


def stack_kernel(at_ref, *refs):
    out_ref = refs[-1]
    core, chip = at_ref[0], at_ref[1]
    blocks = refs[:-1]
    mine, other = blocks[: len(blocks) // 2], blocks[len(blocks) // 2 :]
    turn = 0
    for ours, theirs in zip(mine, other):
        count, rows, _ = ours.shape
        for at in range(count):
            start = (chip ^ turn) * 2 * rows
            out_ref[pl.ds(pl.multiple_of(start + core * rows, rows), rows), :] = ours[at]
            out_ref[pl.ds(pl.multiple_of(start + (1 - core) * rows, rows), rows), :] = theirs[at]
            turn += 1


def mix_kernel(rows_ref, weight_ref, out_ref):
    out_ref[...] = lax.dot_general(
        rows_ref[...], weight_ref[...], (((1,), (1,)), ((), ())), preferred_element_type=WIDE
    ).astype(HALF)


def send_kernel(
    mixed_ref, tokens_ref, postmix_ref, prefeed_ref, hot_ref, after_ref, input_ref, out_ref
):
    mixed = jnp.concatenate([mixed_ref[i] for i in range(mixed_ref.shape[0])], axis=1)
    residual = tokens_ref[...].astype(WIDE)
    after = (residual + rms_scale(mixed.astype(WIDE), postmix_ref[...])).astype(HALF)
    after_ref[...] = after
    given = rms_scale(after.astype(WIDE), prefeed_ref[...])
    input_ref[...] = given.astype(HALF)
    width = out_ref.shape[1]
    folded = jnp.concatenate(
        [given[:, at : at + width] for at in range(0, given.shape[1], width)], axis=0
    ).astype(HALF)
    dims = (((0,), (0,)), ((), ()))
    out_ref[...] = lax.dot_general(
        hot_ref[...], folded, dims, preferred_element_type=WIDE
    ).astype(HALF)


def turned(values, by):
    by = by % values.shape[1]
    return pltpu.roll(values, by, 1) if by else values


def hold_gate_kernel(after_ref, weight_ref, held_ref, done):
    load = pltpu.make_async_copy(weight_ref, held_ref, done)
    load.start()
    load.wait()


def expert_kernel(came_ref, gate_ref, up_ref, down_ref, out_ref, held_up, held_down, done):
    groups, fold, tall, width = came_ref.shape
    capacity = tall // fold
    spans = [pl.ds(part * width, width) for part in range(fold)]
    loads = [(up_ref.at[span], held_up.at[span]) for span in spans]
    loads += [(down_ref.at[:, span], held_down.at[:, span]) for span in spans]
    loads = [
        pltpu.make_async_copy(source, target, done.at[number])
        for number, (source, target) in enumerate(loads)
    ]
    for load in loads:
        load.start()
    area = lax.broadcasted_iota(jnp.int32, (groups, tall, width), 1) // capacity
    came = [came_ref[:, at].astype(WIDE) for at in range(fold)]
    gates, ups, given = 0.0, 0.0, []
    for part in range(fold):
        for at in range(fold):
            piece = turned(came[at], (at - part) * capacity)
            rows = piece if at == 0 else jnp.where(area == at, piece, rows)
        given.append(rows.reshape(groups * tall, width).astype(HALF))
        gates = gates + jnp.dot(
            given[part], gate_ref[part * width : (part + 1) * width], preferred_element_type=WIDE
        )
    for part in range(fold):
        loads[part].wait()
        ups = ups + jnp.dot(
            given[part], held_up[part * width : (part + 1) * width], preferred_element_type=WIDE
        )
    hidden = (jax.nn.silu(gates) * ups).astype(HALF)
    answers = []
    for part in range(fold):
        loads[fold + part].wait()
        answer = jnp.dot(
            hidden, held_down[:, part * width : (part + 1) * width], preferred_element_type=WIDE
        )
        answers.append(answer.reshape(groups, tall, width))
    for at in range(fold):
        for part in range(fold):
            piece = turned(answers[part], (part - at) * capacity)
            packed = piece if part == 0 else jnp.where(area == part, piece, packed)
        out_ref[:, at] = packed.astype(HALF)


def shared_kernel(input_ref, gate_ref, up_ref, down_ref, out_ref):
    rows = input_ref[...]
    gates = jnp.dot(rows, gate_ref[...], preferred_element_type=WIDE)
    ups = jnp.dot(rows, up_ref[...], preferred_element_type=WIDE)
    hidden = (jax.nn.silu(gates) * ups).astype(HALF)
    out_ref[...] = jnp.dot(hidden, down_ref[...], preferred_element_type=WIDE)


def final_kernel(back_ref, weights_ref, shared_ref, after_ref, gain_ref, out_ref):
    sequences = out_ref.shape[0]
    picked = jnp.dot(weights_ref[...], back_ref[...], preferred_element_type=WIDE)
    step = 2 * sequences
    routed = jnp.concatenate(
        [
            picked[at : at + sequences] + picked[at + sequences : at + step]
            for at in range(0, picked.shape[0], step)
        ],
        axis=1,
    )
    out_ref[...] = (
        after_ref[...].astype(WIDE) + rms_scale(routed + shared_ref[...], gain_ref[...])
    ).astype(HALF)


def on_device(
    tokens,
    premix_gain,
    postmix_gain,
    prefeed_gain,
    postfeed_gain,
    query_weight,
    key_weight,
    value_weight,
    outgate_weight,
    ingate_weight,
    forget_weight,
    ingate_bias,
    forget_bias,
    memory_state,
    normalizer,
    stabilizer,
    output_weight,
    expert_ids,
    route_weights,
    expert_gate,
    expert_up,
    expert_down,
    shared_gate,
    shared_up,
    shared_down,
):
    sequences, model_width = tokens.shape
    devices = lax.axis_size("ep")
    heads, width = memory_state.shape[1], memory_state.shape[3]
    planes = devices // heads
    chips = heads // 2
    place = lax.axis_index("ep")
    at = jnp.stack([place % 2, (place // 2) % chips]).astype(jnp.int32)

    rows = query_weight.shape[0]
    piece_width = model_width // planes
    local_count = expert_gate.shape[0]
    experts_total = local_count * devices
    choose_count = expert_ids.shape[1]
    capacity = min(
        sequences, max(2, 2 * ((sequences * choose_count + experts_total - 1) // experts_total))
    )
    fold = max(1, 8 // capacity)
    tall = fold * capacity
    slot_count = experts_total * tall
    slot_width = model_width // fold

    kept, sent, held_tokens, normed, pieces = local_call(
        functools.partial(start_kernel, planes=planes),
        [
            ((2, *query_weight.shape), HALF, "v"),
            ((2, *query_weight.shape), HALF, "v"),
            ((sequences, model_width), HALF, "v"),
            ((sequences, model_width), HALF, "v"),
            ((devices, sequences, piece_width), HALF, "h"),
        ],
        (at, tokens, premix_gain[None], query_weight, key_weight, value_weight, outgate_weight),
        "shhhhhh",
        scratch=[pltpu.VMEM((1, model_width), WIDE), pltpu.SemaphoreType.DMA((6,))],
    )
    came = swap(sent, CORE)
    rows_in = exchange(pieces)
    dealt = local_call(
        deal_kernel, [((2 * rows, 4 * width), HALF, "v")] * chips, (at, kept, came), "svv"
    )
    blocks = [dealt[0]] + [swap(dealt[turn], CORE * 2 * turn) for turn in range(1, chips)]

    own_out = output_weight.T[None]
    near_out = [own_out] + [swap(own_out, CORE * 2 * turn) for turn in range(1, chips)]
    far_out = [swap(block, CORE) for block in near_out]
    (mix_weight,) = local_call(
        stack_kernel,
        [((piece_width, heads * width), HALF, "v")],
        (at, *near_out, *far_out),
        "s" + "v" * 2 * chips,
    )

    small = (
        ingate_weight.T,
        forget_weight.T,
        ingate_bias[None],
        forget_bias[None],
        stabilizer,
        expert_ids,
        route_weights,
    )
    keep_old, write_new, next_stabilizer, hot, pick, *gains, held_normalizer = local_call(
        functools.partial(prepare_kernel, fold=fold, capacity=capacity),
        [
            ((sequences, heads), WIDE, "v"),
            ((sequences, heads), WIDE, "v"),
            ((sequences, heads), WIDE, "h"),
            ((fold * sequences, slot_count), HALF, "v"),
            ((2 * fold * sequences, slot_count), HALF, "v"),
            ((1, model_width), WIDE, "v"),
            ((1, model_width), WIDE, "v"),
            ((1, model_width), WIDE, "v"),
            (normalizer.shape, WIDE, "v"),
        ],
        (normed, postmix_gain[None], prefeed_gain[None], postfeed_gain[None], normalizer, *small),
        "v" + "h" * 11,
        scratch=[
            *(pltpu.VMEM(array.shape, array.dtype) for array in small),
            pltpu.SemaphoreType.DMA((11,)),
        ],
    )

    (partial,) = local_call(
        project_kernel,
        [((devices * sequences, 4 * width), HALF, "h")],
        (at, rows_in.reshape(devices * sequences, piece_width), *blocks),
        "sv" + "v" * chips,
        scratch=[pltpu.VMEM((piece_width, 4 * width), HALF)],
    )
    partial = partial.reshape(devices, sequences, 4 * width)
    parts = exchange(partial)
    early = 3 * sequences // 8
    (early_memory,) = local_call(
        hold_kernel,
        [((early, *memory_state.shape[1:]), WIDE, "v")],
        (partial, memory_state),
        "hh",
        scratch=[pltpu.SemaphoreType.DMA],
    )
    gated, keys, values = local_call(
        read_kernel,
        [
            ((planes, sequences, heads * width), HALF, "h"),
            ((heads, sequences, width), WIDE, "v"),
            ((heads, sequences, width), WIDE, "v"),
        ],
        (parts, keep_old, write_new, held_normalizer, early_memory, memory_state),
        "vvvvvh",
        scratch=[
            pltpu.VMEM((sequences - early, *memory_state.shape[1:]), WIDE),
            pltpu.SemaphoreType.DMA((sequences - early,)),
        ],
    )
    lines = [[low + heads * plane for plane in range(planes)] for low in range(heads)]
    gathered = exchange(gated, lines)
    (mixed,) = local_call(
        mix_kernel,
        [((planes * sequences, piece_width), HALF, "h")],
        (gathered.reshape(planes * sequences, heads * width), mix_weight),
    )
    mixed = exchange(mixed.reshape(planes, sequences, piece_width), lines)
    after_mix, expert_input, outgoing = local_call(
        send_kernel,
        [
            ((sequences, model_width), HALF, "v"),
            ((sequences, model_width), HALF, "v"),
            ((slot_count, slot_width), HALF, "h"),
        ],
        (mixed, held_tokens, gains[0], gains[1], hot),
    )
    outgoing = outgoing.reshape(experts_total, tall, slot_width)
    arrived = exchange(outgoing)
    arrived = arrived.reshape(devices, local_count, tall, slot_width)
    answers = []
    for expert in range(local_count):
        (held_gate,) = local_call(
            hold_gate_kernel,
            [(expert_gate.shape[1:], HALF, "v")],
            (after_mix, expert_gate[expert]),
            "vh",
            scratch=[pltpu.SemaphoreType.DMA],
        )
        (answer,) = local_call(
            expert_kernel,
            [((devices // fold, fold, tall, slot_width), HALF, "h")],
            (
                arrived[:, expert].reshape(devices // fold, fold, tall, slot_width),
                held_gate,
                expert_up[expert],
                expert_down[expert],
            ),
            "vvhh",
            scratch=[
                pltpu.VMEM(expert_up.shape[1:], HALF),
                pltpu.VMEM(expert_down.shape[1:], HALF),
                pltpu.SemaphoreType.DMA((2 * fold,)),
            ],
        )
        answers.append(answer.reshape(devices, tall, slot_width))
    answered = jnp.stack(answers, axis=1).reshape(experts_total, tall, slot_width)
    returned = exchange(answered)

    (shared_out,) = local_call(
        shared_kernel,
        [((sequences, model_width), WIDE, "v")],
        (expert_input, shared_gate, shared_up, shared_down),
    )
    key_rows, value_rows = keys.swapaxes(0, 1), values.swapaxes(0, 1)
    next_memory = (
        keep_old[..., None, None] * memory_state
        + write_new[..., None, None] * value_rows[..., :, None] * key_rows[..., None, :]
    )
    next_normalizer = keep_old[..., None] * normalizer + write_new[..., None] * key_rows
    (next_tokens,) = local_call(
        final_kernel,
        [((sequences, model_width), HALF, "h")],
        (returned.reshape(slot_count, slot_width), pick, shared_out, after_mix, gains[2]),
    )
    return (next_tokens, next_memory, next_normalizer, next_stabilizer)


def solution(mesh):
    in_specs = (
        P("ep", None),
        P(),
        P(),
        P(),
        P(),
        P("ep", None),
        P("ep", None),
        P("ep", None),
        P("ep", None),
        P(),
        P(),
        P(),
        P(),
        P("ep", None, None, None),
        P("ep", None, None),
        P("ep", None),
        P(None, "ep"),
        P("ep", None),
        P("ep", None),
        P("ep", None, None),
        P("ep", None, None),
        P("ep", None, None),
        P(),
        P(),
        P(),
    )
    out_specs = (P("ep", None), P("ep", None, None, None), P("ep", None, None), P("ep", None))

    return jax.shard_map(
        on_device, mesh=mesh, in_specs=in_specs, out_specs=out_specs, check_vma=False
    )
```

time: 196 us -> 112 us (0.57)
  waiting for transfers between devices: 74.7 us -> 44.2 us
  blocking collectives: 38.7 us -> 8.89 us
  Pallas kernels: 0 us -> 21.7 us
  matrix products: 16.8 us -> 0 us
  between operations: 14.6 us -> 0.85 us
  local copies, waits for them, and re-layouts: 14 us -> 1.82 us
  other arithmetic: 9.39 us -> 4.75 us
  starting transfers between devices: 26.9 us -> 29.5 us
    all_to_all x8 -> x5, waiting for transfers between devices: 66.9 us -> 27.2 us  [exchange(): lax.all_to_all(values, 'ep', split_axis=0, concat_axis=0, tiled=True, axi...]
    all_gather x1 -> x0, blocking collectives: 38.7 us -> none  [on_device(): lax.all_gather(gated_out, 'ep', axis=0, tiled=True)]
    pallas_call x0 -> x13, Pallas kernels: none -> 21.7 us  [local_call(): pl.pallas_call(body, out_shape=[SPACES[space](shape, kind) for shape, kin...]
    ppermute x0 -> x11, waiting for transfers between devices: none -> 17 us  [swap(): return lax.ppermute(values, 'ep', [(i, i ^ bit) for i in range(devices)])]
    dot_general x11 -> x0, matrix products: 16.8 us -> none  [the longest x1 5.57 us: memory_step(): jnp.einsum('shvk,shk->shv', memory_state, query_heads, precision=lax.Prec...]
    all_to_all x0 -> x1, blocking collectives: none -> 8.89 us  [exchange(): lax.all_to_all(values, 'ep', split_axis=0, concat_axis=0, tiled=True, axi...]
    ppermute x0 -> x11, starting transfers between devices: none -> 7.94 us  [swap(): return lax.ppermute(values, 'ep', [(i, i ^ bit) for i in range(devices)])]
    all_gather x1 -> x0, waiting for transfers between devices: 7.7 us -> none  [on_device(): piece_rows = lax.all_gather(normed, 'ep', axis=0, tiled=True)]
  transfers between devices with their start and end apart: 9 -> 16, of which waited for: 9 -> 8; matrix products, arithmetic and copies ran while one was open for 7% -> 5% of each run, Pallas kernels for 0% -> 10%
where the time goes in v2:
time: 112 us
  waiting for transfers between devices  44.2 us (39%)
  starting transfers between devices  29.5 us (26%)
  Pallas kernels  21.7 us (19%)
  blocking collectives  8.89 us (8%)
  other arithmetic  4.75 us (4%)
  local copies, waits for them, and re-layouts  1.82 us (2%)
    all_to_all x5, waiting for transfers between devices, exchange(): lax.all_to_all(values, 'ep', split_axis=0, concat_axis=0, tiled=True, axi...  27.2 us
    pallas_call x13, Pallas kernels, local_call(): pl.pallas_call(body, out_shape=[SPACES[space](shape, kind) for shape, kin...  21.7 us
    all_to_all x5, starting transfers between devices, exchange(): lax.all_to_all(values, 'ep', split_axis=0, concat_axis=0, tiled=True, axi...  21.5 us
    ppermute x11, waiting for transfers between devices, swap(): return lax.ppermute(values, 'ep', [(i, i ^ bit) for i in range(devices)])  17 us
    all_to_all x1, blocking collectives, exchange(): lax.all_to_all(values, 'ep', split_axis=0, concat_axis=0, tiled=True, axi...  8.89 us
    ppermute x11, starting transfers between devices, swap(): return lax.ppermute(values, 'ep', [(i, i ^ bit) for i in range(devices)])  7.94 us
    add x1, other arithmetic, on_device(): keep_old[..., None, None] * memory_state  4.59 us
  transfers between devices with their start and end apart: 16, of which 8 were waited for; matrix products, arithmetic and copies ran while one was open for 5% of the time, Pallas kernels for 10%

profile of v2, /device:TPU:0, one launch (start us, length us, event | category | flops | bytes accessed | tf_op | source)
XLA Modules:
  0.0 111.6 jit_solution(15953713493967253082)
XLA Ops:
  0.7 2.4 %shard_map.264 = (bf16[2,64,1024]{2,1,0:T(8,128)(2,1)S(1)}, bf16[2,64,1024]{2,1,0:T(8,128)(2,1)S(1)}, bf16[8,2048]{1,0:T(8,128)(2,1)S(1)}, bf16[8,2048]{1,0:T(8,128)(2,1)S(1)}, bf16[32,8,512]{2,1,0:T(8,128)(2,1)}) custom-call(s32[2]{0:T(128)S(1)} %pad_add_fusion.at_ref, bf16[8,2048]{1,0:T(8,128)(2,1)} %tokens_ref.1, f32[1,2048]{1,0:T(1,128)} %bitcast.48, ...), custom_call_target="tpu_custom_call" | custom-call | tf_op jit(solution)/shard_map/pallas_call | solution.py:40
  3.2 7.3 %all-to-all-start = ((bf16[32,8,512]{2,1,0:T(8,128)(2,1)}), bf16[32,8,512]{2,1,0:T(8,128)(2,1)S(1)}, u32[]{:S(2)}, u32[]{:S(2)}) async-start(bf16[32,8,512]{2,1,0:T(8,128)(2,1)} %get-tuple-element.28), calls=%async_computation | async-start | bytes 524288 | tf_op jit(solution)/shard_map/all_to_all | solution.py:26
  12.7 1.8 %collective-permute-start.1 = (bf16[128,512]{1,0:T(8,128)(2,1)S(1)}, bf16[128,512]{1,0:T(8,128)(2,1)S(1)}, u32[]{:S(2)}, u32[]{:S(2)}) collective-permute-start(bf16[128,512]{1,0:T(8,128)(2,1)S(1)} %get-tuple-element.32), channel_id=1, source_target_pairs={{0,2},{1,3},{2,0},{3,1},{4,6},{5,7},{6,4},{7,5},{8,10},{9,11},{10,... | collective-permute-start | bytes 393224 | tf_op jit(solution)/shard_map/ppermute | solution.py:22
  14.6 1.5 %collective-permute-start.2 = (bf16[128,512]{1,0:T(8,128)(2,1)S(1)}, bf16[128,512]{1,0:T(8,128)(2,1)S(1)}, u32[]{:S(2)}, u32[]{:S(2)}) collective-permute-start(bf16[128,512]{1,0:T(8,128)(2,1)S(1)} %get-tuple-element.33), channel_id=1, source_target_pairs={{0,4},{1,5},{2,6},{3,7},{4,0},{5,1},{6,2},{7,3},{8,12},{9,13},{10,... | collective-permute-start | bytes 393224 | tf_op jit(solution)/shard_map/ppermute | solution.py:22
  16.3 3.9 %collective-permute-done.1.refs_1_ = bf16[128,512]{1,0:T(8,128)(2,1)S(1)} collective-permute-done((bf16[128,512]{1,0:T(8,128)(2,1)S(1)}, bf16[128,512]{1,0:T(8,128)(2,1)S(1)}, u32[]{:S(2)}, u32[]{:S(2)}) %collective-permute-start.1) | collective-permute-done | bytes 131104 | tf_op jit(solution)/shard_map/ppermute | solution.py:22
  20.2 3.4 %collective-permute-done.2.refs_2_ = bf16[128,512]{1,0:T(8,128)(2,1)S(1)} collective-permute-done((bf16[128,512]{1,0:T(8,128)(2,1)S(1)}, bf16[128,512]{1,0:T(8,128)(2,1)S(1)}, u32[]{:S(2)}, u32[]{:S(2)}) %collective-permute-start.2) | collective-permute-done | bytes 131104 | tf_op jit(solution)/shard_map/ppermute | solution.py:22
  23.6 1.6 %shard_map.266 = bf16[256,512]{1,0:T(8,128)(2,1)} custom-call(s32[2]{0:T(128)S(1)} %pad_add_fusion.at_ref, bf16[256,512]{1,0:T(8,128)(2,1)S(1)} %bitcast.30, bf16[128,512]{1,0:T(8,128)(2,1)S(1)} %get-tuple-element.31.refs_0_, bf16[128,512]{1,0:T(8,128)(2,1)S(1)} %collective-permute-done.1.refs_1_, bf16[128,512]{1,0:T(8,128)(2,1)S(1)} %collective-permute-done.2.refs_2_, ...), custom_call_target="tpu_custom_call" | custom-call | tf_op jit(solution)/shard_map/pallas_call | solution.py:40
  25.2 4.1 %all-to-all-start.1 = ((bf16[32,8,512]{2,1,0:T(8,128)(2,1)}), bf16[32,8,512]{2,1,0:T(8,128)(2,1)S(1)}, u32[]{:S(2)}, u32[]{:S(2)}) async-start(bf16[32,8,512]{2,1,0:T(8,128)(2,1)} %bitcast.38), calls=%async_computation.1 | async-start | bytes 524288 | tf_op jit(solution)/shard_map/all_to_all | solution.py:26
  29.3 2.7 %collective-permute-start.6 = (bf16[1,64,1024]{2,1,0:T(8,128)(2,1)}, bf16[1,64,1024]{2,1,0:T(8,128)(2,1)S(1)}, u32[]{:S(2)}, u32[]{:S(2)}) collective-permute-start(bf16[1,64,1024]{2,1,0:T(8,128)(2,1)} %bitcast.32), channel_id=1, source_target_pairs={{0,6},{1,7},{2,4},{3,5},{4,2},{5,3},{6,0},{7,1},{8,14},{9,15},{10,... | collective-permute-start | bytes 393224 | tf_op jit(solution)/shard_map/ppermute | solution.py:22
  32.8 6.1 %collective-permute-done.6.refs_3_ = bf16[1,64,1024]{2,1,0:T(8,128)(2,1)S(1)} collective-permute-done((bf16[1,64,1024]{2,1,0:T(8,128)(2,1)}, bf16[1,64,1024]{2,1,0:T(8,128)(2,1)S(1)}, u32[]{:S(2)}, u32[]{:S(2)}) %collective-permute-start.6) | collective-permute-done | bytes 131104 | tf_op jit(solution)/shard_map/ppermute | solution.py:22
  38.9 2.3 %collective-permute-done.5.refs_2_ = bf16[1,64,1024]{2,1,0:T(8,128)(2,1)S(1)} collective-permute-done((bf16[1,64,1024]{2,1,0:T(8,128)(2,1)}, bf16[1,64,1024]{2,1,0:T(8,128)(2,1)S(1)}, u32[]{:S(2)}, u32[]{:S(2)}) %collective-permute-start.5) | collective-permute-done | bytes 131104 | tf_op jit(solution)/shard_map/ppermute | solution.py:22
  41.7 1.7 %shard_map.267 = (f32[8,8]{1,0:T(8,128)S(1)}, f32[8,8]{1,0:T(8,128)S(1)}, f32[8,8]{1,0:T(8,128)}, bf16[16,256]{1,0:T(8,128)(2,1)S(1)}, bf16[32,256]{1,0:T(8,128)...) custom-call(bf16[8,2048]{1,0:T(8,128)(2,1)S(1)} %get-tuple-element.3, ...), custom_call_target="tpu_custom_call" | custom-call | tf_op jit(solution)/shard_map/pallas_call | solution.py:40
  43.5 1.4 %shard_map.268.early_ref = f32[3,8,128,128]{3,2,1,0:T(8,128)S(1)} custom-call(bf16[32,8,512]{2,1,0:T(8,128)(2,1)} %bitcast.39, f32[8,8,128,128]{3,2,1,0:T(8,128)} %memory_ref.3), custom_call_target="tpu_custom_call" | custom-call | tf_op jit(solution)/shard_map/pallas_call | solution.py:40
  44.9 3.7 %shard_map.269 = (bf16[4,8,1024]{2,1,0:T(8,128)(2,1)}, f32[8,8,128]{2,1,0:T(8,128)S(1)}, f32[8,8,128]{2,1,0:T(8,128)S(1)}) custom-call(bf16[32,8,512]{2,1,0:T(8,128)(2,1)S(1)} %all-to-all-done.1.parts_ref, f32[8,8]{1,0:T(8,128)S(1)} %get-tuple-element.36.keep_ref, f32[8,8]{1,0:T(8,128)S(1)} %get-tuple-element.37.write_ref, ...), custom_call_target="tpu_custom_call" | custom-call | tf_op jit(solution)/shard_map/pallas_call | solution.py:40
  48.6 4.6 %all-to-all-start.2 = ((bf16[4,8,1024]{2,1,0:T(8,128)(2,1)}), bf16[4,8,1024]{2,1,0:T(8,128)(2,1)S(1)}, u32[]{:S(2)}, u32[]{:S(2)}) async-start(bf16[4,8,1024]{2,1,0:T(8,128)(2,1)} %get-tuple-element.39), calls=%async_computation.2 | async-start | bytes 131072 | tf_op jit(solution)/shard_map/all_to_all | solution.py:26
  53.9 5.1 %all-to-all-done.2 = bf16[4,8,1024]{2,1,0:T(8,128)(2,1)S(1)} async-done(((bf16[4,8,1024]{2,1,0:T(8,128)(2,1)}), bf16[4,8,1024]{2,1,0:T(8,128)(2,1)S(1)}, u32[]{:S(2)}, u32[]{:S(2)}) %all-to-all-start.2) | async-done | bytes 65568 | tf_op jit(solution)/shard_map/all_to_all | solution.py:26
  60.0 8.9 %all_to_all.30.mixed_ref = bf16[4,8,512]{2,1,0:T(8,128)(2,1)S(1)} all-to-all(bf16[4,8,512]{2,1,0:T(8,128)(2,1)} %bitcast.45), channel_id=1, replica_groups={{0,8,16,24},{1,9,17,25},{2,10,18,26},{3,11,19,27},{4,12,20,28},{5,13,21..., dimensions={0} | all-to-all | bytes 65536 | tf_op jit(solution)/shard_map/all_to_all | solution.py:26
  70.2 2.6 %all-to-all-start.4 = ((bf16[32,8,1024]{2,1,0:T(8,128)(2,1)}), bf16[32,8,1024]{2,1,0:T(8,128)(2,1)S(1)}, u32[]{:S(2)}, u32[]{:S(2)}) async-start(bf16[32,8,1024]{2,1,0:T(8,128)(2,1)} %bitcast.44), calls=%async_computation.4 | async-start | bytes 1048576 | tf_op jit(solution)/shard_map/all_to_all | solution.py:26
  72.8 1.6 %shard_map.273.gate_ref = bf16[2048,512]{1,0:T(8,128)(2,1)S(1)} custom-call(bf16[8,2048]{1,0:T(8,128)(2,1)S(1)} %get-tuple-element.45.after_ref, bf16[2048,512]{1,0:T(8,128)(2,1)} %bitcast.43), custom_call_target="tpu_custom_call" | custom-call | tf_op jit(solution)/shard_map/pallas_call | solution.py:40
  74.4 14.0 %all-to-all-done.4 = bf16[32,8,1024]{2,1,0:T(8,128)(2,1)S(1)} async-done(((bf16[32,8,1024]{2,1,0:T(8,128)(2,1)}), bf16[32,8,1024]{2,1,0:T(8,128)(2,1)S(1)}, u32[]{:S(2)}, u32[]{:S(2)}) %all-to-all-start.4) | async-done | bytes 524320 | tf_op jit(solution)/shard_map/all_to_all | solution.py:26
  88.4 3.8 %shard_map.274 = bf16[16,2,8,1024]{3,2,1,0:T(8,128)(2,1)} custom-call(bf16[16,2,8,1024]{3,2,1,0:T(8,128)(2,1)S(1)} %bitcast.28, bf16[2048,512]{1,0:T(8,128)(2,1)S(1)} %shard_map.273.gate_ref, bf16[2048,512]{1,0:T(8,128)(2,1)} %bitcast.41, bf16[512,2048]{1,0:T(8,128)(2,1)} %bitcast.42), custom_call_target="tpu_custom_call" | custom-call | tf_op jit(solution)/shard_map/pallas_call | solution.py:40
  92.2 2.9 %all-to-all-start.5 = ((bf16[32,8,1024]{2,1,0:T(8,128)(2,1)}), bf16[32,8,1024]{2,1,0:T(8,128)(2,1)S(1)}, u32[]{:S(2)}, u32[]{:S(2)}) async-start(bf16[32,8,1024]{2,1,0:T(8,128)(2,1)} %bitcast.40), calls=%async_computation.5 | async-start | bytes 1048576 | tf_op jit(solution)/shard_map/all_to_all | solution.py:26
  96.0 4.6 %multiply_add_fusion = f32[8,8,128,128]{3,2,1,0:T(8,128)} fusion(f32[8,8,128,128]{3,2,1,0:T(8,128)} %memory_ref.3, f32[8,8,128]{2,1,0:T(8,128)S(1)} %copy.31, f32[8,8,128]{2,1,0:T(8,128)S(1)} %copy.30, f32[8,8]{1,0:T(8,128)S(1)} %get-tuple-element.36.keep_ref), kind=kLoop, calls=%fused_computation | loop fusion | flops 3145728 | bytes 8454400 | tf_op jit(solution)/shard_map/add | solution.py:569
  102.6 8.1 %all-to-all-done.5 = bf16[32,8,1024]{2,1,0:T(8,128)(2,1)S(1)} async-done(((bf16[32,8,1024]{2,1,0:T(8,128)(2,1)}), bf16[32,8,1024]{2,1,0:T(8,128)(2,1)S(1)}, u32[]{:S(2)}, u32[]{:S(2)}) %all-to-all-start.5) | async-done | bytes 524320 | tf_op jit(solution)/shard_map/all_to_all | solution.py:26
  (40 shorter events, 10.7 us)
Async XLA Ops:
  3.2 20.4 %all-to-all-start = ((bf16[32,8,512]{2,1,0:T(8,128)(2,1)}), bf16[32,8,512]{2,1,0:T(8,128)(2,1)S(1)}, u32[]{:S(2)}, u32[]{:S(2)}) async-start(bf16[32,8,512]{2,1,0:T(8,128)(2,1)} %get-tuple-element.28), calls=%async_computation | async-start | bytes 524288 | tf_op jit(solution)/shard_map/all_to_all | solution.py:26
  10.5 1.6 %collective-permute-start = (bf16[2,64,1024]{2,1,0:T(8,128)(2,1)S(1)}, bf16[2,64,1024]{2,1,0:T(8,128)(2,1)S(1)}, u32[]{:S(2)}, u32[]{:S(2)}) collective-permute-start(bf16[2,64,1024]{2,1,0:T(8,128)(2,1)S(1)} %get-tuple-element.30), channel_id=1, source_target_pairs={{0,1},{1,0},{2,3},{3,2},{4,5},{5,4},{6,7},{7,6},{8,9},{9,8},{10,11... | collective-permute-start | bytes 786440 | tf_op jit(solution)/shard_map/ppermute | solution.py:22
  12.7 7.4 %collective-permute-start.1 = (bf16[128,512]{1,0:T(8,128)(2,1)S(1)}, bf16[128,512]{1,0:T(8,128)(2,1)S(1)}, u32[]{:S(2)}, u32[]{:S(2)}) collective-permute-start(bf16[128,512]{1,0:T(8,128)(2,1)S(1)} %get-tuple-element.32), channel_id=1, source_target_pairs={{0,2},{1,3},{2,0},{3,1},{4,6},{5,7},{6,4},{7,5},{8,10},{9,11},{10,... | collective-permute-start | bytes 393224 | tf_op jit(solution)/shard_map/ppermute | solution.py:22
  14.6 9.0 %collective-permute-start.2 = (bf16[128,512]{1,0:T(8,128)(2,1)S(1)}, bf16[128,512]{1,0:T(8,128)(2,1)S(1)}, u32[]{:S(2)}, u32[]{:S(2)}) collective-permute-start(bf16[128,512]{1,0:T(8,128)(2,1)S(1)} %get-tuple-element.33), channel_id=1, source_target_pairs={{0,4},{1,5},{2,6},{3,7},{4,0},{5,1},{6,2},{7,3},{8,12},{9,13},{10,... | collective-permute-start | bytes 393224 | tf_op jit(solution)/shard_map/ppermute | solution.py:22
  16.0 7.6 %collective-permute-start.3 = (bf16[128,512]{1,0:T(8,128)(2,1)S(1)}, bf16[128,512]{1,0:T(8,128)(2,1)S(1)}, u32[]{:S(2)}, u32[]{:S(2)}) collective-permute-start(bf16[128,512]{1,0:T(8,128)(2,1)S(1)} %get-tuple-element.34), channel_id=1, source_target_pairs={{0,6},{1,7},{2,4},{3,5},{4,2},{5,3},{6,0},{7,1},{8,14},{9,15},{10,... | collective-permute-start | bytes 393224 | tf_op jit(solution)/shard_map/ppermute | solution.py:22
  25.2 19.7 %all-to-all-start.1 = ((bf16[32,8,512]{2,1,0:T(8,128)(2,1)}), bf16[32,8,512]{2,1,0:T(8,128)(2,1)S(1)}, u32[]{:S(2)}, u32[]{:S(2)}) async-start(bf16[32,8,512]{2,1,0:T(8,128)(2,1)} %bitcast.38), calls=%async_computation.1 | async-start | bytes 524288 | tf_op jit(solution)/shard_map/all_to_all | solution.py:26
  29.3 9.7 %collective-permute-start.6 = (bf16[1,64,1024]{2,1,0:T(8,128)(2,1)}, bf16[1,64,1024]{2,1,0:T(8,128)(2,1)S(1)}, u32[]{:S(2)}, u32[]{:S(2)}) collective-permute-start(bf16[1,64,1024]{2,1,0:T(8,128)(2,1)} %bitcast.32), channel_id=1, source_target_pairs={{0,6},{1,7},{2,4},{3,5},{4,2},{5,3},{6,0},{7,1},{8,14},{9,15},{10,... | collective-permute-start | bytes 393224 | tf_op jit(solution)/shard_map/ppermute | solution.py:22
  32.0 9.2 %collective-permute-start.5 = (bf16[1,64,1024]{2,1,0:T(8,128)(2,1)}, bf16[1,64,1024]{2,1,0:T(8,128)(2,1)S(1)}, u32[]{:S(2)}, u32[]{:S(2)}) collective-permute-start(bf16[1,64,1024]{2,1,0:T(8,128)(2,1)} %bitcast.33), channel_id=1, source_target_pairs={{0,4},{1,5},{2,6},{3,7},{4,0},{5,1},{6,2},{7,3},{8,12},{9,13},{10,... | collective-permute-start | bytes 393224 | tf_op jit(solution)/shard_map/ppermute | solution.py:22
  32.6 8.6 %collective-permute-start.4 = (bf16[1,64,1024]{2,1,0:T(8,128)(2,1)}, bf16[1,64,1024]{2,1,0:T(8,128)(2,1)S(1)}, u32[]{:S(2)}, u32[]{:S(2)}) collective-permute-start(bf16[1,64,1024]{2,1,0:T(8,128)(2,1)} %bitcast.34), channel_id=1, source_target_pairs={{0,2},{1,3},{2,0},{3,1},{4,6},{5,7},{6,4},{7,5},{8,10},{9,11},{10,... | collective-permute-start | bytes 393224 | tf_op jit(solution)/shard_map/ppermute | solution.py:22
  32.8 20.4 %collective-permute-start.7 = (bf16[1,64,1024]{2,1,0:T(8,128)(2,1)}, bf16[1,64,1024]{2,1,0:T(8,128)(2,1)S(1)}, u32[]{:S(2)}, u32[]{:S(2)}) collective-permute-start(bf16[1,64,1024]{2,1,0:T(8,128)(2,1)} %bitcast.35), channel_id=1, source_target_pairs={{0,1},{1,0},{2,3},{3,2},{4,5},{5,4},{6,7},{7,6},{8,9},{9,8},{10,11... | collective-permute-start | bytes 393224 | tf_op jit(solution)/shard_map/ppermute | solution.py:22
  38.9 14.3 %collective-permute-start.10 = (bf16[1,64,1024]{2,1,0:T(8,128)(2,1)S(1)}, bf16[1,64,1024]{2,1,0:T(8,128)(2,1)S(1)}, u32[]{:S(2)}, u32[]{:S(2)}) collective-permute-start(bf16[1,64,1024]{2,1,0:T(8,128)(2,1)S(1)} %collective-permute-done.6.refs_3_), channel_id=1, source_target_pairs={{0,1},{1,0},{2,3},{3,2},{4,5},{5,4},{6,7},{7,6},{8,9},{9,8},{10,11... | collective-permute-start | bytes 393224 | tf_op jit(solution)/shard_map/ppermute | solution.py:22
  41.2 12.1 %collective-permute-start.9 = (bf16[1,64,1024]{2,1,0:T(8,128)(2,1)S(1)}, bf16[1,64,1024]{2,1,0:T(8,128)(2,1)S(1)}, u32[]{:S(2)}, u32[]{:S(2)}) collective-permute-start(bf16[1,64,1024]{2,1,0:T(8,128)(2,1)S(1)} %collective-permute-done.5.refs_2_), channel_id=1, source_target_pairs={{0,1},{1,0},{2,3},{3,2},{4,5},{5,4},{6,7},{7,6},{8,9},{9,8},{10,11... | collective-permute-start | bytes 393224 | tf_op jit(solution)/shard_map/ppermute | solution.py:22
  41.2 12.1 %collective-permute-start.8 = (bf16[1,64,1024]{2,1,0:T(8,128)(2,1)S(1)}, bf16[1,64,1024]{2,1,0:T(8,128)(2,1)S(1)}, u32[]{:S(2)}, u32[]{:S(2)}) collective-permute-start(bf16[1,64,1024]{2,1,0:T(8,128)(2,1)S(1)} %collective-permute-done.4.refs_1_), channel_id=1, source_target_pairs={{0,1},{1,0},{2,3},{3,2},{4,5},{5,4},{6,7},{7,6},{8,9},{9,8},{10,11... | collective-permute-start | bytes 393224 | tf_op jit(solution)/shard_map/ppermute | solution.py:22
  44.9 8.4 %copy-start.3 = (bf16[1024,64]{0,1:T(8,128)(2,1)S(1)}, bf16[1024,64]{0,1:T(8,128)(2,1)}, u32[]{:S(2)}) copy-start(bf16[1024,64]{0,1:T(8,128)(2,1)} %param.41) | copy-start | bytes 393220
  48.6 10.4 %all-to-all-start.2 = ((bf16[4,8,1024]{2,1,0:T(8,128)(2,1)}), bf16[4,8,1024]{2,1,0:T(8,128)(2,1)S(1)}, u32[]{:S(2)}, u32[]{:S(2)}) async-start(bf16[4,8,1024]{2,1,0:T(8,128)(2,1)} %get-tuple-element.39), calls=%async_computation.2 | async-start | bytes 131072 | tf_op jit(solution)/shard_map/all_to_all | solution.py:26
  70.2 18.2 %all-to-all-start.4 = ((bf16[32,8,1024]{2,1,0:T(8,128)(2,1)}), bf16[32,8,1024]{2,1,0:T(8,128)(2,1)S(1)}, u32[]{:S(2)}, u32[]{:S(2)}) async-start(bf16[32,8,1024]{2,1,0:T(8,128)(2,1)} %bitcast.44), calls=%async_computation.4 | async-start | bytes 1048576 | tf_op jit(solution)/shard_map/all_to_all | solution.py:26
  88.4 6.8 %copy-start.4 = (f32[8,8,128]{2,1,0:T(8,128)S(1)}, f32[8,8,128]{2,1,0:T(8,128)}, u32[]{:S(2)}) copy-start(f32[8,8,128]{2,1,0:T(8,128)} %refs_3_.3) | copy-start | bytes 98308
  92.2 18.5 %all-to-all-start.5 = ((bf16[32,8,1024]{2,1,0:T(8,128)(2,1)}), bf16[32,8,1024]{2,1,0:T(8,128)(2,1)S(1)}, u32[]{:S(2)}, u32[]{:S(2)}) async-start(bf16[32,8,1024]{2,1,0:T(8,128)(2,1)} %bitcast.40), calls=%async_computation.5 | async-start | bytes 1048576 | tf_op jit(solution)/shard_map/all_to_all | solution.py:26
  96.0 4.6 %copy-start = (bf16[2048,512]{1,0:T(8,128)(2,1)S(1)}, bf16[2048,512]{1,0:T(8,128)(2,1)}, u32[]{:S(2)}) copy-start(bf16[2048,512]{1,0:T(8,128)(2,1)} %gate_ref.1) | copy-start | bytes 6291460
  96.0 4.6 %copy-start.1 = (bf16[2048,512]{1,0:T(8,128)(2,1)S(1)}, bf16[2048,512]{1,0:T(8,128)(2,1)}, u32[]{:S(2)}) copy-start(bf16[2048,512]{1,0:T(8,128)(2,1)} %up_ref.1) | copy-start | bytes 6291460
  96.0 5.6 %copy-start.2 = (bf16[512,2048]{1,0:T(8,128)(2,1)S(1)}, bf16[512,2048]{1,0:T(8,128)(2,1)}, u32[]{:S(2)}) copy-start(bf16[512,2048]{1,0:T(8,128)(2,1)} %down_ref.1) | copy-start | bytes 6291460

commit v3 on v2

--- a/solution.py
+++ b/solution.py
@@ -253,44 +253,60 @@
             gated_ref[copy, :, head * width : (head + 1) * width] = gated
 
 
+def merge_kernel(*refs):
+    out_ref = refs[-1]
+    for number, block in enumerate(refs[:-1]):
+        out_ref[number] = block[0]
+
+
 def stack_kernel(at_ref, *refs):
-    out_ref = refs[-1]
-    core, chip = at_ref[0], at_ref[1]
-    blocks = refs[:-1]
-    mine, other = blocks[: len(blocks) // 2], blocks[len(blocks) // 2 :]
-    turn = 0
-    for ours, theirs in zip(mine, other):
-        count, rows, _ = ours.shape
-        for at in range(count):
-            start = (chip ^ turn) * 2 * rows
-            out_ref[pl.ds(pl.multiple_of(start + core * rows, rows), rows), :] = ours[at]
-            out_ref[pl.ds(pl.multiple_of(start + (1 - core) * rows, rows), rows), :] = theirs[at]
-            turn += 1
-
-
-def mix_kernel(rows_ref, weight_ref, out_ref):
-    out_ref[...] = lax.dot_general(
-        rows_ref[...], weight_ref[...], (((1,), (1,)), ((), ())), preferred_element_type=WIDE
+    blocks, out_ref = refs[:-1], refs[-1]
+    core, chip, side = at_ref[0], at_ref[1], at_ref[2]
+    chips = len(blocks) // 2
+    count, rows, _ = blocks[0].shape
+    for turn in range(chips):
+        for number in range(count):
+            start = ((side ^ number) * chips + (chip ^ turn)) * 2 * rows
+            for block, half in ((blocks[turn], core), (blocks[chips + turn], 1 - core)):
+                place = pl.ds(pl.multiple_of(start + half * rows, rows), rows)
+                out_ref[place, :] = block[number]
+
+
+def mix_kernel(*refs):
+    rows = jnp.concatenate([ref[...] for ref in refs[:-2]], axis=0)
+    refs[-1][...] = lax.dot_general(
+        rows, refs[-2][...], (((1,), (1,)), ((), ())), preferred_element_type=WIDE
     ).astype(HALF)
 
 
-def send_kernel(
-    mixed_ref, tokens_ref, postmix_ref, prefeed_ref, hot_ref, after_ref, input_ref, out_ref
-):
-    mixed = jnp.concatenate([mixed_ref[i] for i in range(mixed_ref.shape[0])], axis=1)
-    residual = tokens_ref[...].astype(WIDE)
-    after = (residual + rms_scale(mixed.astype(WIDE), postmix_ref[...])).astype(HALF)
-    after_ref[...] = after
+def send_kernel(at_ref, *refs, pieces):
+    mixed, refs = [piece[...].astype(WIDE) for piece in refs[:pieces]], refs[pieces:]
+    homes = (len(refs) - 5) // 2
+    tokens, hots, refs = refs[:homes], refs[homes : 2 * homes], refs[2 * homes :]
+    postmix_ref, prefeed_ref, after_ref, input_ref, out_ref = refs
+    sequences = after_ref.shape[0]
+    if homes == 2:
+        ours, theirs = mixed
+        theirs = jnp.concatenate([theirs[sequences:], theirs[:sequences]], axis=0)
+        first = at_ref[3] == 0
+        mixed = [jnp.where(first, ours, theirs), jnp.where(first, theirs, ours)]
+    mixed = jnp.concatenate(mixed, axis=1)
+    residual = jnp.concatenate([ref[...].astype(WIDE) for ref in tokens], axis=0)
+    after = (residual + rms_scale(mixed, postmix_ref[...])).astype(HALF)
+    after_ref[...] = after[:sequences]
     given = rms_scale(after.astype(WIDE), prefeed_ref[...])
-    input_ref[...] = given.astype(HALF)
-    width = out_ref.shape[1]
-    folded = jnp.concatenate(
-        [given[:, at : at + width] for at in range(0, given.shape[1], width)], axis=0
-    ).astype(HALF)
+    input_ref[...] = given[:sequences].astype(HALF)
+    blocks, _, tall, width = out_ref.shape
     dims = (((0,), (0,)), ((), ()))
-    out_ref[...] = lax.dot_general(
-        hot_ref[...], folded, dims, preferred_element_type=WIDE
-    ).astype(HALF)
+    for home, hot in enumerate(hots):
+        mine = given[home * sequences : (home + 1) * sequences]
+        folded = jnp.concatenate(
+            [mine[:, at : at + width] for at in range(0, given.shape[1], width)], axis=0
+        ).astype(HALF)
+        start = at_ref[3] * (blocks * tall) if homes == 2 else 0
+        lanes = hot[:, pl.ds(pl.multiple_of(start, blocks * tall), blocks * tall)]
+        rows = lax.dot_general(lanes, folded, dims, preferred_element_type=WIDE)
+        out_ref[:, home] = rows.astype(HALF).reshape(blocks, tall, width)
 
 
 def turned(values, by):
@@ -304,7 +320,8 @@
     load.wait()
 
 
-def expert_kernel(came_ref, gate_ref, up_ref, down_ref, out_ref, held_up, held_down, done):
+def expert_kernel(at_ref, came_ref, gate_ref, up_ref, down_ref, out_ref, held_up, held_down, done, *, split
+):
     groups, fold, tall, width = came_ref.shape
     capacity = tall // fold
     spans = [pl.ds(part * width, width) for part in range(fold)]
@@ -344,7 +361,7 @@
         for part in range(fold):
             piece = turned(answers[part], (part - at) * capacity)
             packed = piece if part == 0 else jnp.where(area == part, piece, packed)
-        out_ref[:, at] = packed.astype(HALF)
+        out_ref[at ^ at_ref[3] if split else at] = packed.astype(HALF)
 
 
 def shared_kernel(input_ref, gate_ref, up_ref, down_ref, out_ref):
@@ -403,8 +420,12 @@
     heads, width = memory_state.shape[1], memory_state.shape[3]
     planes = devices // heads
     chips = heads // 2
+    groups = planes // 2
+    copies = 1 if groups == 2 else groups
     place = lax.axis_index("ep")
-    at = jnp.stack([place % 2, (place // 2) % chips]).astype(jnp.int32)
+    at = jnp.stack(
+        [place % 2, place // 2 % chips, place // heads % 2, place // (2 * heads)]
+    ).astype(jnp.int32)
 
     rows = query_weight.shape[0]
     piece_width = model_width // planes
@@ -440,12 +461,16 @@
     blocks = [dealt[0]] + [swap(dealt[turn], CORE * 2 * turn) for turn in range(1, chips)]
 
     own_out = output_weight.T[None]
-    near_out = [own_out] + [swap(own_out, CORE * 2 * turn) for turn in range(1, chips)]
-    far_out = [swap(block, CORE) for block in near_out]
+    across_out = swap(own_out, heads)
+    (pair,) = local_call(
+        merge_kernel, [((2, *own_out.shape[1:]), HALF, "v")], (own_out, across_out)
+    )
+    ours = [pair] + [swap(pair, CORE * 2 * turn) for turn in range(1, chips)]
+    theirs = [swap(block, CORE) for block in ours]
     (mix_weight,) = local_call(
         stack_kernel,
-        [((piece_width, heads * width), HALF, "v")],
-        (at, *near_out, *far_out),
+        [((2 * piece_width, heads * width), HALF, "v")],
+        (at, *ours, *theirs),
         "s" + "v" * 2 * chips,
     )
 
@@ -499,7 +524,7 @@
     gated, keys, values = local_call(
         read_kernel,
         [
-            ((planes, sequences, heads * width), HALF, "h"),
+            ((copies, sequences, heads * width), HALF, "v"),
             ((heads, sequences, width), WIDE, "v"),
             ((heads, sequences, width), WIDE, "v"),
         ],
@@ -510,26 +535,52 @@
             pltpu.SemaphoreType.DMA((sequences - early,)),
         ],
     )
-    lines = [[low + heads * plane for plane in range(planes)] for low in range(heads)]
-    gathered = exchange(gated, lines)
-    (mixed,) = local_call(
-        mix_kernel,
-        [((planes * sequences, piece_width), HALF, "h")],
-        (gathered.reshape(planes * sequences, heads * width), mix_weight),
-    )
-    mixed = exchange(mixed.reshape(planes, sequences, piece_width), lines)
+    paired = groups == 2 and fold == 2
+    if groups == 2:
+        gated_rows = [gated[0], swap(gated[0], 2 * heads)]
+        (own_mixed,) = local_call(
+            mix_kernel,
+            [((2 * sequences, 2 * piece_width), HALF, "v")],
+            (*gated_rows, mix_weight),
+        )
+        mixed = [own_mixed, swap(own_mixed, 2 * heads)]
+        if not paired:
+            theirs = mixed[1][sequences:]
+            first = at[3] == 0
+            mixed = [
+                jnp.where(first, own_mixed[:sequences], theirs),
+                jnp.where(first, theirs, own_mixed[:sequences]),
+            ]
+    else:
+        lines = [[low + 2 * heads * at for at in range(groups)] for low in range(2 * heads)]
+        gathered = exchange(gated, lines).reshape(groups * sequences, heads * width)
+        (mixed,) = local_call(
+            mix_kernel,
+            [((groups * sequences, 2 * piece_width), HALF, "h")],
+            (gathered, mix_weight),
+        )
+        mixed = exchange(mixed.reshape(groups, sequences, 2 * piece_width), lines)
+        mixed = [mixed[number] for number in range(groups)]
+    homes = 2 if paired else 1
+    held, hots, members = [held_tokens], [hot], None
+    if paired:
+        held.append(swap(held_tokens, 2 * heads))
+        hots.append(swap(hot, 2 * heads))
+        half = devices // 2
+        members = [list(range(half)), list(range(half, devices))]
     after_mix, expert_input, outgoing = local_call(
-        send_kernel,
+        functools.partial(send_kernel, pieces=len(mixed)),
         [
             ((sequences, model_width), HALF, "v"),
             ((sequences, model_width), HALF, "v"),
-            ((slot_count, slot_width), HALF, "h"),
+            ((experts_total // homes, homes, tall, slot_width), HALF, "h"),
         ],
-        (mixed, held_tokens, gains[0], gains[1], hot),
-    )
-    outgoing = outgoing.reshape(experts_total, tall, slot_width)
-    arrived = exchange(outgoing)
-    arrived = arrived.reshape(devices, local_count, tall, slot_width)
+        (at, *mixed, *held, *hots, gains[0], gains[1]),
+        "s" + "v" * (len(mixed) + 2 * homes + 2),
+    )
+    outgoing = outgoing.reshape(experts_total // homes, homes * tall, slot_width)
+    arrived = exchange(outgoing, members)
+    arrived = arrived.reshape(devices // homes, local_count, homes * tall, slot_width)
     answers = []
     for expert in range(local_count):
         (held_gate,) = local_call(
@@ -540,21 +591,24 @@
             scratch=[pltpu.SemaphoreType.DMA],
         )
         (answer,) = local_call(
-            expert_kernel,
-            [((devices // fold, fold, tall, slot_width), HALF, "h")],
+            functools.partial(expert_kernel, split=paired),
+            [((fold, devices // fold, tall, slot_width), HALF, "h")],
             (
+                at,
                 arrived[:, expert].reshape(devices // fold, fold, tall, slot_width),
                 held_gate,
                 expert_up[expert],
                 expert_down[expert],
             ),
-            "vvhh",
+            "svvhh",
             scratch=[
                 pltpu.VMEM(expert_up.shape[1:], HALF),
                 pltpu.VMEM(expert_down.shape[1:], HALF),
                 pltpu.SemaphoreType.DMA((2 * fold,)),
             ],
         )
+        if not paired:
+            answer = answer.swapaxes(0, 1)
         answers.append(answer.reshape(devices, tall, slot_width))
     answered = jnp.stack(answers, axis=1).reshape(experts_total, tall, slot_width)
     returned = exchange(answered)

time: 112 us -> 107 us (0.955)
  blocking collectives: 8.89 us -> 0 us
  starting transfers between devices: 29.5 us -> 32.9 us
  waiting for transfers between devices: 44.2 us -> 41.8 us
  local copies, waits for them, and re-layouts: 1.82 us -> 3.91 us
    all_to_all x5 -> x4, waiting for transfers between devices: 27.2 us -> 17 us  [exchange(): lax.all_to_all(values, 'ep', split_axis=0, concat_axis=0, tiled=True, axi...]
    all_to_all x1 -> x0, blocking collectives: 8.89 us -> none  [exchange(): lax.all_to_all(values, 'ep', split_axis=0, concat_axis=0, tiled=True, axi...]
    ppermute x11 -> x16, waiting for transfers between devices: 17 us -> 24.9 us  [swap(): return lax.ppermute(values, 'ep', [(i, i ^ bit) for i in range(devices)])]
    ppermute x11 -> x16, starting transfers between devices: 7.94 us -> 15.5 us  [swap(): return lax.ppermute(values, 'ep', [(i, i ^ bit) for i in range(devices)])]
    all_to_all x5 -> x4, starting transfers between devices: 21.5 us -> 17.4 us  [exchange(): lax.all_to_all(values, 'ep', split_axis=0, concat_axis=0, tiled=True, axi...]
    unnamed x11 -> x31, local copies, waits for them, and re-layouts: 1.67 us -> 3.75 us
    pallas_call x13 -> x14, Pallas kernels: 21.7 us -> 22.4 us  [local_call(): pl.pallas_call(body, out_shape=[SPACES[space](shape, kind) for shape, kin...]
  transfers between devices with their start and end apart: 16 -> 20, of which waited for: 8 -> 8; matrix products, arithmetic and copies ran while one was open for 5% -> 5% of each run, Pallas kernels for 10% -> 11%
where the time goes in v3:
time: 107 us
  waiting for transfers between devices  41.8 us (39%)
  starting transfers between devices  32.9 us (31%)
  Pallas kernels  22.4 us (21%)
  other arithmetic  4.77 us (4%)
  local copies, waits for them, and re-layouts  3.91 us (4%)
    ppermute x16, waiting for transfers between devices, swap(): return lax.ppermute(values, 'ep', [(i, i ^ bit) for i in range(devices)])  24.9 us
    pallas_call x14, Pallas kernels, local_call(): pl.pallas_call(body, out_shape=[SPACES[space](shape, kind) for shape, kin...  22.4 us
    all_to_all x4, starting transfers between devices, exchange(): lax.all_to_all(values, 'ep', split_axis=0, concat_axis=0, tiled=True, axi...  17.4 us
    all_to_all x4, waiting for transfers between devices, exchange(): lax.all_to_all(values, 'ep', split_axis=0, concat_axis=0, tiled=True, axi...  17 us
    ppermute x16, starting transfers between devices, swap(): return lax.ppermute(values, 'ep', [(i, i ^ bit) for i in range(devices)])  15.5 us
    add x1, other arithmetic, on_device(): keep_old[..., None, None] * memory_state  4.6 us
    unnamed x31, local copies, waits for them, and re-layouts  3.75 us
  transfers between devices with their start and end apart: 20, of which 8 were waited for; matrix products, arithmetic and copies ran while one was open for 5% of the time, Pallas kernels for 11%

profile of v3, /device:TPU:0, one launch (start us, length us, event | category | flops | bytes accessed | tf_op | source)
XLA Modules:
  0.0 106.7 jit_solution(11163764402584585571)
XLA Ops:
  0.8 2.4 %shard_map.264 = (bf16[2,64,1024]{2,1,0:T(8,128)(2,1)S(1)}, bf16[2,64,1024]{2,1,0:T(8,128)(2,1)S(1)}, bf16[8,2048]{1,0:T(8,128)(2,1)S(1)}, bf16[8,2048]{1,0:T(8,128)(2,1)S(1)}, bf16[32,8,512]{2,1,0:T(8,128)(2,1)}) custom-call(s32[4]{0:T(128)S(1)} %pad_add_fusion.at_ref, bf16[8,2048]{1,0:T(8,128)(2,1)} %tokens_ref.1, f32[1,2048]{1,0:T(1,128)} %bitcast.46, ...), custom_call_target="tpu_custom_call" | custom-call | tf_op jit(solution)/shard_map/pallas_call | solution.py:40
  3.2 7.3 %all-to-all-start = ((bf16[32,8,512]{2,1,0:T(8,128)(2,1)}), bf16[32,8,512]{2,1,0:T(8,128)(2,1)S(1)}, u32[]{:S(2)}, u32[]{:S(2)}) async-start(bf16[32,8,512]{2,1,0:T(8,128)(2,1)} %get-tuple-element.28), calls=%async_computation | async-start | bytes 524288 | tf_op jit(solution)/shard_map/all_to_all | solution.py:26
  10.9 1.6 %collective-permute-start.5 = (bf16[1,64,1024]{2,1,0:T(8,128)(2,1)}, bf16[1,64,1024]{2,1,0:T(8,128)(2,1)S(1)}, u32[]{:S(2)}, u32[]{:S(2)}) collective-permute-start(bf16[1,64,1024]{2,1,0:T(8,128)(2,1)} %bitcast.33), channel_id=1, source_target_pairs={{0,8},{1,9},{2,10},{3,11},{4,12},{5,13},{6,14},{7,15},{8,0},{9,1},... | collective-permute-start | bytes 393224 | tf_op jit(solution)/shard_map/ppermute | solution.py:22
  13.1 1.5 %collective-permute-start.1 = (bf16[128,512]{1,0:T(8,128)(2,1)S(1)}, bf16[128,512]{1,0:T(8,128)(2,1)S(1)}, u32[]{:S(2)}, u32[]{:S(2)}) collective-permute-start(bf16[128,512]{1,0:T(8,128)(2,1)S(1)} %get-tuple-element.32), channel_id=1, source_target_pairs={{0,2},{1,3},{2,0},{3,1},{4,6},{5,7},{6,4},{7,5},{8,10},{9,11},{10,... | collective-permute-start | bytes 393224 | tf_op jit(solution)/shard_map/ppermute | solution.py:22
  16.7 3.7 %collective-permute-done.5.refs_1_ = bf16[1,64,1024]{2,1,0:T(8,128)(2,1)S(1)} collective-permute-done((bf16[1,64,1024]{2,1,0:T(8,128)(2,1)}, bf16[1,64,1024]{2,1,0:T(8,128)(2,1)S(1)}, u32[]{:S(2)}, u32[]{:S(2)}) %collective-permute-start.5) | collective-permute-done | bytes 131104 | tf_op jit(solution)/shard_map/ppermute | solution.py:22
  21.3 2.5 %collective-permute-done.2.refs_2_ = bf16[128,512]{1,0:T(8,128)(2,1)S(1)} collective-permute-done((bf16[128,512]{1,0:T(8,128)(2,1)S(1)}, bf16[128,512]{1,0:T(8,128)(2,1)S(1)}, u32[]{:S(2)}, u32[]{:S(2)}) %collective-permute-start.2) | collective-permute-done | bytes 131104 | tf_op jit(solution)/shard_map/ppermute | solution.py:22
  23.8 1.6 %shard_map.266 = bf16[256,512]{1,0:T(8,128)(2,1)} custom-call(s32[4]{0:T(128)S(1)} %pad_add_fusion.at_ref, bf16[256,512]{1,0:T(8,128)(2,1)S(1)} %bitcast.31, bf16[128,512]{1,0:T(8,128)(2,1)S(1)} %get-tuple-element.31.refs_0_, bf16[128,512]{1,0:T(8,128)(2,1)S(1)} %collective-permute-done.1.refs_1_, bf16[128,512]{1,0:T(8,128)(2,1)S(1)} %collective-permute-done.2.refs_2_, ...), custom_call_target="tpu_custom_call" | custom-call | tf_op jit(solution)/shard_map/pallas_call | solution.py:40
  25.4 3.9 %all-to-all-start.1 = ((bf16[32,8,512]{2,1,0:T(8,128)(2,1)}), bf16[32,8,512]{2,1,0:T(8,128)(2,1)S(1)}, u32[]{:S(2)}, u32[]{:S(2)}) async-start(bf16[32,8,512]{2,1,0:T(8,128)(2,1)} %bitcast.37), calls=%async_computation.1 | async-start | bytes 524288 | tf_op jit(solution)/shard_map/all_to_all | solution.py:26
  29.3 2.7 %collective-permute-start.8 = (bf16[2,64,1024]{2,1,0:T(8,128)(2,1)S(1)}, bf16[2,64,1024]{2,1,0:T(8,128)(2,1)S(1)}, u32[]{:S(2)}, u32[]{:S(2)}) collective-permute-start(bf16[2,64,1024]{2,1,0:T(8,128)(2,1)S(1)} %shard_map.270.refs_0_), channel_id=1, source_target_pairs={{0,6},{1,7},{2,4},{3,5},{4,2},{5,3},{6,0},{7,1},{8,14},{9,15},{10,... | collective-permute-start | bytes 786440 | tf_op jit(solution)/shard_map/ppermute | solution.py:22
  32.8 9.2 %collective-permute-done.8.refs_3_ = bf16[2,64,1024]{2,1,0:T(8,128)(2,1)S(1)} collective-permute-done((bf16[2,64,1024]{2,1,0:T(8,128)(2,1)S(1)}, bf16[2,64,1024]{2,1,0:T(8,128)(2,1)S(1)}, u32[]{:S(2)}, u32[]{:S(2)}) %collective-permute-start.8) | collective-permute-done | bytes 262176 | tf_op jit(solution)/shard_map/ppermute | solution.py:22
  42.1 4.8 %collective-permute-done.7.refs_2_ = bf16[2,64,1024]{2,1,0:T(8,128)(2,1)S(1)} collective-permute-done((bf16[2,64,1024]{2,1,0:T(8,128)(2,1)S(1)}, bf16[2,64,1024]{2,1,0:T(8,128)(2,1)S(1)}, u32[]{:S(2)}, u32[]{:S(2)}) %collective-permute-start.7) | collective-permute-done | bytes 262176 | tf_op jit(solution)/shard_map/ppermute | solution.py:22
  47.3 1.7 %shard_map.267 = (f32[8,8]{1,0:T(8,128)S(1)}, f32[8,8]{1,0:T(8,128)S(1)}, f32[8,8]{1,0:T(8,128)}, bf16[16,256]{1,0:T(8,128)(2,1)S(1)}, bf16[32,256]{1,0:T(8,128)...) custom-call(bf16[8,2048]{1,0:T(8,128)(2,1)S(1)} %get-tuple-element.3, ...), custom_call_target="tpu_custom_call" | custom-call | tf_op jit(solution)/shard_map/pallas_call | solution.py:40
  51.8 3.1 %shard_map.269 = (bf16[1,8,1024]{2,1,0:T(8,128)(2,1)S(1)}, f32[8,8,128]{2,1,0:T(8,128)S(1)}, f32[8,8,128]{2,1,0:T(8,128)S(1)}) custom-call(bf16[32,8,512]{2,1,0:T(8,128)(2,1)S(1)} %all-to-all-done.1.parts_ref, f32[8,8]{1,0:T(8,128)S(1)} %get-tuple-element.36.keep_ref, f32[8,8]{1,0:T(8,128)S(1)} %get-tuple-element.37.write_ref, ...), custom_call_target="tpu_custom_call" | custom-call | tf_op jit(solution)/shard_map/pallas_call | solution.py:40
  54.9 2.6 %collective-permute-start.4 = (bf16[8,1024]{1,0:T(8,128)(2,1)S(1)}, bf16[8,1024]{1,0:T(8,128)(2,1)S(1)}, u32[]{:S(2)}, u32[]{:S(2)}) collective-permute-start(bf16[8,1024]{1,0:T(8,128)(2,1)S(1)} %bitcast.35), channel_id=1, source_target_pairs={{0,16},{1,17},{2,18},{3,19},{4,20},{5,21},{6,22},{7,23},{8,24},{9,... | collective-permute-start | bytes 49160 | tf_op jit(solution)/shard_map/ppermute | solution.py:22
  60.4 2.4 %collective-permute-start.13 = (bf16[16,1024]{1,0:T(8,128)(2,1)S(1)}, bf16[16,1024]{1,0:T(8,128)(2,1)S(1)}, u32[]{:S(2)}, u32[]{:S(2)}) collective-permute-start(bf16[16,1024]{1,0:T(8,128)(2,1)S(1)} %shard_map.272.refs_0_), channel_id=1, source_target_pairs={{0,16},{1,17},{2,18},{3,19},{4,20},{5,21},{6,22},{7,23},{8,24},{9,... | collective-permute-start | bytes 98312 | tf_op jit(solution)/shard_map/ppermute | solution.py:22
  63.3 4.0 %collective-permute-done.15.refs_5_ = bf16[16,256]{1,0:T(8,128)(2,1)S(1)} collective-permute-done((bf16[16,256]{1,0:T(8,128)(2,1)S(1)}, bf16[16,256]{1,0:T(8,128)(2,1)S(1)}, u32[]{:S(2)}, u32[]{:S(2)}) %collective-permute-start.15) | collective-permute-done | bytes 8224 | tf_op jit(solution)/shard_map/ppermute | solution.py:22
  67.3 1.8 %shard_map.273 = (bf16[8,2048]{1,0:T(8,128)(2,1)S(1)}, bf16[8,2048]{1,0:T(8,128)(2,1)S(1)}, bf16[16,2,8,1024]{3,2,1,0:T(8,128)(2,1)}) custom-call(s32[4]{0:T(128)S(1)} %pad_add_fusion.at_ref, bf16[16,1024]{1,0:T(8,128)(2,1)S(1)} %shard_map.272.refs_0_, bf16[16,1024]{1,0:T(8,128)(2,1)S(1)} %collective-permute-done.13.refs_1_, ...), custom_call_target="tpu_custom_call" | custom-call | tf_op jit(solution)/shard_map/pallas_call | solution.py:40
  69.1 3.6 %all-to-all-start.2 = ((bf16[16,16,1024]{2,1,0:T(8,128)(2,1)}), bf16[16,16,1024]{2,1,0:T(8,128)(2,1)S(1)}, u32[]{:S(2)}, u32[]{:S(2)}) async-start(bf16[16,16,1024]{2,1,0:T(8,128)(2,1)} %bitcast.43), calls=%async_computation.2 | async-start | bytes 1048576 | tf_op jit(solution)/shard_map/all_to_all | solution.py:26
  72.7 1.6 %shard_map.274.gate_ref = bf16[2048,512]{1,0:T(8,128)(2,1)S(1)} custom-call(bf16[8,2048]{1,0:T(8,128)(2,1)S(1)} %get-tuple-element.45.after_ref, bf16[2048,512]{1,0:T(8,128)(2,1)} %bitcast.39), custom_call_target="tpu_custom_call" | custom-call | tf_op jit(solution)/shard_map/pallas_call | solution.py:40
  74.3 8.9 %all-to-all-done.2 = bf16[16,16,1024]{2,1,0:T(8,128)(2,1)S(1)} async-done(((bf16[16,16,1024]{2,1,0:T(8,128)(2,1)}), bf16[16,16,1024]{2,1,0:T(8,128)(2,1)S(1)}, u32[]{:S(2)}, u32[]{:S(2)}) %all-to-all-start.2) | async-done | bytes 524320 | tf_op jit(solution)/shard_map/all_to_all | solution.py:26
  83.2 4.3 %shard_map.275 = bf16[2,16,8,1024]{3,2,1,0:T(8,128)(2,1)} custom-call(s32[4]{0:T(128)S(1)} %pad_add_fusion.at_ref, bf16[16,2,8,1024]{3,2,1,0:T(8,128)(2,1)S(1)} %bitcast.30, bf16[2048,512]{1,0:T(8,128)(2,1)S(1)} %shard_map.274.gate_ref, bf16[2048,512]{1,0:T(8,128)(2,1)} %bitcast.40, bf16[512,2048]{1,0:T(8,128)(2,1)} %bitcast.41), custom_call_target="tpu_custom_call" | custom-call | tf_op jit(solution)/shard_map/pallas_call | solution.py:40
  87.5 2.6 %all-to-all-start.3 = ((bf16[32,8,1024]{2,1,0:T(8,128)(2,1)}), bf16[32,8,1024]{2,1,0:T(8,128)(2,1)S(1)}, u32[]{:S(2)}, u32[]{:S(2)}) async-start(bf16[32,8,1024]{2,1,0:T(8,128)(2,1)} %bitcast.42), calls=%async_computation.3 | async-start | bytes 1048576 | tf_op jit(solution)/shard_map/all_to_all | solution.py:26
  91.1 4.6 %multiply_add_fusion = f32[8,8,128,128]{3,2,1,0:T(8,128)} fusion(f32[8,8,128,128]{3,2,1,0:T(8,128)} %memory_ref.3, f32[8,8,128]{2,1,0:T(8,128)S(1)} %copy.31, f32[8,8,128]{2,1,0:T(8,128)S(1)} %copy.30, f32[8,8]{1,0:T(8,128)S(1)} %get-tuple-element.36.keep_ref), kind=kLoop, calls=%fused_computation | loop fusion | flops 3145728 | bytes 8454400 | tf_op jit(solution)/shard_map/add | solution.py:623
  97.7 8.1 %all-to-all-done.3 = bf16[32,8,1024]{2,1,0:T(8,128)(2,1)S(1)} async-done(((bf16[32,8,1024]{2,1,0:T(8,128)(2,1)}), bf16[32,8,1024]{2,1,0:T(8,128)(2,1)S(1)}, u32[]{:S(2)}, u32[]{:S(2)}) %all-to-all-start.3) | async-done | bytes 524320 | tf_op jit(solution)/shard_map/all_to_all | solution.py:26
  (68 shorter events, 15.3 us)
Async XLA Ops:
  3.2 20.6 %all-to-all-start = ((bf16[32,8,512]{2,1,0:T(8,128)(2,1)}), bf16[32,8,512]{2,1,0:T(8,128)(2,1)S(1)}, u32[]{:S(2)}, u32[]{:S(2)}) async-start(bf16[32,8,512]{2,1,0:T(8,128)(2,1)} %get-tuple-element.28), calls=%async_computation | async-start | bytes 524288 | tf_op jit(solution)/shard_map/all_to_all | solution.py:26
  10.5 2.0 %collective-permute-start = (bf16[2,64,1024]{2,1,0:T(8,128)(2,1)S(1)}, bf16[2,64,1024]{2,1,0:T(8,128)(2,1)S(1)}, u32[]{:S(2)}, u32[]{:S(2)}) collective-permute-start(bf16[2,64,1024]{2,1,0:T(8,128)(2,1)S(1)} %get-tuple-element.30), channel_id=1, source_target_pairs={{0,1},{1,0},{2,3},{3,2},{4,5},{5,4},{6,7},{7,6},{8,9},{9,8},{10,11... | collective-permute-start | bytes 786440 | tf_op jit(solution)/shard_map/ppermute | solution.py:22
  10.9 9.5 %collective-permute-start.5 = (bf16[1,64,1024]{2,1,0:T(8,128)(2,1)}, bf16[1,64,1024]{2,1,0:T(8,128)(2,1)S(1)}, u32[]{:S(2)}, u32[]{:S(2)}) collective-permute-start(bf16[1,64,1024]{2,1,0:T(8,128)(2,1)} %bitcast.33), channel_id=1, source_target_pairs={{0,8},{1,9},{2,10},{3,11},{4,12},{5,13},{6,14},{7,15},{8,0},{9,1},... | collective-permute-start | bytes 393224 | tf_op jit(solution)/shard_map/ppermute | solution.py:22
  13.1 8.2 %collective-permute-start.1 = (bf16[128,512]{1,0:T(8,128)(2,1)S(1)}, bf16[128,512]{1,0:T(8,128)(2,1)S(1)}, u32[]{:S(2)}, u32[]{:S(2)}) collective-permute-start(bf16[128,512]{1,0:T(8,128)(2,1)S(1)} %get-tuple-element.32), channel_id=1, source_target_pairs={{0,2},{1,3},{2,0},{3,1},{4,6},{5,7},{6,4},{7,5},{8,10},{9,11},{10,... | collective-permute-start | bytes 393224 | tf_op jit(solution)/shard_map/ppermute | solution.py:22
  14.6 9.2 %collective-permute-start.2 = (bf16[128,512]{1,0:T(8,128)(2,1)S(1)}, bf16[128,512]{1,0:T(8,128)(2,1)S(1)}, u32[]{:S(2)}, u32[]{:S(2)}) collective-permute-start(bf16[128,512]{1,0:T(8,128)(2,1)S(1)} %get-tuple-element.33), channel_id=1, source_target_pairs={{0,4},{1,5},{2,6},{3,7},{4,0},{5,1},{6,2},{7,3},{8,12},{9,13},{10,... | collective-permute-start | bytes 393224 | tf_op jit(solution)/shard_map/ppermute | solution.py:22
  16.1 7.7 %collective-permute-start.3 = (bf16[128,512]{1,0:T(8,128)(2,1)S(1)}, bf16[128,512]{1,0:T(8,128)(2,1)S(1)}, u32[]{:S(2)}, u32[]{:S(2)}) collective-permute-start(bf16[128,512]{1,0:T(8,128)(2,1)S(1)} %get-tuple-element.34), channel_id=1, source_target_pairs={{0,6},{1,7},{2,4},{3,5},{4,2},{5,3},{6,0},{7,1},{8,14},{9,15},{10,... | collective-permute-start | bytes 393224 | tf_op jit(solution)/shard_map/ppermute | solution.py:22
  25.4 26.3 %all-to-all-start.1 = ((bf16[32,8,512]{2,1,0:T(8,128)(2,1)}), bf16[32,8,512]{2,1,0:T(8,128)(2,1)S(1)}, u32[]{:S(2)}, u32[]{:S(2)}) async-start(bf16[32,8,512]{2,1,0:T(8,128)(2,1)} %bitcast.37), calls=%async_computation.1 | async-start | bytes 524288 | tf_op jit(solution)/shard_map/all_to_all | solution.py:26
  29.3 12.8 %collective-permute-start.8 = (bf16[2,64,1024]{2,1,0:T(8,128)(2,1)S(1)}, bf16[2,64,1024]{2,1,0:T(8,128)(2,1)S(1)}, u32[]{:S(2)}, u32[]{:S(2)}) collective-permute-start(bf16[2,64,1024]{2,1,0:T(8,128)(2,1)S(1)} %shard_map.270.refs_0_), channel_id=1, source_target_pairs={{0,6},{1,7},{2,4},{3,5},{4,2},{5,3},{6,0},{7,1},{8,14},{9,15},{10,... | collective-permute-start | bytes 786440 | tf_op jit(solution)/shard_map/ppermute | solution.py:22
  32.0 14.8 %collective-permute-start.7 = (bf16[2,64,1024]{2,1,0:T(8,128)(2,1)S(1)}, bf16[2,64,1024]{2,1,0:T(8,128)(2,1)S(1)}, u32[]{:S(2)}, u32[]{:S(2)}) collective-permute-start(bf16[2,64,1024]{2,1,0:T(8,128)(2,1)S(1)} %shard_map.270.refs_0_), channel_id=1, source_target_pairs={{0,4},{1,5},{2,6},{3,7},{4,0},{5,1},{6,2},{7,3},{8,12},{9,13},{10,... | collective-permute-start | bytes 786440 | tf_op jit(solution)/shard_map/ppermute | solution.py:22
  32.6 14.3 %collective-permute-start.6 = (bf16[2,64,1024]{2,1,0:T(8,128)(2,1)S(1)}, bf16[2,64,1024]{2,1,0:T(8,128)(2,1)S(1)}, u32[]{:S(2)}, u32[]{:S(2)}) collective-permute-start(bf16[2,64,1024]{2,1,0:T(8,128)(2,1)S(1)} %shard_map.270.refs_0_), channel_id=1, source_target_pairs={{0,2},{1,3},{2,0},{3,1},{4,6},{5,7},{6,4},{7,5},{8,10},{9,11},{10,... | collective-permute-start | bytes 786440 | tf_op jit(solution)/shard_map/ppermute | solution.py:22
  32.8 24.6 %collective-permute-start.9 = (bf16[2,64,1024]{2,1,0:T(8,128)(2,1)S(1)}, bf16[2,64,1024]{2,1,0:T(8,128)(2,1)S(1)}, u32[]{:S(2)}, u32[]{:S(2)}) collective-permute-start(bf16[2,64,1024]{2,1,0:T(8,128)(2,1)S(1)} %shard_map.270.refs_0_), channel_id=1, source_target_pairs={{0,1},{1,0},{2,3},{3,2},{4,5},{5,4},{6,7},{7,6},{8,9},{9,8},{10,11... | collective-permute-start | bytes 786440 | tf_op jit(solution)/shard_map/ppermute | solution.py:22
  42.0 15.8 %collective-permute-start.12 = (bf16[2,64,1024]{2,1,0:T(8,128)(2,1)S(1)}, bf16[2,64,1024]{2,1,0:T(8,128)(2,1)S(1)}, u32[]{:S(2)}, u32[]{:S(2)}) collective-permute-start(bf16[2,64,1024]{2,1,0:T(8,128)(2,1)S(1)} %collective-permute-done.8.refs_3_), channel_id=1, source_target_pairs={{0,1},{1,0},{2,3},{3,2},{4,5},{5,4},{6,7},{7,6},{8,9},{9,8},{10,11... | collective-permute-start | bytes 786440 | tf_op jit(solution)/shard_map/ppermute | solution.py:22
  46.8 11.0 %collective-permute-start.11 = (bf16[2,64,1024]{2,1,0:T(8,128)(2,1)S(1)}, bf16[2,64,1024]{2,1,0:T(8,128)(2,1)}, u32[]{:S(2)}, u32[]{:S(2)}) collective-permute-start(bf16[2,64,1024]{2,1,0:T(8,128)(2,1)S(1)} %collective-permute-done.7.refs_2_), channel_id=1, source_target_pairs={{0,1},{1,0},{2,3},{3,2},{4,5},{5,4},{6,7},{7,6},{8,9},{9,8},{10,11... | collective-permute-start | bytes 786440 | tf_op jit(solution)/shard_map/ppermute | solution.py:22
  46.8 11.0 %collective-permute-start.10 = (bf16[2,64,1024]{2,1,0:T(8,128)(2,1)S(1)}, bf16[2,64,1024]{2,1,0:T(8,128)(2,1)}, u32[]{:S(2)}, u32[]{:S(2)}) collective-permute-start(bf16[2,64,1024]{2,1,0:T(8,128)(2,1)S(1)} %collective-permute-done.6.refs_1_), channel_id=1, source_target_pairs={{0,1},{1,0},{2,3},{3,2},{4,5},{5,4},{6,7},{7,6},{8,9},{9,8},{10,11... | collective-permute-start | bytes 786440 | tf_op jit(solution)/shard_map/ppermute | solution.py:22
  54.8 12.5 %copy-start.11 = (f32[1,2048]{1,0:T(1,128)S(1)}, f32[1,2048]{1,0:T(1,128)}, u32[]{:S(2)}) copy-start(f32[1,2048]{1,0:T(1,128)} %copy-done.10) | copy-start | bytes 24580
  54.8 12.5 %copy-start.13 = (f32[1,2048]{1,0:T(1,128)S(1)}, f32[1,2048]{1,0:T(1,128)}, u32[]{:S(2)}) copy-start(f32[1,2048]{1,0:T(1,128)} %copy-done.12) | copy-start | bytes 24580
  54.9 4.9 %collective-permute-start.4 = (bf16[8,1024]{1,0:T(8,128)(2,1)S(1)}, bf16[8,1024]{1,0:T(8,128)(2,1)S(1)}, u32[]{:S(2)}, u32[]{:S(2)}) collective-permute-start(bf16[8,1024]{1,0:T(8,128)(2,1)S(1)} %bitcast.35), channel_id=1, source_target_pairs={{0,16},{1,17},{2,18},{3,19},{4,20},{5,21},{6,22},{7,23},{8,24},{9,... | collective-permute-start | bytes 49160 | tf_op jit(solution)/shard_map/ppermute | solution.py:22
  57.4 9.9 %collective-permute-start.14 = (bf16[8,2048]{1,0:T(8,128)(2,1)S(1)}, bf16[8,2048]{1,0:T(8,128)(2,1)S(1)}, u32[]{:S(2)}, u32[]{:S(2)}) collective-permute-start(bf16[8,2048]{1,0:T(8,128)(2,1)S(1)} %get-tuple-element.40.refs_2_), channel_id=1, source_target_pairs={{0,16},{1,17},{2,18},{3,19},{4,20},{5,21},{6,22},{7,23},{8,24},{9,... | collective-permute-start | bytes 98312 | tf_op jit(solution)/shard_map/ppermute | solution.py:22
  60.4 6.9 %collective-permute-start.13 = (bf16[16,1024]{1,0:T(8,128)(2,1)S(1)}, bf16[16,1024]{1,0:T(8,128)(2,1)S(1)}, u32[]{:S(2)}, u32[]{:S(2)}) collective-permute-start(bf16[16,1024]{1,0:T(8,128)(2,1)S(1)} %shard_map.272.refs_0_), channel_id=1, source_target_pairs={{0,16},{1,17},{2,18},{3,19},{4,20},{5,21},{6,22},{7,23},{8,24},{9,... | collective-permute-start | bytes 98312 | tf_op jit(solution)/shard_map/ppermute | solution.py:22
  62.7 4.5 %collective-permute-start.15 = (bf16[16,256]{1,0:T(8,128)(2,1)S(1)}, bf16[16,256]{1,0:T(8,128)(2,1)S(1)}, u32[]{:S(2)}, u32[]{:S(2)}) collective-permute-start(bf16[16,256]{1,0:T(8,128)(2,1)S(1)} %copy-done.9), channel_id=1, source_target_pairs={{0,16},{1,17},{2,18},{3,19},{4,20},{5,21},{6,22},{7,23},{8,24},{9,... | collective-permute-start | bytes 24584 | tf_op jit(solution)/shard_map/ppermute | solution.py:22
  69.1 14.1 %all-to-all-start.2 = ((bf16[16,16,1024]{2,1,0:T(8,128)(2,1)}), bf16[16,16,1024]{2,1,0:T(8,128)(2,1)S(1)}, u32[]{:S(2)}, u32[]{:S(2)}) async-start(bf16[16,16,1024]{2,1,0:T(8,128)(2,1)} %bitcast.43), calls=%async_computation.2 | async-start | bytes 1048576 | tf_op jit(solution)/shard_map/all_to_all | solution.py:26
  87.5 18.2 %all-to-all-start.3 = ((bf16[32,8,1024]{2,1,0:T(8,128)(2,1)}), bf16[32,8,1024]{2,1,0:T(8,128)(2,1)S(1)}, u32[]{:S(2)}, u32[]{:S(2)}) async-start(bf16[32,8,1024]{2,1,0:T(8,128)(2,1)} %bitcast.42), calls=%async_computation.3 | async-start | bytes 1048576 | tf_op jit(solution)/shard_map/all_to_all | solution.py:26
  95.7 10.1 %copy-start.5 = (bf16[32,256]{1,0:T(8,128)(2,1)S(1)}, bf16[32,256]{1,0:T(8,128)(2,1)}, u32[]{:S(2)}) copy-start(bf16[32,256]{1,0:T(8,128)(2,1)} %copy-done.4) | copy-start | bytes 49156
  95.7 10.1 %copy-start.7 = (f32[1,2048]{1,0:T(1,128)S(1)}, f32[1,2048]{1,0:T(1,128)}, u32[]{:S(2)}) copy-start(f32[1,2048]{1,0:T(1,128)} %copy-done.6) | copy-start | bytes 24580
  (11 other events, 36.4 us)

commit v4 on v3

--- a/solution.py
+++ b/solution.py
@@ -58,7 +58,8 @@
         copy.wait()
 
 
-def start_kernel(at_ref, tokens_ref, gain_ref, *refs, planes):
+def start_kernel(tokens_ref, gain_ref, *refs, planes):
+    core = lax.axis_index("ep") % 2
     weights, outs, (scale_ref, done) = refs[:4], refs[4:-2], refs[-2:]
     kept_ref, sent_ref, held_ref, normed_ref, pieces_ref = outs
     loads = [
@@ -74,8 +75,8 @@
         for number, (source, target) in enumerate(pairs):
             pltpu.make_async_copy(source, target, done.at[2 + number]).start()
 
-    pl.when(at_ref[0] == 0)(lambda: place(weights[:2], weights[2:]))
-    pl.when(at_ref[0] != 0)(lambda: place(weights[2:], weights[:2]))
+    pl.when(core == 0)(lambda: place(weights[:2], weights[2:]))
+    pl.when(core != 0)(lambda: place(weights[2:], weights[:2]))
     for load in loads:
         load.wait()
     normed = rms_scale(held_ref[...].astype(WIDE), scale_ref[...]).astype(HALF)
@@ -170,19 +171,9 @@
     load.wait()
 
 
-def read_kernel(
-    parts_ref,
-    keep_ref,
-    write_ref,
-    normalizer_ref,
-    early_ref,
-    memory_ref,
-    gated_ref,
-    keys_ref,
-    values_ref,
-    late_ref,
-    done,
-):
+def read_kernel(*refs):
+    parts_ref, keep_ref, write_ref, normalizer_ref, early_ref, memory_ref = refs[:6]
+    side, (gated_ref, keys_ref, values_ref, late_ref, done) = refs[6:-5], refs[-5:]
     early = early_ref.shape[0]
     loads = [
         pltpu.make_async_copy(memory_ref.at[early + at], late_ref.at[at], done.at[at])
@@ -190,6 +181,11 @@
     ]
     for load in loads:
         load.start()
+    start = memory_ref.shape[1] * memory_ref.shape[3]
+    for ref in side:
+        for row in range(0, ref.shape[0], gated_ref.shape[1]):
+            gated_ref[0, :, start : start + ref.shape[1]] = ref[row : row + gated_ref.shape[1]]
+            start += ref.shape[1]
     copies, sequences, _ = gated_ref.shape
     heads, width = memory_ref.shape[1], memory_ref.shape[3]
     planes = parts_ref.shape[0] // heads
@@ -273,7 +269,8 @@
 
 
 def mix_kernel(*refs):
-    rows = jnp.concatenate([ref[...] for ref in refs[:-2]], axis=0)
+    depth = refs[-2].shape[1]
+    rows = jnp.concatenate([ref[:, :depth] for ref in refs[:-2]], axis=0)
     refs[-1][...] = lax.dot_general(
         rows, refs[-2][...], (((1,), (1,)), ((), ())), preferred_element_type=WIDE
     ).astype(HALF)
@@ -281,32 +278,54 @@
 
 def send_kernel(at_ref, *refs, pieces):
     mixed, refs = [piece[...].astype(WIDE) for piece in refs[:pieces]], refs[pieces:]
-    homes = (len(refs) - 5) // 2
-    tokens, hots, refs = refs[:homes], refs[homes : 2 * homes], refs[2 * homes :]
+    tokens, hots = [refs[0][...]], [refs[1]]
+    side, refs = refs[2:-5], refs[-5:]
+    homes = 1 + len(side)
     postmix_ref, prefeed_ref, after_ref, input_ref, out_ref = refs
-    sequences = after_ref.shape[0]
+    sequences, model_width = after_ref.shape
+    slots = hots[0].shape[1]
     if homes == 2:
+        start = side[0].shape[1] - hots[0].shape[0] // sequences * slots
+        tokens.append(side[0][:, start - model_width : start])
+        hots.append(side[0].at[:, pl.ds(start, side[0].shape[1] - start)])
         ours, theirs = mixed
         theirs = jnp.concatenate([theirs[sequences:], theirs[:sequences]], axis=0)
         first = at_ref[3] == 0
         mixed = [jnp.where(first, ours, theirs), jnp.where(first, theirs, ours)]
     mixed = jnp.concatenate(mixed, axis=1)
-    residual = jnp.concatenate([ref[...].astype(WIDE) for ref in tokens], axis=0)
+    residual = jnp.concatenate([rows.astype(WIDE) for rows in tokens], axis=0)
     after = (residual + rms_scale(mixed, postmix_ref[...])).astype(HALF)
     after_ref[...] = after[:sequences]
     given = rms_scale(after.astype(WIDE), prefeed_ref[...])
     input_ref[...] = given[:sequences].astype(HALF)
     blocks, _, tall, width = out_ref.shape
     dims = (((0,), (0,)), ((), ()))
+    start = at_ref[3] * (blocks * tall) if homes == 2 else 0
+    step = out_ref.shape[3]
+    folded, lanes = [], []
     for home, hot in enumerate(hots):
         mine = given[home * sequences : (home + 1) * sequences]
-        folded = jnp.concatenate(
-            [mine[:, at : at + width] for at in range(0, given.shape[1], width)], axis=0
-        ).astype(HALF)
-        start = at_ref[3] * (blocks * tall) if homes == 2 else 0
-        lanes = hot[:, pl.ds(pl.multiple_of(start, blocks * tall), blocks * tall)]
-        rows = lax.dot_general(lanes, folded, dims, preferred_element_type=WIDE)
-        out_ref[:, home] = rows.astype(HALF).reshape(blocks, tall, width)
+        folded.append(
+            jnp.concatenate([mine[:, at : at + step] for at in range(0, model_width, step)], axis=0)
+        )
+        lanes.append(
+            jnp.concatenate(
+                [
+                    hot[:, pl.ds(pl.multiple_of(start + at, blocks * tall), blocks * tall)]
+                    for at in range(0, hot.shape[1], slots)
+                ],
+                axis=0,
+            ).astype(WIDE)
+        )
+    for half in range(homes):
+        rows, picks = folded[half], lanes[half]
+        if homes == 2:
+            rows = jnp.where(first, rows, folded[1 - half])
+            picks = jnp.where(first, picks, lanes[1 - half])
+        rows = lax.dot_general(
+            picks.astype(HALF), rows.astype(HALF), dims, preferred_element_type=WIDE
+        )
+        out_ref[:, half] = rows.astype(HALF).reshape(blocks, tall, width)
 
 
 def turned(values, by):
@@ -320,7 +339,7 @@
     load.wait()
 
 
-def expert_kernel(at_ref, came_ref, gate_ref, up_ref, down_ref, out_ref, held_up, held_down, done, *, split
+def expert_kernel(came_ref, gate_ref, up_ref, down_ref, out_ref, held_up, held_down, done
 ):
     groups, fold, tall, width = came_ref.shape
     capacity = tall // fold
@@ -361,7 +380,7 @@
         for part in range(fold):
             piece = turned(answers[part], (part - at) * capacity)
             packed = piece if part == 0 else jnp.where(area == part, piece, packed)
-        out_ref[at ^ at_ref[3] if split else at] = packed.astype(HALF)
+        out_ref[at] = packed.astype(HALF)
 
 
 def shared_kernel(input_ref, gate_ref, up_ref, down_ref, out_ref):
@@ -449,8 +468,8 @@
             ((sequences, model_width), HALF, "v"),
             ((devices, sequences, piece_width), HALF, "h"),
         ],
-        (at, tokens, premix_gain[None], query_weight, key_weight, value_weight, outgate_weight),
-        "shhhhhh",
+        (tokens, premix_gain[None], query_weight, key_weight, value_weight, outgate_weight),
+        "hhhhhh",
         scratch=[pltpu.VMEM((1, model_width), WIDE), pltpu.SemaphoreType.DMA((6,))],
     )
     came = swap(sent, CORE)
@@ -521,21 +540,23 @@
         "hh",
         scratch=[pltpu.SemaphoreType.DMA],
     )
+    paired = groups == 2 and fold == 2
+    side = (held_tokens, hot) if paired else ()
+    payload = heads * width + (model_width + fold * slot_count if paired else 0)
     gated, keys, values = local_call(
         read_kernel,
         [
-            ((copies, sequences, heads * width), HALF, "v"),
+            ((copies, sequences, payload), HALF, "v"),
             ((heads, sequences, width), WIDE, "v"),
             ((heads, sequences, width), WIDE, "v"),
         ],
-        (parts, keep_old, write_new, held_normalizer, early_memory, memory_state),
-        "vvvvvh",
+        (parts, keep_old, write_new, held_normalizer, early_memory, memory_state, *side),
+        "vvvvvh" + "v" * len(side),
         scratch=[
             pltpu.VMEM((sequences - early, *memory_state.shape[1:]), WIDE),
             pltpu.SemaphoreType.DMA((sequences - early,)),
         ],
     )
-    paired = groups == 2 and fold == 2
     if groups == 2:
         gated_rows = [gated[0], swap(gated[0], 2 * heads)]
         (own_mixed,) = local_call(
@@ -562,12 +583,11 @@
         mixed = exchange(mixed.reshape(groups, sequences, 2 * piece_width), lines)
         mixed = [mixed[number] for number in range(groups)]
     homes = 2 if paired else 1
-    held, hots, members = [held_tokens], [hot], None
+    members = None
     if paired:
-        held.append(swap(held_tokens, 2 * heads))
-        hots.append(swap(hot, 2 * heads))
         half = devices // 2
         members = [list(range(half)), list(range(half, devices))]
+    side = gated_rows[1:] if paired else []
     after_mix, expert_input, outgoing = local_call(
         functools.partial(send_kernel, pieces=len(mixed)),
         [
@@ -575,8 +595,8 @@
             ((sequences, model_width), HALF, "v"),
             ((experts_total // homes, homes, tall, slot_width), HALF, "h"),
         ],
-        (at, *mixed, *held, *hots, gains[0], gains[1]),
-        "s" + "v" * (len(mixed) + 2 * homes + 2),
+        (at, *mixed, held_tokens, hot, *side, gains[0], gains[1]),
+        "s" + "v" * (len(mixed) + len(side) + 4),
     )
     outgoing = outgoing.reshape(experts_total // homes, homes * tall, slot_width)
     arrived = exchange(outgoing, members)
@@ -591,16 +611,15 @@
             scratch=[pltpu.SemaphoreType.DMA],
         )
         (answer,) = local_call(
-            functools.partial(expert_kernel, split=paired),
+            expert_kernel,
             [((fold, devices // fold, tall, slot_width), HALF, "h")],
             (
-                at,
                 arrived[:, expert].reshape(devices // fold, fold, tall, slot_width),
                 held_gate,
                 expert_up[expert],
                 expert_down[expert],
             ),
-            "svvhh",
+            "vvhh",
             scratch=[
                 pltpu.VMEM(expert_up.shape[1:], HALF),
                 pltpu.VMEM(expert_down.shape[1:], HALF),

time: 107 us -> 105 us (0.981)
  starting transfers between devices: 32.9 us -> 30.6 us
  waiting for transfers between devices: 41.8 us -> 44 us
  Pallas kernels: 22.4 us -> 21.2 us
    ppermute x16 -> x14, starting transfers between devices: 15.5 us -> 13 us  [swap(): return lax.ppermute(values, 'ep', [(i, i ^ bit) for i in range(devices)])]
    ppermute x16 -> x14, waiting for transfers between devices: 24.9 us -> 27 us  [swap(): return lax.ppermute(values, 'ep', [(i, i ^ bit) for i in range(devices)])]
    pallas_call x14, Pallas kernels: 22.4 us -> 21.2 us  [local_call(): pl.pallas_call(body, out_shape=[SPACES[space](shape, kind) for shape, kin...]
  transfers between devices with their start and end apart: 20 -> 18, of which waited for: 8 -> 9; matrix products, arithmetic and copies ran while one was open for 5% -> 5% of each run, Pallas kernels for 11% -> 12%
where the time goes in v4:
time: 105 us
  waiting for transfers between devices  44 us (42%)
  starting transfers between devices  30.6 us (29%)
  Pallas kernels  21.2 us (20%)
  other arithmetic  4.77 us (5%)
  local copies, waits for them, and re-layouts  3.3 us (3%)
    ppermute x14, waiting for transfers between devices, swap(): return lax.ppermute(values, 'ep', [(i, i ^ bit) for i in range(devices)])  27 us
    pallas_call x14, Pallas kernels, local_call(): pl.pallas_call(body, out_shape=[SPACES[space](shape, kind) for shape, kin...  21.2 us
    all_to_all x4, starting transfers between devices, exchange(): lax.all_to_all(values, 'ep', split_axis=0, concat_axis=0, tiled=True, axi...  17.6 us
    all_to_all x4, waiting for transfers between devices, exchange(): lax.all_to_all(values, 'ep', split_axis=0, concat_axis=0, tiled=True, axi...  17 us
    ppermute x14, starting transfers between devices, swap(): return lax.ppermute(values, 'ep', [(i, i ^ bit) for i in range(devices)])  13 us
    add x1, other arithmetic, on_device(): keep_old[..., None, None] * memory_state  4.6 us
    unnamed x31, local copies, waits for them, and re-layouts  3.15 us
  transfers between devices with their start and end apart: 18, of which 9 were waited for; matrix products, arithmetic and copies ran while one was open for 5% of the time, Pallas kernels for 12%

profile of v4, /device:TPU:0, one launch (start us, length us, event | category | flops | bytes accessed | tf_op | source)
XLA Modules:
  0.0 104.8 jit_solution(5363083795950632548)
XLA Ops:
  0.6 1.9 %shard_map.264 = (bf16[2,64,1024]{2,1,0:T(8,128)(2,1)S(1)}, bf16[2,64,1024]{2,1,0:T(8,128)(2,1)S(1)}, bf16[8,2048]{1,0:T(8,128)(2,1)S(1)}, bf16[8,2048]{1,0:T(8,128)(2,1)S(1)}, bf16[32,8,512]{2,1,0:T(8,128)(2,1)}) custom-call(bf16[8,2048]{1,0:T(8,128)(2,1)} %tokens_ref.1, f32[1,2048]{1,0:T(1,128)} %bitcast.46, bf16[64,1024]{1,0:T(8,128)(2,1)} %refs_0_.1, ...), custom_call_target="tpu_custom_call" | custom-call | tf_op jit(solution)/shard_map/pallas_call | solution.py:40
  2.5 7.3 %all-to-all-start = ((bf16[32,8,512]{2,1,0:T(8,128)(2,1)}), bf16[32,8,512]{2,1,0:T(8,128)(2,1)S(1)}, u32[]{:S(2)}, u32[]{:S(2)}) async-start(bf16[32,8,512]{2,1,0:T(8,128)(2,1)} %get-tuple-element.28), calls=%async_computation | async-start | bytes 524288 | tf_op jit(solution)/shard_map/all_to_all | solution.py:26
  12.1 1.8 %collective-permute-start.1 = (bf16[128,512]{1,0:T(8,128)(2,1)S(1)}, bf16[128,512]{1,0:T(8,128)(2,1)S(1)}, u32[]{:S(2)}, u32[]{:S(2)}) collective-permute-start(bf16[128,512]{1,0:T(8,128)(2,1)S(1)} %get-tuple-element.32), channel_id=1, source_target_pairs={{0,2},{1,3},{2,0},{3,1},{4,6},{5,7},{6,4},{7,5},{8,10},{9,11},{10,... | collective-permute-start | bytes 393224 | tf_op jit(solution)/shard_map/ppermute | solution.py:22
  15.6 1.8 %collective-permute-start.5 = (bf16[1,64,1024]{2,1,0:T(8,128)(2,1)}, bf16[1,64,1024]{2,1,0:T(8,128)(2,1)S(1)}, u32[]{:S(2)}, u32[]{:S(2)}) collective-permute-start(bf16[1,64,1024]{2,1,0:T(8,128)(2,1)} %bitcast.33), channel_id=1, source_target_pairs={{0,8},{1,9},{2,10},{3,11},{4,12},{5,13},{6,14},{7,15},{8,0},{9,1},... | collective-permute-start | bytes 393224 | tf_op jit(solution)/shard_map/ppermute | solution.py:22
  17.4 2.1 %collective-permute-done.1.refs_1_ = bf16[128,512]{1,0:T(8,128)(2,1)S(1)} collective-permute-done((bf16[128,512]{1,0:T(8,128)(2,1)S(1)}, bf16[128,512]{1,0:T(8,128)(2,1)S(1)}, u32[]{:S(2)}, u32[]{:S(2)}) %collective-permute-start.1) | collective-permute-done | bytes 131104 | tf_op jit(solution)/shard_map/ppermute | solution.py:22
  19.5 3.4 %collective-permute-done.2.refs_2_ = bf16[128,512]{1,0:T(8,128)(2,1)S(1)} collective-permute-done((bf16[128,512]{1,0:T(8,128)(2,1)S(1)}, bf16[128,512]{1,0:T(8,128)(2,1)S(1)}, u32[]{:S(2)}, u32[]{:S(2)}) %collective-permute-start.2) | collective-permute-done | bytes 131104 | tf_op jit(solution)/shard_map/ppermute | solution.py:22
  23.0 1.6 %shard_map.266 = bf16[256,512]{1,0:T(8,128)(2,1)} custom-call(s32[4]{0:T(128)S(1)} %pad_add_fusion.at_ref, bf16[256,512]{1,0:T(8,128)(2,1)S(1)} %bitcast.31, bf16[128,512]{1,0:T(8,128)(2,1)S(1)} %get-tuple-element.31.refs_0_, bf16[128,512]{1,0:T(8,128)(2,1)S(1)} %collective-permute-done.1.refs_1_, bf16[128,512]{1,0:T(8,128)(2,1)S(1)} %collective-permute-done.2.refs_2_, ...), custom_call_target="tpu_custom_call" | custom-call | tf_op jit(solution)/shard_map/pallas_call | solution.py:40
  24.5 4.1 %all-to-all-start.1 = ((bf16[32,8,512]{2,1,0:T(8,128)(2,1)}), bf16[32,8,512]{2,1,0:T(8,128)(2,1)S(1)}, u32[]{:S(2)}, u32[]{:S(2)}) async-start(bf16[32,8,512]{2,1,0:T(8,128)(2,1)} %bitcast.37), calls=%async_computation.1 | async-start | bytes 524288 | tf_op jit(solution)/shard_map/all_to_all | solution.py:26
  29.6 2.7 %collective-permute-start.8 = (bf16[2,64,1024]{2,1,0:T(8,128)(2,1)S(1)}, bf16[2,64,1024]{2,1,0:T(8,128)(2,1)S(1)}, u32[]{:S(2)}, u32[]{:S(2)}) collective-permute-start(bf16[2,64,1024]{2,1,0:T(8,128)(2,1)S(1)} %shard_map.270.refs_0_), channel_id=1, source_target_pairs={{0,6},{1,7},{2,4},{3,5},{4,2},{5,3},{6,0},{7,1},{8,14},{9,15},{10,... | collective-permute-start | bytes 786440 | tf_op jit(solution)/shard_map/ppermute | solution.py:22
  33.1 8.3 %collective-permute-done.8.refs_3_ = bf16[2,64,1024]{2,1,0:T(8,128)(2,1)S(1)} collective-permute-done((bf16[2,64,1024]{2,1,0:T(8,128)(2,1)S(1)}, bf16[2,64,1024]{2,1,0:T(8,128)(2,1)S(1)}, u32[]{:S(2)}, u32[]{:S(2)}) %collective-permute-start.8) | collective-permute-done | bytes 262176 | tf_op jit(solution)/shard_map/ppermute | solution.py:22
  41.5 5.1 %collective-permute-done.7.refs_2_ = bf16[2,64,1024]{2,1,0:T(8,128)(2,1)S(1)} collective-permute-done((bf16[2,64,1024]{2,1,0:T(8,128)(2,1)S(1)}, bf16[2,64,1024]{2,1,0:T(8,128)(2,1)S(1)}, u32[]{:S(2)}, u32[]{:S(2)}) %collective-permute-start.7) | collective-permute-done | bytes 262176 | tf_op jit(solution)/shard_map/ppermute | solution.py:22
  47.1 1.7 %shard_map.267 = (f32[8,8]{1,0:T(8,128)S(1)}, f32[8,8]{1,0:T(8,128)S(1)}, f32[8,8]{1,0:T(8,128)}, bf16[16,256]{1,0:T(8,128)(2,1)S(1)}, bf16[32,256]{1,0:T(8,128)...) custom-call(bf16[8,2048]{1,0:T(8,128)(2,1)S(1)} %get-tuple-element.3, ...), custom_call_target="tpu_custom_call" | custom-call | tf_op jit(solution)/shard_map/pallas_call | solution.py:40
  50.9 3.1 %shard_map.269 = (bf16[1,8,3584]{2,1,0:T(8,128)(2,1)S(1)}, f32[8,8,128]{2,1,0:T(8,128)S(1)}, f32[8,8,128]{2,1,0:T(8,128)S(1)}) custom-call(bf16[32,8,512]{2,1,0:T(8,128)(2,1)S(1)} %all-to-all-done.1.refs_0_, f32[8,8]{1,0:T(8,128)S(1)} %get-tuple-element.36.refs_1_, f32[8,8]{1,0:T(8,128)S(1)} %get-tuple-element.37.refs_2_, ...), custom_call_target="tpu_custom_call" | custom-call | tf_op jit(solution)/shard_map/pallas_call | solution.py:40
  54.0 2.2 %collective-permute-start.4 = (bf16[8,3584]{1,0:T(8,128)(2,1)S(1)}, bf16[8,3584]{1,0:T(8,128)(2,1)S(1)}, u32[]{:S(2)}, u32[]{:S(2)}) collective-permute-start(bf16[8,3584]{1,0:T(8,128)(2,1)S(1)} %bitcast.35), channel_id=1, source_target_pairs={{0,16},{1,17},{2,18},{3,19},{4,20},{5,21},{6,22},{7,23},{8,24},{9,... | collective-permute-start | bytes 172040 | tf_op jit(solution)/shard_map/ppermute | solution.py:22
  57.5 2.7 %collective-permute-done.4.refs_1_.refs_4_ = bf16[8,3584]{1,0:T(8,128)(2,1)S(1)} collective-permute-done((bf16[8,3584]{1,0:T(8,128)(2,1)S(1)}, bf16[8,3584]{1,0:T(8,128)(2,1)S(1)}, u32[]{:S(2)}, u32[]{:S(2)}) %collective-permute-start.4) | collective-permute-done | bytes 57376 | tf_op jit(solution)/shard_map/ppermute | solution.py:22
  62.0 4.0 %collective-permute-done.13.refs_1_ = bf16[16,1024]{1,0:T(8,128)(2,1)S(1)} collective-permute-done((bf16[16,1024]{1,0:T(8,128)(2,1)S(1)}, bf16[16,1024]{1,0:T(8,128)(2,1)S(1)}, u32[]{:S(2)}, u32[]{:S(2)}) %collective-permute-start.13) | collective-permute-done | bytes 32800 | tf_op jit(solution)/shard_map/ppermute | solution.py:22
  66.0 1.8 %shard_map.273 = (bf16[8,2048]{1,0:T(8,128)(2,1)S(1)}, bf16[8,2048]{1,0:T(8,128)(2,1)S(1)}, bf16[16,2,8,1024]{3,2,1,0:T(8,128)(2,1)}) custom-call(s32[4]{0:T(128)S(1)} %copy-done.7, bf16[16,1024]{1,0:T(8,128)(2,1)S(1)} %shard_map.272.refs_0_, bf16[16,1024]{1,0:T(8,128)(2,1)S(1)} %collective-permute-done.13.refs_1_, ...), custom_call_target="tpu_custom_call" | custom-call | tf_op jit(solution)/shard_map/pallas_call | solution.py:40
  67.8 3.6 %all-to-all-start.2 = ((bf16[16,16,1024]{2,1,0:T(8,128)(2,1)}), bf16[16,16,1024]{2,1,0:T(8,128)(2,1)S(1)}, u32[]{:S(2)}, u32[]{:S(2)}) async-start(bf16[16,16,1024]{2,1,0:T(8,128)(2,1)} %bitcast.43), calls=%async_computation.2 | async-start | bytes 1048576 | tf_op jit(solution)/shard_map/all_to_all | solution.py:26
  71.4 1.6 %shard_map.274.gate_ref = bf16[2048,512]{1,0:T(8,128)(2,1)S(1)} custom-call(bf16[8,2048]{1,0:T(8,128)(2,1)S(1)} %get-tuple-element.45.after_ref, bf16[2048,512]{1,0:T(8,128)(2,1)} %bitcast.42), custom_call_target="tpu_custom_call" | custom-call | tf_op jit(solution)/shard_map/pallas_call | solution.py:40
  73.0 8.9 %all-to-all-done.2 = bf16[16,16,1024]{2,1,0:T(8,128)(2,1)S(1)} async-done(((bf16[16,16,1024]{2,1,0:T(8,128)(2,1)}), bf16[16,16,1024]{2,1,0:T(8,128)(2,1)S(1)}, u32[]{:S(2)}, u32[]{:S(2)}) %all-to-all-start.2) | async-done | bytes 524320 | tf_op jit(solution)/shard_map/all_to_all | solution.py:26
  81.9 3.7 %shard_map.275 = bf16[2,16,8,1024]{3,2,1,0:T(8,128)(2,1)} custom-call(bf16[16,2,8,1024]{3,2,1,0:T(8,128)(2,1)S(1)} %bitcast.29, bf16[2048,512]{1,0:T(8,128)(2,1)S(1)} %shard_map.274.gate_ref, bf16[2048,512]{1,0:T(8,128)(2,1)} %bitcast.40, bf16[512,2048]{1,0:T(8,128)(2,1)} %bitcast.41), custom_call_target="tpu_custom_call" | custom-call | tf_op jit(solution)/shard_map/pallas_call | solution.py:40
  85.7 2.6 %all-to-all-start.3 = ((bf16[32,8,1024]{2,1,0:T(8,128)(2,1)}), bf16[32,8,1024]{2,1,0:T(8,128)(2,1)S(1)}, u32[]{:S(2)}, u32[]{:S(2)}) async-start(bf16[32,8,1024]{2,1,0:T(8,128)(2,1)} %bitcast.39), calls=%async_computation.3 | async-start | bytes 1048576 | tf_op jit(solution)/shard_map/all_to_all | solution.py:26
  89.2 4.6 %multiply_add_fusion = f32[8,8,128,128]{3,2,1,0:T(8,128)} fusion(f32[8,8,128,128]{3,2,1,0:T(8,128)} %refs_5_.1, f32[8,8,128]{2,1,0:T(8,128)S(1)} %copy.31, f32[8,8,128]{2,1,0:T(8,128)S(1)} %copy.30, f32[8,8]{1,0:T(8,128)S(1)} %get-tuple-element.36.refs_1_), kind=kLoop, calls=%fused_computation | loop fusion | flops 3145728 | bytes 8454400 | tf_op jit(solution)/shard_map/add | solution.py:642
  95.8 8.1 %all-to-all-done.3 = bf16[32,8,1024]{2,1,0:T(8,128)(2,1)S(1)} async-done(((bf16[32,8,1024]{2,1,0:T(8,128)(2,1)}), bf16[32,8,1024]{2,1,0:T(8,128)(2,1)S(1)}, u32[]{:S(2)}, u32[]{:S(2)}) %all-to-all-start.3) | async-done | bytes 524320 | tf_op jit(solution)/shard_map/all_to_all | solution.py:26
  (64 shorter events, 15.0 us)
Async XLA Ops:
  2.5 20.4 %all-to-all-start = ((bf16[32,8,512]{2,1,0:T(8,128)(2,1)}), bf16[32,8,512]{2,1,0:T(8,128)(2,1)S(1)}, u32[]{:S(2)}, u32[]{:S(2)}) async-start(bf16[32,8,512]{2,1,0:T(8,128)(2,1)} %get-tuple-element.28), calls=%async_computation | async-start | bytes 524288 | tf_op jit(solution)/shard_map/all_to_all | solution.py:26
  9.9 1.6 %collective-permute-start = (bf16[2,64,1024]{2,1,0:T(8,128)(2,1)S(1)}, bf16[2,64,1024]{2,1,0:T(8,128)(2,1)S(1)}, u32[]{:S(2)}, u32[]{:S(2)}) collective-permute-start(bf16[2,64,1024]{2,1,0:T(8,128)(2,1)S(1)} %get-tuple-element.30), channel_id=1, source_target_pairs={{0,1},{1,0},{2,3},{3,2},{4,5},{5,4},{6,7},{7,6},{8,9},{9,8},{10,11... | collective-permute-start | bytes 786440 | tf_op jit(solution)/shard_map/ppermute | solution.py:22
  10.3 36.9 %copy-start.6 = (s32[4]{0:T(128)}, s32[4]{0:T(128)S(1)}, u32[]{:S(2)}) copy-start(s32[4]{0:T(128)S(1)} %pad_add_fusion.at_ref) | copy-start | bytes 52
  12.1 7.4 %collective-permute-start.1 = (bf16[128,512]{1,0:T(8,128)(2,1)S(1)}, bf16[128,512]{1,0:T(8,128)(2,1)S(1)}, u32[]{:S(2)}, u32[]{:S(2)}) collective-permute-start(bf16[128,512]{1,0:T(8,128)(2,1)S(1)} %get-tuple-element.32), channel_id=1, source_target_pairs={{0,2},{1,3},{2,0},{3,1},{4,6},{5,7},{6,4},{7,5},{8,10},{9,11},{10,... | collective-permute-start | bytes 393224 | tf_op jit(solution)/shard_map/ppermute | solution.py:22
  13.9 9.0 %collective-permute-start.2 = (bf16[128,512]{1,0:T(8,128)(2,1)S(1)}, bf16[128,512]{1,0:T(8,128)(2,1)S(1)}, u32[]{:S(2)}, u32[]{:S(2)}) collective-permute-start(bf16[128,512]{1,0:T(8,128)(2,1)S(1)} %get-tuple-element.33), channel_id=1, source_target_pairs={{0,4},{1,5},{2,6},{3,7},{4,0},{5,1},{6,2},{7,3},{8,12},{9,13},{10,... | collective-permute-start | bytes 393224 | tf_op jit(solution)/shard_map/ppermute | solution.py:22
  15.4 7.6 %collective-permute-start.3 = (bf16[128,512]{1,0:T(8,128)(2,1)S(1)}, bf16[128,512]{1,0:T(8,128)(2,1)S(1)}, u32[]{:S(2)}, u32[]{:S(2)}) collective-permute-start(bf16[128,512]{1,0:T(8,128)(2,1)S(1)} %get-tuple-element.34), channel_id=1, source_target_pairs={{0,6},{1,7},{2,4},{3,5},{4,2},{5,3},{6,0},{7,1},{8,14},{9,15},{10,... | collective-permute-start | bytes 393224 | tf_op jit(solution)/shard_map/ppermute | solution.py:22
  15.6 13.0 %collective-permute-start.5 = (bf16[1,64,1024]{2,1,0:T(8,128)(2,1)}, bf16[1,64,1024]{2,1,0:T(8,128)(2,1)S(1)}, u32[]{:S(2)}, u32[]{:S(2)}) collective-permute-start(bf16[1,64,1024]{2,1,0:T(8,128)(2,1)} %bitcast.33), channel_id=1, source_target_pairs={{0,8},{1,9},{2,10},{3,11},{4,12},{5,13},{6,14},{7,15},{8,0},{9,1},... | collective-permute-start | bytes 393224 | tf_op jit(solution)/shard_map/ppermute | solution.py:22
  24.5 26.4 %all-to-all-start.1 = ((bf16[32,8,512]{2,1,0:T(8,128)(2,1)}), bf16[32,8,512]{2,1,0:T(8,128)(2,1)S(1)}, u32[]{:S(2)}, u32[]{:S(2)}) async-start(bf16[32,8,512]{2,1,0:T(8,128)(2,1)} %bitcast.37), calls=%async_computation.1 | async-start | bytes 524288 | tf_op jit(solution)/shard_map/all_to_all | solution.py:26
  29.6 11.9 %collective-permute-start.8 = (bf16[2,64,1024]{2,1,0:T(8,128)(2,1)S(1)}, bf16[2,64,1024]{2,1,0:T(8,128)(2,1)S(1)}, u32[]{:S(2)}, u32[]{:S(2)}) collective-permute-start(bf16[2,64,1024]{2,1,0:T(8,128)(2,1)S(1)} %shard_map.270.refs_0_), channel_id=1, source_target_pairs={{0,6},{1,7},{2,4},{3,5},{4,2},{5,3},{6,0},{7,1},{8,14},{9,15},{10,... | collective-permute-start | bytes 786440 | tf_op jit(solution)/shard_map/ppermute | solution.py:22
  32.3 14.3 %collective-permute-start.7 = (bf16[2,64,1024]{2,1,0:T(8,128)(2,1)S(1)}, bf16[2,64,1024]{2,1,0:T(8,128)(2,1)S(1)}, u32[]{:S(2)}, u32[]{:S(2)}) collective-permute-start(bf16[2,64,1024]{2,1,0:T(8,128)(2,1)S(1)} %shard_map.270.refs_0_), channel_id=1, source_target_pairs={{0,4},{1,5},{2,6},{3,7},{4,0},{5,1},{6,2},{7,3},{8,12},{9,13},{10,... | collective-permute-start | bytes 786440 | tf_op jit(solution)/shard_map/ppermute | solution.py:22
  32.9 13.8 %collective-permute-start.6 = (bf16[2,64,1024]{2,1,0:T(8,128)(2,1)S(1)}, bf16[2,64,1024]{2,1,0:T(8,128)(2,1)S(1)}, u32[]{:S(2)}, u32[]{:S(2)}) collective-permute-start(bf16[2,64,1024]{2,1,0:T(8,128)(2,1)S(1)} %shard_map.270.refs_0_), channel_id=1, source_target_pairs={{0,2},{1,3},{2,0},{3,1},{4,6},{5,7},{6,4},{7,5},{8,10},{9,11},{10,... | collective-permute-start | bytes 786440 | tf_op jit(solution)/shard_map/ppermute | solution.py:22
  33.1 23.1 %collective-permute-start.9 = (bf16[2,64,1024]{2,1,0:T(8,128)(2,1)S(1)}, bf16[2,64,1024]{2,1,0:T(8,128)(2,1)S(1)}, u32[]{:S(2)}, u32[]{:S(2)}) collective-permute-start(bf16[2,64,1024]{2,1,0:T(8,128)(2,1)S(1)} %shard_map.270.refs_0_), channel_id=1, source_target_pairs={{0,1},{1,0},{2,3},{3,2},{4,5},{5,4},{6,7},{7,6},{8,9},{9,8},{10,11... | collective-permute-start | bytes 786440 | tf_op jit(solution)/shard_map/ppermute | solution.py:22
  41.5 14.8 %collective-permute-start.12 = (bf16[2,64,1024]{2,1,0:T(8,128)(2,1)S(1)}, bf16[2,64,1024]{2,1,0:T(8,128)(2,1)S(1)}, u32[]{:S(2)}, u32[]{:S(2)}) collective-permute-start(bf16[2,64,1024]{2,1,0:T(8,128)(2,1)S(1)} %collective-permute-done.8.refs_3_), channel_id=1, source_target_pairs={{0,1},{1,0},{2,3},{3,2},{4,5},{5,4},{6,7},{7,6},{8,9},{9,8},{10,11... | collective-permute-start | bytes 786440 | tf_op jit(solution)/shard_map/ppermute | solution.py:22
  46.6 9.6 %collective-permute-start.11 = (bf16[2,64,1024]{2,1,0:T(8,128)(2,1)S(1)}, bf16[2,64,1024]{2,1,0:T(8,128)(2,1)}, u32[]{:S(2)}, u32[]{:S(2)}) collective-permute-start(bf16[2,64,1024]{2,1,0:T(8,128)(2,1)S(1)} %collective-permute-done.7.refs_2_), channel_id=1, source_target_pairs={{0,1},{1,0},{2,3},{3,2},{4,5},{5,4},{6,7},{7,6},{8,9},{9,8},{10,11... | collective-permute-start | bytes 786440 | tf_op jit(solution)/shard_map/ppermute | solution.py:22
  46.6 9.6 %collective-permute-start.10 = (bf16[2,64,1024]{2,1,0:T(8,128)(2,1)S(1)}, bf16[2,64,1024]{2,1,0:T(8,128)(2,1)}, u32[]{:S(2)}, u32[]{:S(2)}) collective-permute-start(bf16[2,64,1024]{2,1,0:T(8,128)(2,1)S(1)} %collective-permute-done.6.refs_1_), channel_id=1, source_target_pairs={{0,1},{1,0},{2,3},{3,2},{4,5},{5,4},{6,7},{7,6},{8,9},{9,8},{10,11... | collective-permute-start | bytes 786440 | tf_op jit(solution)/shard_map/ppermute | solution.py:22
  54.0 12.0 %copy-start.11 = (f32[1,2048]{1,0:T(1,128)S(1)}, f32[1,2048]{1,0:T(1,128)}, u32[]{:S(2)}) copy-start(f32[1,2048]{1,0:T(1,128)} %copy-done.10) | copy-start | bytes 24580
  54.0 12.0 %copy-start.13 = (f32[1,2048]{1,0:T(1,128)S(1)}, f32[1,2048]{1,0:T(1,128)}, u32[]{:S(2)}) copy-start(f32[1,2048]{1,0:T(1,128)} %copy-done.12) | copy-start | bytes 24580
  54.0 6.2 %collective-permute-start.4 = (bf16[8,3584]{1,0:T(8,128)(2,1)S(1)}, bf16[8,3584]{1,0:T(8,128)(2,1)S(1)}, u32[]{:S(2)}, u32[]{:S(2)}) collective-permute-start(bf16[8,3584]{1,0:T(8,128)(2,1)S(1)} %bitcast.35), channel_id=1, source_target_pairs={{0,16},{1,17},{2,18},{3,19},{4,20},{5,21},{6,22},{7,23},{8,24},{9,... | collective-permute-start | bytes 172040 | tf_op jit(solution)/shard_map/ppermute | solution.py:22
  60.8 5.2 %collective-permute-start.13 = (bf16[16,1024]{1,0:T(8,128)(2,1)S(1)}, bf16[16,1024]{1,0:T(8,128)(2,1)S(1)}, u32[]{:S(2)}, u32[]{:S(2)}) collective-permute-start(bf16[16,1024]{1,0:T(8,128)(2,1)S(1)} %shard_map.272.refs_0_), channel_id=1, source_target_pairs={{0,16},{1,17},{2,18},{3,19},{4,20},{5,21},{6,22},{7,23},{8,24},{9,... | collective-permute-start | bytes 98312 | tf_op jit(solution)/shard_map/ppermute | solution.py:22
  67.8 14.1 %all-to-all-start.2 = ((bf16[16,16,1024]{2,1,0:T(8,128)(2,1)}), bf16[16,16,1024]{2,1,0:T(8,128)(2,1)S(1)}, u32[]{:S(2)}, u32[]{:S(2)}) async-start(bf16[16,16,1024]{2,1,0:T(8,128)(2,1)} %bitcast.43), calls=%async_computation.2 | async-start | bytes 1048576 | tf_op jit(solution)/shard_map/all_to_all | solution.py:26
  81.9 6.5 %copy-start.14 = (f32[8,8,128]{2,1,0:T(8,128)S(1)}, f32[8,8,128]{2,1,0:T(8,128)}, u32[]{:S(2)}) copy-start(f32[8,8,128]{2,1,0:T(8,128)} %refs_3_.3) | copy-start | bytes 98308
  85.7 18.2 %all-to-all-start.3 = ((bf16[32,8,1024]{2,1,0:T(8,128)(2,1)}), bf16[32,8,1024]{2,1,0:T(8,128)(2,1)S(1)}, u32[]{:S(2)}, u32[]{:S(2)}) async-start(bf16[32,8,1024]{2,1,0:T(8,128)(2,1)} %bitcast.39), calls=%async_computation.3 | async-start | bytes 1048576 | tf_op jit(solution)/shard_map/all_to_all | solution.py:26
  93.8 10.1 %copy-start.5 = (bf16[32,256]{1,0:T(8,128)(2,1)S(1)}, bf16[32,256]{1,0:T(8,128)(2,1)}, u32[]{:S(2)}) copy-start(bf16[32,256]{1,0:T(8,128)(2,1)} %copy-done.4) | copy-start | bytes 49156
  93.8 10.1 %copy-start.9 = (f32[1,2048]{1,0:T(1,128)S(1)}, f32[1,2048]{1,0:T(1,128)}, u32[]{:S(2)}) copy-start(f32[1,2048]{1,0:T(1,128)} %copy-done.8) | copy-start | bytes 24580
  (9 other events, 26.2 us)

commit v5 on v4

--- a/solution.py
+++ b/solution.py
@@ -268,11 +268,13 @@
                 out_ref[place, :] = block[number]
 
 
-def mix_kernel(*refs):
-    depth = refs[-2].shape[1]
-    rows = jnp.concatenate([ref[:, :depth] for ref in refs[:-2]], axis=0)
-    refs[-1][...] = lax.dot_general(
-        rows, refs[-2][...], (((1,), (1,)), ((), ())), preferred_element_type=WIDE
+def mix_kernel(at_ref, *refs, blocks):
+    out_ref, held_ref = refs[-2:]
+    stack_kernel(at_ref, *refs[:blocks], held_ref)
+    depth = held_ref.shape[1]
+    rows = jnp.concatenate([ref[:, :depth] for ref in refs[blocks:-2]], axis=0)
+    out_ref[...] = lax.dot_general(
+        rows, held_ref[...], (((1,), (1,)), ((), ())), preferred_element_type=WIDE
     ).astype(HALF)
 
 
@@ -486,12 +488,9 @@
     )
     ours = [pair] + [swap(pair, CORE * 2 * turn) for turn in range(1, chips)]
     theirs = [swap(block, CORE) for block in ours]
-    (mix_weight,) = local_call(
-        stack_kernel,
-        [((2 * piece_width, heads * width), HALF, "v")],
-        (at, *ours, *theirs),
-        "s" + "v" * 2 * chips,
-    )
+    out_blocks = (*ours, *theirs)
+    mix = functools.partial(mix_kernel, blocks=len(out_blocks))
+    mix_scratch = [pltpu.VMEM((2 * piece_width, heads * width), HALF)]
 
     small = (
         ingate_weight.T,
@@ -560,9 +559,11 @@
     if groups == 2:
         gated_rows = [gated[0], swap(gated[0], 2 * heads)]
         (own_mixed,) = local_call(
-            mix_kernel,
+            mix,
             [((2 * sequences, 2 * piece_width), HALF, "v")],
-            (*gated_rows, mix_weight),
+            (at, *out_blocks, *gated_rows),
+            "s" + "v" * (len(out_blocks) + 2),
+            mix_scratch,
         )
         mixed = [own_mixed, swap(own_mixed, 2 * heads)]
         if not paired:
@@ -576,9 +577,11 @@
         lines = [[low + 2 * heads * at for at in range(groups)] for low in range(2 * heads)]
         gathered = exchange(gated, lines).reshape(groups * sequences, heads * width)
         (mixed,) = local_call(
-            mix_kernel,
+            mix,
             [((groups * sequences, 2 * piece_width), HALF, "h")],
-            (gathered, mix_weight),
+            (at, *out_blocks, gathered),
+            "s" + "v" * (len(out_blocks) + 1),
+            mix_scratch,
         )
         mixed = exchange(mixed.reshape(groups, sequences, 2 * piece_width), lines)
         mixed = [mixed[number] for number in range(groups)]

time: 105 us -> 107 us (1.019)
  waiting for transfers between devices: 44 us -> 45.2 us
    ppermute x14, waiting for transfers between devices: 27 us -> 28.2 us  [swap(): return lax.ppermute(values, 'ep', [(i, i ^ bit) for i in range(devices)])]
    pallas_call x14 -> x13, Pallas kernels: 21.2 us -> 21.2 us  [local_call(): pl.pallas_call(body, out_shape=[SPACES[space](shape, kind) for shape, kin...]
  transfers between devices with their start and end apart: 18 -> 18, of which waited for: 9 -> 9; matrix products, arithmetic and copies ran while one was open for 5% -> 5% of each run, Pallas kernels for 12% -> 10%
where the time goes in v5:
time: 107 us; the launch traced here: 106 us
  waiting for transfers between devices  45.2 us (42%)
  starting transfers between devices  30.6 us (29%)
  Pallas kernels  21.2 us (20%)
  other arithmetic  4.77 us (4%)
  local copies, waits for them, and re-layouts  3.3 us (3%)
    ppermute x14, waiting for transfers between devices, swap(): return lax.ppermute(values, 'ep', [(i, i ^ bit) for i in range(devices)])  28.2 us
    pallas_call x13, Pallas kernels, local_call(): pl.pallas_call(body, out_shape=[SPACES[space](shape, kind) for shape, kin...  21.2 us
    all_to_all x4, starting transfers between devices, exchange(): lax.all_to_all(values, 'ep', split_axis=0, concat_axis=0, tiled=True, axi...  17.6 us
    all_to_all x4, waiting for transfers between devices, exchange(): lax.all_to_all(values, 'ep', split_axis=0, concat_axis=0, tiled=True, axi...  17 us
    ppermute x14, starting transfers between devices, swap(): return lax.ppermute(values, 'ep', [(i, i ^ bit) for i in range(devices)])  13 us
    add x1, other arithmetic, on_device(): keep_old[..., None, None] * memory_state  4.6 us
    unnamed x31, local copies, waits for them, and re-layouts  3.15 us
  transfers between devices with their start and end apart: 18, of which 9 were waited for; matrix products, arithmetic and copies ran while one was open for 5% of the time, Pallas kernels for 10%

profile of v5, /device:TPU:0, one launch (start us, length us, event | category | flops | bytes accessed | tf_op | source)
XLA Modules:
  0.0 106.0 jit_solution(5232767038724810240)
XLA Ops:
  0.6 1.9 %shard_map.265 = (bf16[2,64,1024]{2,1,0:T(8,128)(2,1)S(1)}, bf16[2,64,1024]{2,1,0:T(8,128)(2,1)S(1)}, bf16[8,2048]{1,0:T(8,128)(2,1)S(1)}, bf16[8,2048]{1,0:T(8,128)(2,1)S(1)}, bf16[32,8,512]{2,1,0:T(8,128)(2,1)}) custom-call(bf16[8,2048]{1,0:T(8,128)(2,1)} %tokens_ref.1, f32[1,2048]{1,0:T(1,128)} %bitcast.46, bf16[64,1024]{1,0:T(8,128)(2,1)} %refs_0_.1, ...), custom_call_target="tpu_custom_call" | custom-call | tf_op jit(solution)/shard_map/pallas_call | solution.py:40
  2.5 7.3 %all-to-all-start = ((bf16[32,8,512]{2,1,0:T(8,128)(2,1)}), bf16[32,8,512]{2,1,0:T(8,128)(2,1)S(1)}, u32[]{:S(2)}, u32[]{:S(2)}) async-start(bf16[32,8,512]{2,1,0:T(8,128)(2,1)} %get-tuple-element.28), calls=%async_computation | async-start | bytes 524288 | tf_op jit(solution)/shard_map/all_to_all | solution.py:26
  12.1 1.8 %collective-permute-start.9 = (bf16[128,512]{1,0:T(8,128)(2,1)S(1)}, bf16[128,512]{1,0:T(8,128)(2,1)S(1)}, u32[]{:S(2)}, u32[]{:S(2)}) collective-permute-start(bf16[128,512]{1,0:T(8,128)(2,1)S(1)} %get-tuple-element.32), channel_id=1, source_target_pairs={{0,2},{1,3},{2,0},{3,1},{4,6},{5,7},{6,4},{7,5},{8,10},{9,11},{10,... | collective-permute-start | bytes 393224 | tf_op jit(solution)/shard_map/ppermute | solution.py:22
  15.6 1.8 %collective-permute-start = (bf16[1,64,1024]{2,1,0:T(8,128)(2,1)}, bf16[1,64,1024]{2,1,0:T(8,128)(2,1)S(1)}, u32[]{:S(2)}, u32[]{:S(2)}) collective-permute-start(bf16[1,64,1024]{2,1,0:T(8,128)(2,1)} %bitcast.33), channel_id=1, source_target_pairs={{0,8},{1,9},{2,10},{3,11},{4,12},{5,13},{6,14},{7,15},{8,0},{9,1},... | collective-permute-start | bytes 393224 | tf_op jit(solution)/shard_map/ppermute | solution.py:22
  17.4 2.1 %collective-permute-done.9.refs_1_ = bf16[128,512]{1,0:T(8,128)(2,1)S(1)} collective-permute-done((bf16[128,512]{1,0:T(8,128)(2,1)S(1)}, bf16[128,512]{1,0:T(8,128)(2,1)S(1)}, u32[]{:S(2)}, u32[]{:S(2)}) %collective-permute-start.9) | collective-permute-done | bytes 131104 | tf_op jit(solution)/shard_map/ppermute | solution.py:22
  19.5 3.4 %collective-permute-done.10.refs_2_ = bf16[128,512]{1,0:T(8,128)(2,1)S(1)} collective-permute-done((bf16[128,512]{1,0:T(8,128)(2,1)S(1)}, bf16[128,512]{1,0:T(8,128)(2,1)S(1)}, u32[]{:S(2)}, u32[]{:S(2)}) %collective-permute-start.10) | collective-permute-done | bytes 131104 | tf_op jit(solution)/shard_map/ppermute | solution.py:22
  24.5 4.1 %all-to-all-start.1 = ((bf16[32,8,512]{2,1,0:T(8,128)(2,1)}), bf16[32,8,512]{2,1,0:T(8,128)(2,1)S(1)}, u32[]{:S(2)}, u32[]{:S(2)}) async-start(bf16[32,8,512]{2,1,0:T(8,128)(2,1)} %bitcast.37), calls=%async_computation.1 | async-start | bytes 524288 | tf_op jit(solution)/shard_map/all_to_all | solution.py:26
  29.6 2.7 %collective-permute-start.3 = (bf16[2,64,1024]{2,1,0:T(8,128)(2,1)S(1)}, bf16[2,64,1024]{2,1,0:T(8,128)(2,1)S(1)}, u32[]{:S(2)}, u32[]{:S(2)}) collective-permute-start(bf16[2,64,1024]{2,1,0:T(8,128)(2,1)S(1)} %shard_map.264.refs_0_), channel_id=1, source_target_pairs={{0,6},{1,7},{2,4},{3,5},{4,2},{5,3},{6,0},{7,1},{8,14},{9,15},{10,... | collective-permute-start | bytes 786440 | tf_op jit(solution)/shard_map/ppermute | solution.py:22
  33.1 8.3 %collective-permute-done.3.refs_3_ = bf16[2,64,1024]{2,1,0:T(8,128)(2,1)S(1)} collective-permute-done((bf16[2,64,1024]{2,1,0:T(8,128)(2,1)S(1)}, bf16[2,64,1024]{2,1,0:T(8,128)(2,1)S(1)}, u32[]{:S(2)}, u32[]{:S(2)}) %collective-permute-start.3) | collective-permute-done | bytes 262176 | tf_op jit(solution)/shard_map/ppermute | solution.py:22
  41.5 5.1 %collective-permute-done.2.refs_2_ = bf16[2,64,1024]{2,1,0:T(8,128)(2,1)S(1)} collective-permute-done((bf16[2,64,1024]{2,1,0:T(8,128)(2,1)S(1)}, bf16[2,64,1024]{2,1,0:T(8,128)(2,1)S(1)}, u32[]{:S(2)}, u32[]{:S(2)}) %collective-permute-start.2) | collective-permute-done | bytes 262176 | tf_op jit(solution)/shard_map/ppermute | solution.py:22
  47.1 1.7 %shard_map.268 = (f32[8,8]{1,0:T(8,128)S(1)}, f32[8,8]{1,0:T(8,128)S(1)}, f32[8,8]{1,0:T(8,128)}, bf16[16,256]{1,0:T(8,128)(2,1)S(1)}, bf16[32,256]{1,0:T(8,128)...) custom-call(bf16[8,2048]{1,0:T(8,128)(2,1)S(1)} %get-tuple-element.3, ...), custom_call_target="tpu_custom_call" | custom-call | tf_op jit(solution)/shard_map/pallas_call | solution.py:40
  51.0 3.1 %shard_map.270 = (bf16[1,8,3584]{2,1,0:T(8,128)(2,1)S(1)}, f32[8,8,128]{2,1,0:T(8,128)S(1)}, f32[8,8,128]{2,1,0:T(8,128)S(1)}) custom-call(bf16[32,8,512]{2,1,0:T(8,128)(2,1)S(1)} %all-to-all-done.1.refs_0_, f32[8,8]{1,0:T(8,128)S(1)} %get-tuple-element.36.refs_1_, f32[8,8]{1,0:T(8,128)S(1)} %get-tuple-element.37.refs_2_, ...), custom_call_target="tpu_custom_call" | custom-call | tf_op jit(solution)/shard_map/pallas_call | solution.py:40
  54.0 2.2 %collective-permute-start.12 = (bf16[8,3584]{1,0:T(8,128)(2,1)S(1)}, bf16[8,3584]{1,0:T(8,128)(2,1)S(1)}, u32[]{:S(2)}, u32[]{:S(2)}) collective-permute-start(bf16[8,3584]{1,0:T(8,128)(2,1)S(1)} %bitcast.35), channel_id=1, source_target_pairs={{0,16},{1,17},{2,18},{3,19},{4,20},{5,21},{6,22},{7,23},{8,24},{9,... | collective-permute-start | bytes 172040 | tf_op jit(solution)/shard_map/ppermute | solution.py:22
  56.3 3.9 %collective-permute-done.12.refs_9_.refs_4_ = bf16[8,3584]{1,0:T(8,128)(2,1)S(1)} collective-permute-done((bf16[8,3584]{1,0:T(8,128)(2,1)S(1)}, bf16[8,3584]{1,0:T(8,128)(2,1)S(1)}, u32[]{:S(2)}, u32[]{:S(2)}) %collective-permute-start.12) | collective-permute-done | bytes 57376 | tf_op jit(solution)/shard_map/ppermute | solution.py:22
  60.2 1.8 %shard_map.271.refs_0_ = bf16[16,1024]{1,0:T(8,128)(2,1)S(1)} custom-call(s32[4]{0:T(128)S(1)} %copy-done.7, bf16[2,64,1024]{2,1,0:T(8,128)(2,1)S(1)} %shard_map.264.refs_0_, bf16[2,64,1024]{2,1,0:T(8,128)(2,1)S(1)} %collective-permute-done.1.refs_1_, bf16[2,64,1024]{2,1,0:T(8,128)(2,1)S(1)} %collective-permute-done.2.refs_2_, ...), custom_call_target="tpu_custom_call" | custom-call | tf_op jit(solution)/shard_map/pallas_call | solution.py:40
  63.2 4.0 %collective-permute-done.13.refs_1_ = bf16[16,1024]{1,0:T(8,128)(2,1)S(1)} collective-permute-done((bf16[16,1024]{1,0:T(8,128)(2,1)S(1)}, bf16[16,1024]{1,0:T(8,128)(2,1)S(1)}, u32[]{:S(2)}, u32[]{:S(2)}) %collective-permute-start.13) | collective-permute-done | bytes 32800 | tf_op jit(solution)/shard_map/ppermute | solution.py:22
  67.2 1.8 %shard_map.272 = (bf16[8,2048]{1,0:T(8,128)(2,1)S(1)}, bf16[8,2048]{1,0:T(8,128)(2,1)S(1)}, bf16[16,2,8,1024]{3,2,1,0:T(8,128)(2,1)}) custom-call(s32[4]{0:T(128)S(1)} %copy-done.7, bf16[16,1024]{1,0:T(8,128)(2,1)S(1)} %shard_map.271.refs_0_, bf16[16,1024]{1,0:T(8,128)(2,1)S(1)} %collective-permute-done.13.refs_1_, ...), custom_call_target="tpu_custom_call" | custom-call | tf_op jit(solution)/shard_map/pallas_call | solution.py:40
  69.0 3.6 %all-to-all-start.2 = ((bf16[16,16,1024]{2,1,0:T(8,128)(2,1)}), bf16[16,16,1024]{2,1,0:T(8,128)(2,1)S(1)}, u32[]{:S(2)}, u32[]{:S(2)}) async-start(bf16[16,16,1024]{2,1,0:T(8,128)(2,1)} %bitcast.43), calls=%async_computation.2 | async-start | bytes 1048576 | tf_op jit(solution)/shard_map/all_to_all | solution.py:26
  72.6 1.6 %shard_map.273.gate_ref = bf16[2048,512]{1,0:T(8,128)(2,1)S(1)} custom-call(bf16[8,2048]{1,0:T(8,128)(2,1)S(1)} %get-tuple-element.45.after_ref, bf16[2048,512]{1,0:T(8,128)(2,1)} %bitcast.42), custom_call_target="tpu_custom_call" | custom-call | tf_op jit(solution)/shard_map/pallas_call | solution.py:40
  74.2 8.9 %all-to-all-done.2 = bf16[16,16,1024]{2,1,0:T(8,128)(2,1)S(1)} async-done(((bf16[16,16,1024]{2,1,0:T(8,128)(2,1)}), bf16[16,16,1024]{2,1,0:T(8,128)(2,1)S(1)}, u32[]{:S(2)}, u32[]{:S(2)}) %all-to-all-start.2) | async-done | bytes 524320 | tf_op jit(solution)/shard_map/all_to_all | solution.py:26
  83.1 3.7 %shard_map.274 = bf16[2,16,8,1024]{3,2,1,0:T(8,128)(2,1)} custom-call(bf16[16,2,8,1024]{3,2,1,0:T(8,128)(2,1)S(1)} %bitcast.29, bf16[2048,512]{1,0:T(8,128)(2,1)S(1)} %shard_map.273.gate_ref, bf16[2048,512]{1,0:T(8,128)(2,1)} %bitcast.40, bf16[512,2048]{1,0:T(8,128)(2,1)} %bitcast.41), custom_call_target="tpu_custom_call" | custom-call | tf_op jit(solution)/shard_map/pallas_call | solution.py:40
  86.8 2.6 %all-to-all-start.3 = ((bf16[32,8,1024]{2,1,0:T(8,128)(2,1)}), bf16[32,8,1024]{2,1,0:T(8,128)(2,1)S(1)}, u32[]{:S(2)}, u32[]{:S(2)}) async-start(bf16[32,8,1024]{2,1,0:T(8,128)(2,1)} %bitcast.39), calls=%async_computation.3 | async-start | bytes 1048576 | tf_op jit(solution)/shard_map/all_to_all | solution.py:26
  90.4 4.6 %multiply_add_fusion = f32[8,8,128,128]{3,2,1,0:T(8,128)} fusion(f32[8,8,128,128]{3,2,1,0:T(8,128)} %refs_5_.1, f32[8,8,128]{2,1,0:T(8,128)S(1)} %copy.31, f32[8,8,128]{2,1,0:T(8,128)S(1)} %copy.30, f32[8,8]{1,0:T(8,128)S(1)} %get-tuple-element.36.refs_1_), kind=kLoop, calls=%fused_computation | loop fusion | flops 3145728 | bytes 8454400 | tf_op jit(solution)/shard_map/add | solution.py:645
  97.0 8.1 %all-to-all-done.3 = bf16[32,8,1024]{2,1,0:T(8,128)(2,1)S(1)} async-done(((bf16[32,8,1024]{2,1,0:T(8,128)(2,1)}), bf16[32,8,1024]{2,1,0:T(8,128)(2,1)S(1)}, u32[]{:S(2)}, u32[]{:S(2)}) %all-to-all-start.3) | async-done | bytes 524320 | tf_op jit(solution)/shard_map/all_to_all | solution.py:26
  (63 shorter events, 14.8 us)
Async XLA Ops:
  2.5 20.4 %all-to-all-start = ((bf16[32,8,512]{2,1,0:T(8,128)(2,1)}), bf16[32,8,512]{2,1,0:T(8,128)(2,1)S(1)}, u32[]{:S(2)}, u32[]{:S(2)}) async-start(bf16[32,8,512]{2,1,0:T(8,128)(2,1)} %get-tuple-element.28), calls=%async_computation | async-start | bytes 524288 | tf_op jit(solution)/shard_map/all_to_all | solution.py:26
  9.9 1.6 %collective-permute-start.8 = (bf16[2,64,1024]{2,1,0:T(8,128)(2,1)S(1)}, bf16[2,64,1024]{2,1,0:T(8,128)(2,1)S(1)}, u32[]{:S(2)}, u32[]{:S(2)}) collective-permute-start(bf16[2,64,1024]{2,1,0:T(8,128)(2,1)S(1)} %get-tuple-element.30), channel_id=1, source_target_pairs={{0,1},{1,0},{2,3},{3,2},{4,5},{5,4},{6,7},{7,6},{8,9},{9,8},{10,11... | collective-permute-start | bytes 786440 | tf_op jit(solution)/shard_map/ppermute | solution.py:22
  10.3 36.9 %copy-start.6 = (s32[4]{0:T(128)}, s32[4]{0:T(128)S(1)}, u32[]{:S(2)}) copy-start(s32[4]{0:T(128)S(1)} %pad_add_fusion.at_ref) | copy-start | bytes 52
  12.1 7.4 %collective-permute-start.9 = (bf16[128,512]{1,0:T(8,128)(2,1)S(1)}, bf16[128,512]{1,0:T(8,128)(2,1)S(1)}, u32[]{:S(2)}, u32[]{:S(2)}) collective-permute-start(bf16[128,512]{1,0:T(8,128)(2,1)S(1)} %get-tuple-element.32), channel_id=1, source_target_pairs={{0,2},{1,3},{2,0},{3,1},{4,6},{5,7},{6,4},{7,5},{8,10},{9,11},{10,... | collective-permute-start | bytes 393224 | tf_op jit(solution)/shard_map/ppermute | solution.py:22
  13.9 9.0 %collective-permute-start.10 = (bf16[128,512]{1,0:T(8,128)(2,1)S(1)}, bf16[128,512]{1,0:T(8,128)(2,1)S(1)}, u32[]{:S(2)}, u32[]{:S(2)}) collective-permute-start(bf16[128,512]{1,0:T(8,128)(2,1)S(1)} %get-tuple-element.33), channel_id=1, source_target_pairs={{0,4},{1,5},{2,6},{3,7},{4,0},{5,1},{6,2},{7,3},{8,12},{9,13},{10,... | collective-permute-start | bytes 393224 | tf_op jit(solution)/shard_map/ppermute | solution.py:22
  15.4 7.6 %collective-permute-start.11 = (bf16[128,512]{1,0:T(8,128)(2,1)S(1)}, bf16[128,512]{1,0:T(8,128)(2,1)S(1)}, u32[]{:S(2)}, u32[]{:S(2)}) collective-permute-start(bf16[128,512]{1,0:T(8,128)(2,1)S(1)} %get-tuple-element.34), channel_id=1, source_target_pairs={{0,6},{1,7},{2,4},{3,5},{4,2},{5,3},{6,0},{7,1},{8,14},{9,15},{10,... | collective-permute-start | bytes 393224 | tf_op jit(solution)/shard_map/ppermute | solution.py:22
  15.6 13.0 %collective-permute-start = (bf16[1,64,1024]{2,1,0:T(8,128)(2,1)}, bf16[1,64,1024]{2,1,0:T(8,128)(2,1)S(1)}, u32[]{:S(2)}, u32[]{:S(2)}) collective-permute-start(bf16[1,64,1024]{2,1,0:T(8,128)(2,1)} %bitcast.33), channel_id=1, source_target_pairs={{0,8},{1,9},{2,10},{3,11},{4,12},{5,13},{6,14},{7,15},{8,0},{9,1},... | collective-permute-start | bytes 393224 | tf_op jit(solution)/shard_map/ppermute | solution.py:22
  24.5 26.4 %all-to-all-start.1 = ((bf16[32,8,512]{2,1,0:T(8,128)(2,1)}), bf16[32,8,512]{2,1,0:T(8,128)(2,1)S(1)}, u32[]{:S(2)}, u32[]{:S(2)}) async-start(bf16[32,8,512]{2,1,0:T(8,128)(2,1)} %bitcast.37), calls=%async_computation.1 | async-start | bytes 524288 | tf_op jit(solution)/shard_map/all_to_all | solution.py:26
  29.6 11.9 %collective-permute-start.3 = (bf16[2,64,1024]{2,1,0:T(8,128)(2,1)S(1)}, bf16[2,64,1024]{2,1,0:T(8,128)(2,1)S(1)}, u32[]{:S(2)}, u32[]{:S(2)}) collective-permute-start(bf16[2,64,1024]{2,1,0:T(8,128)(2,1)S(1)} %shard_map.264.refs_0_), channel_id=1, source_target_pairs={{0,6},{1,7},{2,4},{3,5},{4,2},{5,3},{6,0},{7,1},{8,14},{9,15},{10,... | collective-permute-start | bytes 786440 | tf_op jit(solution)/shard_map/ppermute | solution.py:22
  32.3 14.3 %collective-permute-start.2 = (bf16[2,64,1024]{2,1,0:T(8,128)(2,1)S(1)}, bf16[2,64,1024]{2,1,0:T(8,128)(2,1)S(1)}, u32[]{:S(2)}, u32[]{:S(2)}) collective-permute-start(bf16[2,64,1024]{2,1,0:T(8,128)(2,1)S(1)} %shard_map.264.refs_0_), channel_id=1, source_target_pairs={{0,4},{1,5},{2,6},{3,7},{4,0},{5,1},{6,2},{7,3},{8,12},{9,13},{10,... | collective-permute-start | bytes 786440 | tf_op jit(solution)/shard_map/ppermute | solution.py:22
  32.9 13.8 %collective-permute-start.1 = (bf16[2,64,1024]{2,1,0:T(8,128)(2,1)S(1)}, bf16[2,64,1024]{2,1,0:T(8,128)(2,1)S(1)}, u32[]{:S(2)}, u32[]{:S(2)}) collective-permute-start(bf16[2,64,1024]{2,1,0:T(8,128)(2,1)S(1)} %shard_map.264.refs_0_), channel_id=1, source_target_pairs={{0,2},{1,3},{2,0},{3,1},{4,6},{5,7},{6,4},{7,5},{8,10},{9,11},{10,... | collective-permute-start | bytes 786440 | tf_op jit(solution)/shard_map/ppermute | solution.py:22
  33.1 23.1 %collective-permute-start.4 = (bf16[2,64,1024]{2,1,0:T(8,128)(2,1)S(1)}, bf16[2,64,1024]{2,1,0:T(8,128)(2,1)S(1)}, u32[]{:S(2)}, u32[]{:S(2)}) collective-permute-start(bf16[2,64,1024]{2,1,0:T(8,128)(2,1)S(1)} %shard_map.264.refs_0_), channel_id=1, source_target_pairs={{0,1},{1,0},{2,3},{3,2},{4,5},{5,4},{6,7},{7,6},{8,9},{9,8},{10,11... | collective-permute-start | bytes 786440 | tf_op jit(solution)/shard_map/ppermute | solution.py:22
  41.5 14.8 %collective-permute-start.7 = (bf16[2,64,1024]{2,1,0:T(8,128)(2,1)S(1)}, bf16[2,64,1024]{2,1,0:T(8,128)(2,1)S(1)}, u32[]{:S(2)}, u32[]{:S(2)}) collective-permute-start(bf16[2,64,1024]{2,1,0:T(8,128)(2,1)S(1)} %collective-permute-done.3.refs_3_), channel_id=1, source_target_pairs={{0,1},{1,0},{2,3},{3,2},{4,5},{5,4},{6,7},{7,6},{8,9},{9,8},{10,11... | collective-permute-start | bytes 786440 | tf_op jit(solution)/shard_map/ppermute | solution.py:22
  46.6 9.6 %collective-permute-start.6 = (bf16[2,64,1024]{2,1,0:T(8,128)(2,1)S(1)}, bf16[2,64,1024]{2,1,0:T(8,128)(2,1)}, u32[]{:S(2)}, u32[]{:S(2)}) collective-permute-start(bf16[2,64,1024]{2,1,0:T(8,128)(2,1)S(1)} %collective-permute-done.2.refs_2_), channel_id=1, source_target_pairs={{0,1},{1,0},{2,3},{3,2},{4,5},{5,4},{6,7},{7,6},{8,9},{9,8},{10,11... | collective-permute-start | bytes 786440 | tf_op jit(solution)/shard_map/ppermute | solution.py:22
  46.6 9.6 %collective-permute-start.5 = (bf16[2,64,1024]{2,1,0:T(8,128)(2,1)S(1)}, bf16[2,64,1024]{2,1,0:T(8,128)(2,1)}, u32[]{:S(2)}, u32[]{:S(2)}) collective-permute-start(bf16[2,64,1024]{2,1,0:T(8,128)(2,1)S(1)} %collective-permute-done.1.refs_1_), channel_id=1, source_target_pairs={{0,1},{1,0},{2,3},{3,2},{4,5},{5,4},{6,7},{7,6},{8,9},{9,8},{10,11... | collective-permute-start | bytes 786440 | tf_op jit(solution)/shard_map/ppermute | solution.py:22
  50.9 9.3 %copy-start.7 = (s32[4]{0:T(128)S(1)}, s32[4]{0:T(128)}, u32[]{:S(2)}) copy-start(s32[4]{0:T(128)} %copy-done.6) | copy-start | bytes 52
  50.9 16.3 %copy-start.13 = (f32[1,2048]{1,0:T(1,128)S(1)}, f32[1,2048]{1,0:T(1,128)}, u32[]{:S(2)}) copy-start(f32[1,2048]{1,0:T(1,128)} %copy-done.12) | copy-start | bytes 24580
  51.0 16.2 %copy-start.11 = (f32[1,2048]{1,0:T(1,128)S(1)}, f32[1,2048]{1,0:T(1,128)}, u32[]{:S(2)}) copy-start(f32[1,2048]{1,0:T(1,128)} %copy-done.10) | copy-start | bytes 24580
  54.0 6.2 %collective-permute-start.12 = (bf16[8,3584]{1,0:T(8,128)(2,1)S(1)}, bf16[8,3584]{1,0:T(8,128)(2,1)S(1)}, u32[]{:S(2)}, u32[]{:S(2)}) collective-permute-start(bf16[8,3584]{1,0:T(8,128)(2,1)S(1)} %bitcast.35), channel_id=1, source_target_pairs={{0,16},{1,17},{2,18},{3,19},{4,20},{5,21},{6,22},{7,23},{8,24},{9,... | collective-permute-start | bytes 172040 | tf_op jit(solution)/shard_map/ppermute | solution.py:22
  62.0 5.2 %collective-permute-start.13 = (bf16[16,1024]{1,0:T(8,128)(2,1)S(1)}, bf16[16,1024]{1,0:T(8,128)(2,1)S(1)}, u32[]{:S(2)}, u32[]{:S(2)}) collective-permute-start(bf16[16,1024]{1,0:T(8,128)(2,1)S(1)} %shard_map.271.refs_0_), channel_id=1, source_target_pairs={{0,16},{1,17},{2,18},{3,19},{4,20},{5,21},{6,22},{7,23},{8,24},{9,... | collective-permute-start | bytes 98312 | tf_op jit(solution)/shard_map/ppermute | solution.py:22
  69.0 14.1 %all-to-all-start.2 = ((bf16[16,16,1024]{2,1,0:T(8,128)(2,1)}), bf16[16,16,1024]{2,1,0:T(8,128)(2,1)S(1)}, u32[]{:S(2)}, u32[]{:S(2)}) async-start(bf16[16,16,1024]{2,1,0:T(8,128)(2,1)} %bitcast.43), calls=%async_computation.2 | async-start | bytes 1048576 | tf_op jit(solution)/shard_map/all_to_all | solution.py:26
  86.8 18.2 %all-to-all-start.3 = ((bf16[32,8,1024]{2,1,0:T(8,128)(2,1)}), bf16[32,8,1024]{2,1,0:T(8,128)(2,1)S(1)}, u32[]{:S(2)}, u32[]{:S(2)}) async-start(bf16[32,8,1024]{2,1,0:T(8,128)(2,1)} %bitcast.39), calls=%async_computation.3 | async-start | bytes 1048576 | tf_op jit(solution)/shard_map/all_to_all | solution.py:26
  95.0 10.1 %copy-start.5 = (bf16[32,256]{1,0:T(8,128)(2,1)S(1)}, bf16[32,256]{1,0:T(8,128)(2,1)}, u32[]{:S(2)}) copy-start(bf16[32,256]{1,0:T(8,128)(2,1)} %copy-done.4) | copy-start | bytes 49156
  95.0 10.1 %copy-start.9 = (f32[1,2048]{1,0:T(1,128)S(1)}, f32[1,2048]{1,0:T(1,128)}, u32[]{:S(2)}) copy-start(f32[1,2048]{1,0:T(1,128)} %copy-done.8) | copy-start | bytes 24580
  (9 other events, 27.4 us)
